TPU v7x, 256 devices: a whole 4x4x8 slice. The times are simulated.
256 devices in a mesh: ep: 128 (over z, y, x), tp: 2 (over core).
Axes of the slice: x: 4, y: 4, z: 8, core: 2. Of those that a mesh axis runs over, the one named last changes fastest.
Arguments:
- tokens: bfloat16 [1024, 2048], P('ep'), may hold values from -6 to 6
- first_gain: bfloat16 [2048], replicated, may hold values from 0.099609375 to 1.8984375
- query_weight: bfloat16 [2048, 256], P(None, 'tp'), may hold values from -0.125 to 0.125
- key_weight: bfloat16 [2048, 256], P(None, 'tp'), may hold values from -0.125 to 0.125
- value_weight: bfloat16 [2048, 512], P(None, 'tp'), may hold values from -0.125 to 0.125
- decay_down: bfloat16 [2048, 16], replicated, may hold values from -0.125 to 0.125
- decay_up: bfloat16 [16, 256], P(None, 'tp'), may hold values from -5 to 5
- decay_bias: float32 [256], P('tp'), may hold values from -12 to 4
- head_gain: bfloat16 [256], replicated, may hold values from 0.099609375 to 1.8984375
- recurrent_state: float32 [1024, 2, 128, 256], P('ep', 'tp'), may hold values from -6 to 6
- out_weight: bfloat16 [512, 2048], P('tp'), may hold values from -0.25 to 0.25
- second_gain: bfloat16 [2048], replicated, may hold values from 0.099609375 to 1.8984375
- expert_ids: int32 [1024, 6], P('ep'), may hold values from 0 to 127, all different within a row; in each aligned block of 8 rows (0 to 7, 8 to 15, ...) at most 2 rows name the same one
- route_weights: float32 [1024, 6], P('ep'), may hold values from 0.1 to 1
- expert_gate: bfloat16 [128, 2048, 256], P('ep', None, 'tp'), may hold values from -0.125 to 0.125
- expert_up: bfloat16 [128, 2048, 256], P('ep', None, 'tp'), may hold values from -0.125 to 0.125
- expert_down: bfloat16 [128, 256, 2048], P('ep', 'tp'), may hold values from -0.375 to 0.375
- dense_gate: bfloat16 [2048, 512], P('ep', 'tp'), may hold values from -0.5 to 0.5
- dense_up: bfloat16 [2048, 512], P('ep', 'tp'), may hold values from -0.5 to 0.5
- dense_down: bfloat16 [512, 2048], P('tp', 'ep'), may hold values from -0.25 to 0.25
- branch_gate: bfloat16 [2048], replicated, may hold values from -0.125 to 0.125
Outputs:
- layer_out: bfloat16 [1024, 2048], P('ep', 'tp')
Inputs may be any that keep to these rules, and one draw needn't show every extreme that they name: `expert_ids`: each row names 6 different experts. Within the 8 rows of one index of ep no expert is named by more than 2 rows, a bound that some block reaches.
All inputs are finite; a program needn't handle non-finite values.
Results may differ from a plain program's by a relative error of at most 0.015.
Values may be sent and summed in bfloat16 or wider, within the bound.
No kernel may reach another device: no remote copies, remote signals or barrier semaphores. Data moves between devices by JAX's collectives and lax.ppermute only.
A program may use at most 128 MiB of HBM per device.

v0:
```python
import jax
import jax.numpy as jnp
from jax import lax
from jax.sharding import Mesh
from jax.sharding import PartitionSpec as P

DK = 128
DV = 256
TOPK = 6
EP = ("ep_0", "ep_1", "ep_2")


EPS = 1e-06


def sent_to_all(array, axis):
    devices = lax.axis_size(axis)
    return lax.all_to_all(
        jnp.broadcast_to(array[None], (devices, *array.shape)), axis, 0, 0, tiled=True
    )


def of_everyone(array, axis):
    return sent_to_all(array, axis).astype(jnp.float32).sum(axis=0)


def sent_together(arrays, axis, dim, along):
    widths = [a.shape[along] for a in arrays]
    both = jnp.concatenate(arrays, axis=along)
    out = lax.all_gather(both, axis, axis=dim, tiled=True)
    return tuple(jnp.split(out, [sum(widths[:k]) for k in range(1, len(widths))], axis=along))


def gather_axes(array, axes, dim):
    for axis in reversed(axes):
        array = lax.all_gather(array, axis, axis=dim, tiled=True)
    return array


def in_blocks(array, dim, devices):
    lengths = array.shape
    tiles = array.reshape(*lengths[:dim], devices, lengths[dim] // devices, *lengths[dim + 1 :])
    return jnp.moveaxis(tiles, dim, 0)


def sent_and_summed(array, axis, dim):
    tiles = in_blocks(array, dim, lax.axis_size(axis))
    arrived = lax.all_to_all(tiles, axis, split_axis=0, concat_axis=0, tiled=True)
    return arrived.astype(jnp.float32).sum(axis=0)


def rms_scale(values_in, gain):
    widened = values_in.astype(jnp.float32)
    return (
        widened
        * lax.rsqrt(jnp.mean(widened * widened, axis=-1, keepdims=True) + EPS)
        * gain.astype(jnp.float32)
    )


def shards(
    tokens,
    first_gain,
    query_weight,
    key_weight,
    value_weight,
    decay_down,
    decay_up,
    decay_bias,
    head_gain,
    recurrent_state,
    out_weight,
    second_gain,
    expert_ids,
    route_weights,
    expert_gate,
    expert_up,
    expert_down,
    dense_gate,
    dense_up,
    dense_down,
    branch_gate,
):
    rows_dev = tokens.shape[0]
    normed = rms_scale(tokens, first_gain).astype(jnp.bfloat16)
    query = jnp.dot(normed, query_weight, preferred_element_type=jnp.float32).reshape(
        rows_dev, -1, DK
    ) * DK ** (-0.5)
    keys = jnp.dot(normed, key_weight, preferred_element_type=jnp.float32).reshape(rows_dev, -1, DK)
    values = jnp.dot(normed, value_weight, preferred_element_type=jnp.float32).reshape(
        rows_dev, -1, DV
    )
    decay_low = jnp.dot(normed, decay_down, preferred_element_type=jnp.float32).astype(jnp.bfloat16)
    decay_pre = jnp.dot(decay_low, decay_up, preferred_element_type=jnp.float32) + decay_bias
    log_decay = (jax.nn.log_sigmoid(decay_pre) / 16.0).reshape(rows_dev, -1, DK)
    new_state = (
        jnp.exp(log_decay)[..., None] * recurrent_state + keys[..., None] * values[:, :, None, :]
    )
    head_read = jnp.einsum("shk,shkv->shv", query, new_state, precision=lax.Precision.HIGHEST)
    head_read = (
        head_read
        * lax.rsqrt(jnp.mean(head_read * head_read, axis=-1, keepdims=True) + EPS)
        * head_gain.astype(jnp.float32)
    )
    heads_flat = head_read.astype(jnp.bfloat16).reshape(rows_dev, -1)
    partial_value = jnp.dot(heads_flat, out_weight, preferred_element_type=jnp.float32).astype(
        jnp.bfloat16
    )
    attention = of_everyone(partial_value, "tp").astype(jnp.float32)
    residual = (tokens.astype(jnp.float32) + attention).astype(jnp.bfloat16)
    expert_in = rms_scale(residual, second_gain).astype(jnp.bfloat16)
    branch = jax.nn.sigmoid(jnp.dot(expert_in, branch_gate, preferred_element_type=jnp.float32))
    hidden_cols = dense_gate.shape[1]
    pieces = sent_together((dense_gate, dense_up), EP, 0, 1)
    paired = jnp.concatenate(
        [
            jnp.dot(expert_in, pieces[0], preferred_element_type=jnp.float32),
            jnp.dot(expert_in, pieces[1], preferred_element_type=jnp.float32),
        ],
        axis=1,
    )
    hidden_half = (jax.nn.silu(paired[:, :hidden_cols]) * paired[:, hidden_cols:]).astype(
        jnp.bfloat16
    )
    dense_part = jnp.dot(
        hidden_half, gather_axes(dense_down, EP, 1), preferred_element_type=jnp.float32
    )
    dense = sent_and_summed(dense_part.astype(jnp.bfloat16), "tp", 1)
    experts = lax.axis_size(EP)
    capacity = max(2, 2 * rows_dev * TOPK // experts)
    flat_ids = expert_ids.reshape(-1)
    choices_dev = flat_ids.shape[0]
    onehot = (flat_ids[:, None] == jnp.arange(experts, dtype=jnp.int32)[None, :]).astype(
        jnp.float32
    )
    lower = (
        jnp.arange(choices_dev, dtype=jnp.int32)[:, None]
        > jnp.arange(choices_dev, dtype=jnp.int32)[None, :]
    ).astype(jnp.float32)
    earlier = jnp.dot(lower, onehot, precision=lax.Precision.HIGHEST)
    slot_ids = jnp.sum(earlier * onehot, axis=1)
    slot_hot = (slot_ids[:, None] == jnp.arange(capacity, dtype=jnp.float32)[None, :]).astype(
        jnp.float32
    )
    placing = (onehot[:, :, None] * slot_hot[:, None, :]).reshape(choices_dev, experts * capacity)
    owners = (
        jnp.arange(choices_dev, dtype=jnp.int32)[:, None] // TOPK
        == jnp.arange(rows_dev, dtype=jnp.int32)[None, :]
    ).astype(jnp.float32)
    send_map = jnp.einsum("rs,rt->st", placing, owners).astype(jnp.bfloat16)
    shares = route_weights / jnp.sum(route_weights, axis=-1, keepdims=True)
    weighing = jnp.einsum(
        "rt,rs->ts", owners, placing * shares.reshape(-1)[:, None], precision=lax.Precision.HIGHEST
    )
    outgoing = (
        jnp.dot(send_map, expert_in, preferred_element_type=jnp.float32)
        .astype(jnp.bfloat16)
        .reshape(experts, capacity, -1)
    )
    arrived = lax.all_to_all(outgoing, EP, split_axis=0, concat_axis=0, tiled=True)
    sources = arrived.shape[0]
    items = arrived.shape[1]
    stacked = arrived.reshape(sources * items, -1)
    gate_pre = jnp.dot(stacked, expert_gate[0], preferred_element_type=jnp.float32)
    up_pre = jnp.dot(stacked, expert_up[0], preferred_element_type=jnp.float32)
    activated = (jax.nn.silu(gate_pre) * up_pre).astype(jnp.bfloat16)
    expert_part = (
        jnp.dot(activated, expert_down[0], preferred_element_type=jnp.float32)
        .astype(jnp.bfloat16)
        .reshape(sources, items, -1)
    )
    summed = sent_and_summed(expert_part, "tp", 2).astype(jnp.bfloat16)
    came_back = lax.all_to_all(summed, EP, split_axis=0, concat_axis=0, tiled=True)
    routed = jnp.dot(
        weighing,
        came_back.reshape(experts * capacity, -1).astype(jnp.float32),
        precision=lax.Precision.HIGHEST,
    )
    half_width = dense.shape[1]
    own_half = lax.dynamic_slice_in_dim(
        residual, lax.axis_index("tp") * half_width, half_width, 1
    ).astype(jnp.float32)
    return (own_half + routed + branch[:, None] * dense).astype(jnp.bfloat16)


def solution(mesh):
    split = Mesh(mesh.devices.reshape(8, 4, 4, mesh.shape["tp"]), ("ep_0", "ep_1", "ep_2", "tp"))
    placed = (
        P(EP, None),
        P(),
        P(None, "tp"),
        P(None, "tp"),
        P(None, "tp"),
        P(),
        P(None, "tp"),
        P("tp"),
        P(),
        P(EP, "tp", None, None),
        P("tp", None),
        P(),
        P(EP, None),
        P(EP, None),
        P(EP, None, "tp"),
        P(EP, None, "tp"),
        P(EP, "tp", None),
        P(EP, "tp"),
        P(EP, "tp"),
        P("tp", EP),
        P(),
    )
    return jax.shard_map(
        shards, mesh=split, in_specs=placed, out_specs=P(EP, "tp"), check_vma=False
    )
```

profile of v0, /device:TPU:1, one launch (start us, length us, event | category | flops | bytes accessed | tf_op | source)
XLA Modules:
  0.0 181.6 jit_solution(6299330288382562442)
XLA Ops:
  6.5 0.0 copy-start
  6.5 0.0 copy-start.1
  6.6 0.0 copy-start.11
  6.6 0.0 all-gather.3.cloned.1.call-start
  6.6 1.5 pad_maximum_fusion
  8.1 0.0 all-gather.3.cloned.1.call-update
  8.1 0.9 fusion.37
  9.0 0.7 convert_element_type.85
  9.7 1.3 fusion.69
  11.0 0.0 copy-start.5
  11.0 1.3 convolution_multiply_fusion.2
  12.3 1.5 fusion.67
  13.8 0.0 copy-done.2
  13.8 0.0 copy-done.10
  13.9 0.0 copy-done.9
  13.9 0.0 copy-done.8
  13.9 0.3 fusion.61
  14.2 0.0 copy-done.1
  14.2 0.8 fusion.14
  15.0 0.1 fusion.50
  15.2 0.0 copy-done.11
  15.2 0.3 convolution_convert_fusion.3
  15.5 0.6 broadcast_in_dim.2
  16.1 6.5 %all-to-all-start = ((bf16[2,8,2048]{2,1,0:T(8,128)(2,1)}), bf16[2,8,2048]{2,1,0:T(8,128)(2,1)S(1)}, u32[]{:S(2)}, u32[]{:S(2)}) async-start(bf16[2,8,2048]{2,1,0:T(8,128)(2,1)} %broadcast_in_dim.2), calls=%async_computation | async-start | bytes 131072 | tf_op jit(solution)/shard_map/all_to_all | solution.py:18
  22.6 0.1 eq.58
  22.7 0.1 fusion.43
  22.8 0.1 copy.25
  22.9 0.3 fusion.3
  23.2 0.5 all-to-all-done
  23.7 0.1 fusion.34
  23.8 0.1 broadcast_multiply_fusion
  23.9 0.7 convolution_convert_fusion.1
  24.6 0.0 copy-start.4
  24.6 1.5 reshape.152
  26.2 13.8 %all-to-all-start.1 = ((bf16[128,2,2048]{2,1,0:T(2,128)(2,1)}), bf16[128,2,2048]{2,1,0:T(2,128)(2,1)S(1)}, u32[]{:S(2)}, u32[]{:S(2)}) async-start(bf16[128,2,2048]{2,1,0:T(2,128)(2,1)} %reshape.152), calls=%async_computation.1 | async-start | bytes 2097152 | tf_op jit(solution)/shard_map/all_to_all | solution.py:160
  40.0 0.0 all-gather.5.cloned.1.call-start
  40.0 9.9 %all_gather.13 = bf16[256,64]{0,1:T(8,128)(2,1)S(1)} all-gather(bf16[256,16]{0,1:T(8,128)(2,1)S(1)} %copy-done.4), channel_id=1, replica_groups=mesh['ep_0'=8,'ep_1'=4,'ep_2'=4,'tp'=2] {'ep_2'}, dimensions={1}, use_global_device_ids=true | all-gather | bytes 40960 | tf_op jit(solution)/shard_map/all_gather | solution.py:36
  49.9 11.2 %all_gather.14 = bf16[256,256]{0,1:T(8,128)(2,1)} all-gather(bf16[256,64]{0,1:T(8,128)(2,1)S(1)} %all_gather.13), channel_id=1, replica_groups=mesh['ep_0'=8,'ep_1'=4,'ep_2'=4,'tp'=2] {'ep_1'}, dimensions={1}, use_global_device_ids=true | all-gather | bytes 163840 | tf_op jit(solution)/shard_map/all_gather | solution.py:36
  61.2 0.0 all-gather.5.cloned.1.call-update
  61.2 8.3 %all-to-all-done.1 = bf16[128,2,2048]{2,1,0:T(2,128)(2,1)S(1)} async-done(((bf16[128,2,2048]{2,1,0:T(2,128)(2,1)}), bf16[128,2,2048]{2,1,0:T(2,128)(2,1)S(1)}, u32[]{:S(2)}, u32[]{:S(2)}) %all-to-all-start.1) | async-done | bytes 1048608 | tf_op jit(solution)/shard_map/all_to_all | solution.py:160
  69.5 0.4 reshape.153
  69.9 1.5 fusion.22
  71.4 2.0 %convolution_convert_fusion = bf16[256,2048]{1,0:T(8,128)(2,1)S(1)} fusion(bf16[256,2048]{1,0:T(8,128)(2,1)S(1)} %reshape.153, bf16[1,128,2048]{2,1,0:T(8,128)(2,1)} %param.37, bf16[1,2048,128]{2,1,0:T(8,128)(2,1)} %param.36, f32[256,128]{1,0:T(8,128)S(1)} %fusion.22), kind=kOutput, calls=%fused_computation | convolution fusion | flops 269156352 | bytes 3276800 | tf_op jit(solution)/shard_map/dot_general | solution.py:168
  73.3 0.8 reshape_reshape.3
  74.2 0.8 copy.33
  75.0 0.0 copy-start.3
  75.0 0.0 copy-start.6
  75.0 7.1 %all_to_all.25 = bf16[2,128,2,1024]{3,2,1,0:T(2,128)(2,1)S(1)} all-to-all(bf16[2,128,2,1024]{3,2,1,0:T(2,128)(2,1)S(1)} %bitcast.57), channel_id=1, replica_groups=mesh['ep_0'=8,'ep_1'=4,'ep_2'=4,'tp'=2] {'tp'}, dimensions={0} | all-to-all | bytes 2097152 | tf_op jit(solution)/shard_map/all_to_all | solution.py:48
  82.1 3.1 %reduce_sum.81 = bf16[128,2,1024]{2,1,0:T(2,128)(2,1)} reduce(bf16[2,128,2,1024]{3,2,1,0:T(2,128)(2,1)S(1)} %all_to_all.25, bf16[]{:T(256)} %constant.48.clone.1), dimensions={0}, to_apply=%region_6.7 | reduce | flops 262144 | bytes 1572866 | tf_op jit(solution)/shard_map/reduce_sum | solution.py:49
  85.1 6.3 %all-to-all-start.3 = ((bf16[128,2,1024]{2,1,0:T(2,128)(2,1)}), bf16[128,2,1024]{2,1,0:T(2,128)(2,1)S(1)}, u32[]{:S(2)}, u32[]{:S(2)}) async-start(bf16[128,2,1024]{2,1,0:T(2,128)(2,1)} %reduce_sum.81), calls=%async_computation.3 | async-start | bytes 1048576 | tf_op jit(solution)/shard_map/all_to_all | solution.py:173
  91.4 0.1 reduce_sum.79
  91.5 0.1 broadcast_divide_fusion
  91.6 0.1 mul.174
  91.7 0.0 copy-done.6
  91.7 0.2 fusion.9
  91.9 0.2 fusion.32
  92.2 18.1 %all-to-all-done.3 = bf16[128,2,1024]{2,1,0:T(2,128)(2,1)S(1)} async-done(((bf16[128,2,1024]{2,1,0:T(2,128)(2,1)}), bf16[128,2,1024]{2,1,0:T(2,128)(2,1)S(1)}, u32[]{:S(2)}, u32[]{:S(2)}) %all-to-all-start.3) | async-done | bytes 524320 | tf_op jit(solution)/shard_map/all_to_all | solution.py:173
  110.2 0.2 reshape.154
  110.4 15.2 %all-gather.3.cloned.1.call-done = bf16[2048,512]{1,0:T(8,128)(2,1)} async-done(((bf16[16,512]{1,0:T(8,128)(2,1)}), bf16[2048,512]{1,0:T(8,128)(2,1)}) %all-gather.3.cloned.1.call-update) | async-done | bytes 2097168 | tf_op jit(solution)/shard_map/all_gather | solution.py:30
  125.6 1.5 fusion.12
  127.1 35.2 %all-gather.5.cloned.1.call-done = bf16[256,2048]{0,1:T(8,128)(2,1)} async-done(((bf16[256,256]{0,1:T(8,128)(2,1)}), bf16[256,2048]{0,1:T(8,128)(2,1)}) %all-gather.5.cloned.1.call-update) | async-done | bytes 1048592 | tf_op jit(solution)/shard_map/all_gather | solution.py:36
  162.3 2.4 %convolution_convert_fusion.2 = bf16[8,2048]{1,0:T(8,128)(2,1)S(1)} fusion(bf16[256,2048]{0,1:T(8,128)(2,1)} %all-gather.5.cloned.1.call-done, bf16[2048,512]{1,0:T(8,128)(2,1)} %all-gather.3.cloned.1.call-done, f32[8,256]{1,0:T(8,128)S(1)} %fusion.12, bf16[8,2048]{1,0:T(8,128)(2,1)S(1)} %get-tuple-element.6, f32[2048]{0:T(1024)S(1)} %convert_element_type.98, ...), kind=kOutput, calls=%fused_computation.2 | convolution fusion | flops 16871424 | bytes 2179104 | tf_op jit(solution)/shard_map/dot_general | solution.py:125
  164.7 9.1 %all_to_all.26 = bf16[2,8,1024]{2,1,0:T(8,128)(2,1)S(1)} all-to-all(bf16[2,8,1024]{2,1,0:T(8,128)(2,1)S(1)} %bitcast.60), channel_id=1, replica_groups=mesh['ep_0'=8,'ep_1'=4,'ep_2'=4,'tp'=2] {'tp'}, dimensions={0} | all-to-all | bytes 65536 | tf_op jit(solution)/shard_map/all_to_all | solution.py:48
  173.8 0.9 fusion.2
  (20 shorter events, 0.1 us)
Async XLA Ops:
  6.5 8.6 %copy-start = (bf16[256,2048]{1,0:T(8,128)(2,1)S(1)}, bf16[256,2048]{1,0:T(8,128)(2,1)}, u32[]{:S(2)}) copy-start(bf16[256,2048]{1,0:T(8,128)(2,1)} %param.31) | copy-start | bytes 3145732
  6.5 7.3 %copy-start.2 = (bf16[8,2048]{1,0:T(8,128)(2,1)S(1)}, bf16[8,2048]{1,0:T(8,128)(2,1)}, u32[]{:S(2)}) copy-start(bf16[8,2048]{1,0:T(8,128)(2,1)} %param.21) | copy-start | bytes 98308
  6.5 7.3 %copy-start.10 = (f32[128]{0:T(128)S(1)}, f32[128]{0:T(128)}, u32[]{:S(2)}) copy-start(f32[128]{0:T(128)} %param.28) | copy-start | bytes 1540
  6.5 7.3 %copy-start.9 = (bf16[16,128]{1,0:T(8,128)(2,1)S(1)}, bf16[16,128]{1,0:T(8,128)(2,1)}, u32[]{:S(2)}) copy-start(bf16[16,128]{1,0:T(8,128)(2,1)} %param.27) | copy-start | bytes 12292
  6.5 7.3 %copy-start.8 = (bf16[2048,16]{0,1:T(8,128)(2,1)S(1)}, bf16[2048,16]{0,1:T(8,128)(2,1)}, u32[]{:S(2)}) copy-start(bf16[2048,16]{0,1:T(8,128)(2,1)} %param.26) | copy-start | bytes 196612
  6.5 7.7 %copy-start.1 = (f32[8,1,128,256]{3,2,1,0:T(8,128)S(1)}, f32[8,1,128,256]{3,2,1,0:T(8,128)}, u32[]{:S(2)}) copy-start(f32[8,1,128,256]{3,2,1,0:T(8,128)} %param.30) | copy-start | bytes 3145732
  6.6 8.6 %copy-start.11 = (bf16[256]{0:T(256)(128)(2,1)S(1)}, bf16[256]{0:T(256)(128)(2,1)}, u32[]{:S(2)}) copy-start(bf16[256]{0:T(256)(128)(2,1)} %param.29) | copy-start | bytes 1540
  6.6 119.1 %all-gather.3.cloned.1.call-start = ((), (), s32[]{:S(2)}) async-start(), calls=%async_computation.5 | async-start | bytes 2113536 | tf_op jit(solution)/shard_map/all_gather | solution.py:30
  11.0 11.6 %copy-start.7 = (s32[8,6]{1,0:T(8,128)S(1)}, s32[8,6]{1,0:T(8,128)}, u32[]{:S(2)}) copy-start(s32[8,6]{1,0:T(8,128)} %param.33) | copy-start | bytes 580
  11.0 11.7 %copy-start.5 = (bf16[2048]{0:T(1024)(128)(2,1)S(1)}, bf16[2048]{0:T(1024)(128)(2,1)}, u32[]{:S(2)}) copy-start(bf16[2048]{0:T(1024)(128)(2,1)} %param.32) | copy-start | bytes 12292
  16.1 7.6 %all-to-all-start = ((bf16[2,8,2048]{2,1,0:T(8,128)(2,1)}), bf16[2,8,2048]{2,1,0:T(8,128)(2,1)S(1)}, u32[]{:S(2)}, u32[]{:S(2)}) async-start(bf16[2,8,2048]{2,1,0:T(8,128)(2,1)} %broadcast_in_dim.2), calls=%async_computation | async-start | bytes 131072 | tf_op jit(solution)/shard_map/all_to_all | solution.py:18
  24.6 15.4 %copy-start.4 = (bf16[256,16]{0,1:T(8,128)(2,1)S(1)}, bf16[256,16]{0,1:T(8,128)(2,1)}, u32[]{:S(2)}) copy-start(bf16[256,16]{0,1:T(8,128)(2,1)} %param.40) | copy-start | bytes 24580
  26.2 43.3 %all-to-all-start.1 = ((bf16[128,2,2048]{2,1,0:T(2,128)(2,1)}), bf16[128,2,2048]{2,1,0:T(2,128)(2,1)S(1)}, u32[]{:S(2)}, u32[]{:S(2)}) async-start(bf16[128,2,2048]{2,1,0:T(2,128)(2,1)} %reshape.152), calls=%async_computation.1 | async-start | bytes 2097152 | tf_op jit(solution)/shard_map/all_to_all | solution.py:160
  40.0 122.3 %all-gather.5.cloned.1.call-start = ((), (), s32[]{:S(2)}) async-start(), calls=%async_computation.6 | async-start | bytes 1179648 | tf_op jit(solution)/shard_map/all_gather | solution.py:36
  75.0 16.4 %copy-start.3 = (f32[8,6]{1,0:T(8,128)S(1)}, f32[8,6]{1,0:T(8,128)}, u32[]{:S(2)}) copy-start(f32[8,6]{1,0:T(8,128)} %param.34) | copy-start | bytes 580
  75.0 16.7 %copy-start.6 = (bf16[2048]{0:T(1024)(128)(2,1)S(1)}, bf16[2048]{0:T(1024)(128)(2,1)}, u32[]{:S(2)}) copy-start(bf16[2048]{0:T(1024)(128)(2,1)} %param.41) | copy-start | bytes 12292
  85.1 25.1 %all-to-all-start.3 = ((bf16[128,2,1024]{2,1,0:T(2,128)(2,1)}), bf16[128,2,1024]{2,1,0:T(2,128)(2,1)S(1)}, u32[]{:S(2)}, u32[]{:S(2)}) async-start(bf16[128,2,1024]{2,1,0:T(2,128)(2,1)} %reduce_sum.81), calls=%async_computation.3 | async-start | bytes 1048576 | tf_op jit(solution)/shard_map/all_to_all | solution.py:173
Sparse Core Ops, SparseCore 0:
  11.0 114.5 all-gather.2
  127.4 34.8 all-gather.4
where the time goes:
time: 182 us
  waiting for transfers between devices  77.2 us (42%)
  blocking collectives  37.3 us (20%)
  starting transfers between devices  26.6 us (15%)
  matrix products  15.3 us (8%)
  between operations  13.7 us (8%)
  other arithmetic  6.75 us (4%)
  local copies, waits for them, and re-layouts  4.69 us (3%)
    all_gather x1, waiting for transfers between devices, gather_axes(): array = lax.all_gather(array, axis, axis=dim, tiled=True)  35.2 us
    all_gather x2, blocking collectives, gather_axes(): array = lax.all_gather(array, axis, axis=dim, tiled=True)  21.1 us
    all_to_all x1, waiting for transfers between devices, shards(): lax.all_to_all(summed, EP, split_axis=0, concat_axis=0, tiled=True)  18.1 us
    all_to_all x2, blocking collectives, sent_and_summed(): lax.all_to_all(tiles, axis, split_axis=0, concat_axis=0, tiled=True)  16.2 us
    all_gather x1, waiting for transfers between devices, sent_together(): out = lax.all_gather(both, axis, axis=dim, tiled=True)  15.2 us
    all_to_all x1, starting transfers between devices, shards(): lax.all_to_all(outgoing, EP, split_axis=0, concat_axis=0, tiled=True)  13.8 us
    all_to_all x1, waiting for transfers between devices, shards(): lax.all_to_all(outgoing, EP, split_axis=0, concat_axis=0, tiled=True)  8.27 us
    all_to_all x1, starting transfers between devices, sent_to_all(): lax.all_to_all(jnp.broadcast_to(array[None], (devices, *array.shape)), ax...  6.48 us
  transfers between devices with their start and end apart: 5, of which 5 were waited for; matrix products, arithmetic and copies ran while one was open for 12% of the time, Pallas kernels for 0%

commit v1 on v0

v1 whole, which is shorter than its diff:
```python
import jax
import jax.numpy as jnp
from jax import lax
from jax.sharding import Mesh
from jax.sharding import PartitionSpec as P

DK = 128
DV = 256
TOPK = 6
EP = ("ep_0", "ep_1", "ep_2")


EPS = 1e-06


SWAP = [(0, 1), (1, 0)]


def swapped(array):
    return lax.ppermute(array, "tp", SWAP)


def half_of(array, index, dim):
    width = array.shape[dim] // 2
    return lax.dynamic_slice_in_dim(array, index * width, width, dim)


def exchanged(array, axis):
    return lax.all_to_all(array, axis, split_axis=0, concat_axis=0, tiled=True)


def rms_scale(values_in, gain):
    widened = values_in.astype(jnp.float32)
    return (
        widened
        * lax.rsqrt(jnp.mean(widened * widened, axis=-1, keepdims=True) + EPS)
        * gain.astype(jnp.float32)
    )


def shards(
    tokens,
    first_gain,
    query_weight,
    key_weight,
    value_weight,
    decay_down,
    decay_up,
    decay_bias,
    head_gain,
    recurrent_state,
    out_weight,
    second_gain,
    expert_ids,
    route_weights,
    expert_gate,
    expert_up,
    expert_down,
    dense_gate,
    dense_up,
    dense_down,
    branch_gate,
):
    rows_dev, width = tokens.shape
    core = lax.axis_index("tp")
    lines = lax.axis_size("ep_0")
    experts = lax.axis_size(EP)
    rows_own, hidden = dense_gate.shape
    units = hidden // lines
    packed = jnp.stack([dense_gate, dense_up, dense_down.T], axis=1)
    packed = packed.reshape(rows_own, 3, lines, units).transpose(2, 0, 1, 3)
    packed = packed.reshape(lines, 1, rows_own, 3 * units)
    packed = jnp.broadcast_to(packed, (lines, experts // lines, rows_own, 3 * units))
    dense_weights = exchanged(packed.reshape(experts, rows_own, 3 * units), EP).reshape(
        width, 3 * units
    )

    normed = rms_scale(tokens, first_gain).astype(jnp.bfloat16)
    query = jnp.dot(normed, query_weight, preferred_element_type=jnp.float32) * DK ** (-0.5)
    keys = jnp.dot(normed, key_weight, preferred_element_type=jnp.float32)
    values = jnp.dot(normed, value_weight, preferred_element_type=jnp.float32)
    decay_low = jnp.dot(normed, decay_down, preferred_element_type=jnp.float32).astype(jnp.bfloat16)
    decay_pre = jnp.dot(decay_low, decay_up, preferred_element_type=jnp.float32) + decay_bias
    decay = jnp.exp(jax.nn.log_sigmoid(decay_pre) / 16.0)
    head_read = (
        jnp.sum((query * decay)[:, :, None] * recurrent_state[:, 0], axis=1)
        + jnp.sum(query * keys, axis=1, keepdims=True) * values
    )
    head_read = (
        head_read
        * lax.rsqrt(jnp.mean(head_read * head_read, axis=-1, keepdims=True) + EPS)
        * head_gain.astype(jnp.float32)
    )
    partial_value = jnp.dot(
        head_read.astype(jnp.bfloat16), out_weight, preferred_element_type=jnp.float32
    ).astype(jnp.bfloat16)
    attention = partial_value.astype(jnp.float32) + swapped(partial_value).astype(jnp.float32)
    residual = (tokens.astype(jnp.float32) + attention).astype(jnp.bfloat16)
    expert_in = rms_scale(residual, second_gain).astype(jnp.bfloat16)
    branch = jax.nn.sigmoid(jnp.dot(expert_in, branch_gate, preferred_element_type=jnp.float32))

    capacity = max(2, 2 * rows_dev * TOPK // experts)
    flat_ids = expert_ids.reshape(-1)
    choices_dev = flat_ids.shape[0]
    onehot = (flat_ids[:, None] == jnp.arange(experts, dtype=jnp.int32)[None, :]).astype(
        jnp.float32
    )
    lower = (
        jnp.arange(choices_dev, dtype=jnp.int32)[:, None]
        > jnp.arange(choices_dev, dtype=jnp.int32)[None, :]
    ).astype(jnp.float32)
    earlier = jnp.dot(lower, onehot, precision=lax.Precision.HIGHEST)
    slot_ids = jnp.sum(earlier * onehot, axis=1)
    slot_hot = (slot_ids[:, None] == jnp.arange(capacity, dtype=jnp.float32)[None, :]).astype(
        jnp.float32
    )
    placing = (onehot[:, :, None] * slot_hot[:, None, :]).reshape(choices_dev, experts * capacity)
    owners = (
        jnp.arange(choices_dev, dtype=jnp.int32)[:, None] // TOPK
        == jnp.arange(rows_dev, dtype=jnp.int32)[None, :]
    ).astype(jnp.float32)
    send_map = jnp.einsum("rs,rt->st", placing, owners).astype(jnp.bfloat16)
    shares = route_weights / jnp.sum(route_weights, axis=-1, keepdims=True)
    weighing = jnp.einsum(
        "rt,rs->ts", owners, placing * shares.reshape(-1)[:, None], precision=lax.Precision.HIGHEST
    )

    line_in = exchanged(
        jnp.broadcast_to(expert_in[None], (lines, rows_dev, width)), "ep_0"
    ).reshape(lines * rows_dev, width)
    outgoing = (
        jnp.dot(send_map, half_of(expert_in, core, 1), preferred_element_type=jnp.float32)
        .astype(jnp.bfloat16)
        .reshape(experts, capacity, -1)
    )
    arrived = exchanged(outgoing, EP)
    paired = jnp.dot(line_in, dense_weights, preferred_element_type=jnp.float32)
    line_hidden = (
        jax.nn.silu(paired[:, :units]) * paired[:, units : 2 * units]
    ).astype(jnp.bfloat16)
    line_part = lax.dot_general(
        jnp.pad(line_hidden, ((0, 0), (2 * units, 0))),
        dense_weights,
        (((1,), (1,)), ((), ())),
        preferred_element_type=jnp.float32,
    ).astype(jnp.bfloat16)
    line_sum = half_of(line_part, core, 1).astype(jnp.float32) + swapped(
        half_of(line_part, 1 - core, 1)
    ).astype(jnp.float32)
    dense = (
        exchanged(line_sum.astype(jnp.bfloat16).reshape(lines, rows_dev, width // 2), "ep_0")
        .astype(jnp.float32)
        .sum(axis=0)
    )

    mine = arrived.reshape(experts * capacity, -1)
    theirs = swapped(mine)
    gate, up, down = expert_gate[0], expert_up[0], expert_down[0]
    gate_pre = jnp.dot(
        mine, half_of(gate, core, 0), preferred_element_type=jnp.float32
    ) + jnp.dot(theirs, half_of(gate, 1 - core, 0), preferred_element_type=jnp.float32)
    up_pre = jnp.dot(
        mine, half_of(up, core, 0), preferred_element_type=jnp.float32
    ) + jnp.dot(theirs, half_of(up, 1 - core, 0), preferred_element_type=jnp.float32)
    activated = (jax.nn.silu(gate_pre) * up_pre).astype(jnp.bfloat16)
    for_them = jnp.dot(
        activated, half_of(down, 1 - core, 1), preferred_element_type=jnp.float32
    ).astype(jnp.bfloat16)
    for_me = jnp.dot(
        activated, half_of(down, core, 1), preferred_element_type=jnp.float32
    ).astype(jnp.bfloat16)
    summed = (for_me.astype(jnp.float32) + swapped(for_them).astype(jnp.float32)).astype(
        jnp.bfloat16
    )
    came_back = exchanged(summed.reshape(experts, capacity, -1), EP)
    routed = jnp.dot(
        weighing,
        came_back.reshape(experts * capacity, -1).astype(jnp.float32),
        precision=lax.Precision.HIGHEST,
    )
    own_half = half_of(residual, core, 1).astype(jnp.float32)
    return (own_half + routed + branch[:, None] * dense).astype(jnp.bfloat16)


def solution(mesh):
    split = Mesh(mesh.devices.reshape(8, 4, 4, mesh.shape["tp"]), ("ep_0", "ep_1", "ep_2", "tp"))
    placed = (
        P(EP, None),
        P(),
        P(None, "tp"),
        P(None, "tp"),
        P(None, "tp"),
        P(),
        P(None, "tp"),
        P("tp"),
        P(),
        P(EP, "tp", None, None),
        P("tp", None),
        P(),
        P(EP, None),
        P(EP, None),
        P(EP, None, "tp"),
        P(EP, None, "tp"),
        P(EP, "tp", None),
        P(EP, "tp"),
        P(EP, "tp"),
        P("tp", EP),
        P(),
    )
    return jax.shard_map(
        shards, mesh=split, in_specs=placed, out_specs=P(EP, "tp"), check_vma=False
    )
```

time: 182 us -> 133 us (0.73); the launches traced: 182 us -> 130 us
  blocking collectives: 37.3 us -> 0 us
  starting transfers between devices: 26.6 us -> 41.2 us
  between operations: 13.7 us -> 0.39 us
  waiting for transfers between devices: 77.2 us -> 67.3 us
  matrix products: 15.3 us -> 8.97 us
  local copies, waits for them, and re-layouts: 4.69 us -> 8.84 us
  other arithmetic: 6.75 us -> 3.62 us
    all_gather x2 -> x0, waiting for transfers between devices: 50.4 us -> none  [the longest x1 35.2 us: gather_axes(): array = lax.all_gather(array, axis, axis=dim, tiled=True)]
    all_to_all x3 -> x5, waiting for transfers between devices: 26.8 us -> 64.2 us  [exchanged(): return lax.all_to_all(array, axis, split_axis=0, concat_axis=0, tiled=True)]
    all_gather x2 -> x0, blocking collectives: 21.1 us -> none  [gather_axes(): array = lax.all_gather(array, axis, axis=dim, tiled=True)]
    all_to_all x2 -> x0, blocking collectives: 16.2 us -> none  [sent_and_summed(): lax.all_to_all(tiles, axis, split_axis=0, concat_axis=0, tiled=True)]
    ppermute x0 -> x4, starting transfers between devices: none -> 8.34 us  [swapped(): return lax.ppermute(array, 'tp', SWAP)]
    dot_general x9 -> x12, matrix products: 12 us -> 5.63 us  [the longest x1 1.39 us: shards(): keys = jnp.dot(normed, key_weight, preferred_element_type=jnp.float32)]
    all_to_all x3 -> x5, starting transfers between devices: 26.6 us -> 32.8 us  [exchanged(): return lax.all_to_all(array, axis, split_axis=0, concat_axis=0, tiled=True)]
    unnamed x25 -> x37, local copies, waits for them, and re-layouts: 0.07 us -> 4.05 us
  transfers between devices with their start and end apart: 5 -> 9, of which waited for: 5 -> 8; matrix products, arithmetic and copies ran while one was open for 12% -> 5% of each run, Pallas kernels for 0% -> 0%
where the time goes in v1:
time: 133 us; the launch traced here: 130 us
  waiting for transfers between devices  67.3 us (51%)
  starting transfers between devices  41.2 us (31%)
  matrix products  8.97 us (7%)
  local copies, waits for them, and re-layouts  8.84 us (7%)
  other arithmetic  3.62 us (3%)
    all_to_all x5, waiting for transfers between devices, exchanged(): return lax.all_to_all(array, axis, split_axis=0, concat_axis=0, tiled=True)  64.2 us
    all_to_all x5, starting transfers between devices, exchanged(): return lax.all_to_all(array, axis, split_axis=0, concat_axis=0, tiled=True)  32.8 us
    ppermute x4, starting transfers between devices, swapped(): return lax.ppermute(array, 'tp', SWAP)  8.34 us
    unnamed x37, local copies, waits for them, and re-layouts  4.05 us
    ppermute x4, waiting for transfers between devices, swapped(): return lax.ppermute(array, 'tp', SWAP)  3.05 us
  transfers between devices with their start and end apart: 9, of which 8 were waited for; matrix products, arithmetic and copies ran while one was open for 5% of the time, Pallas kernels for 0%

profile of v1, /device:TPU:1, one launch (start us, length us, event | category | flops | bytes accessed | tf_op | source)
XLA Modules:
  0.0 130.3 jit_solution(12313498341976247935)
XLA Ops:
  0.0 0.8 convert_element_type.108
  0.9 0.9 fusion.38
  1.8 1.4 %convolution_multiply_fusion.2 = f32[8,128]{1,0:T(8,128)S(1)} fusion(bf16[2048,128]{1,0:T(8,128)(2,1)} %param.23, bf16[8,2048]{1,0:T(8,128)(2,1)S(1)} %copy-done.3, f32[2048]{0:T(1024)S(1)} %convert_element_type.108, f32[8]{0:T(128)S(1)} %add_rsqrt_fusion.2), kind=kOutput, calls=%fused_computation.21 | convolution fusion | flops 4260864 | bytes 569376 | tf_op jit(solution)/shard_map/dot_general | solution.py:79
  3.2 1.4 %fusion.8 = f32[8]{0:T(128)S(1)} fusion(f32[8,128]{1,0:T(8,128)S(1)} %convolution_multiply_fusion.2, bf16[2048,128]{1,0:T(8,128)(2,1)} %param.24, bf16[8,2048]{1,0:T(8,128)(2,1)S(1)} %copy-done.3, f32[2048]{0:T(1024)S(1)} %convert_element_type.108, f32[8]{0:T(128)S(1)} %add_rsqrt_fusion.2), kind=kOutput, calls=%fused_computation.23 | convolution fusion | flops 4261880 | bytes 569408 | tf_op jit(solution)/shard_map/dot_general | solution.py:80
  4.6 0.3 fusion.56
  4.9 0.2 fusion.13
  5.2 0.4 multiply_reduce_fusion
  5.6 0.6 copy-done.17
  6.2 0.3 convolution_convert_fusion.1
  6.5 3.2 %collective-permute-start = (bf16[8,2048]{1,0:T(8,128)(2,1)S(1)}, bf16[8,2048]{1,0:T(8,128)(2,1)S(1)}, u32[]{:S(2)}, u32[]{:S(2)}) collective-permute-start(bf16[8,2048]{1,0:T(8,128)(2,1)S(1)} %convolution_convert_fusion.1), channel_id=1, source_target_pairs={{0,1},{1,0},{2,3},{3,2},{4,5},{5,4},{6,7},{7,6},{8,9},{9,8},{10,11... | collective-permute-start | bytes 98312 | tf_op jit(solution)/shard_map/ppermute | solution.py:20
  9.7 0.9 collective-permute-done
  10.6 0.1 fusion.35
  10.7 0.1 fusion.37
  10.8 0.7 broadcast_in_dim.6
  11.5 6.6 %all-to-all-start.2 = ((bf16[8,8,2048]{2,1,0:T(8,128)(2,1)}), bf16[8,8,2048]{2,1,0:T(8,128)(2,1)S(1)}, u32[]{:S(2)}, u32[]{:S(2)}) async-start(bf16[8,8,2048]{2,1,0:T(8,128)(2,1)} %broadcast_in_dim.6), calls=%async_computation.2 | async-start | bytes 524288 | tf_op jit(solution)/shard_map/all_to_all | solution.py:29
  18.2 0.1 stack.12
  18.3 0.6 copy-done.9
  19.0 0.1 stack.13
  19.1 0.6 copy-done.10
  19.7 0.1 stack.14
  19.9 0.3 maximum_bitcast_fusion
  20.2 0.1 broadcast_in_dim.7
  20.3 0.7 copy-done.13
  21.0 0.1 eq.58
  21.1 0.1 fusion.44
  21.2 0.1 copy.22
  21.3 0.3 fusion.5
  21.6 7.8 %all-to-all-done.2 = bf16[8,8,2048]{2,1,0:T(8,128)(2,1)S(1)} async-done(((bf16[8,8,2048]{2,1,0:T(8,128)(2,1)}), bf16[8,8,2048]{2,1,0:T(8,128)(2,1)S(1)}, u32[]{:S(2)}, u32[]{:S(2)}) %all-to-all-start.2) | async-done | bytes 262176 | tf_op jit(solution)/shard_map/all_to_all | solution.py:29
  29.4 0.8 broadcast_in_dim.8
  30.2 9.2 %all-to-all-start.3 = ((bf16[128,16,96]{2,1,0:T(8,128)(2,1)}), bf16[128,16,96]{2,1,0:T(8,128)(2,1)S(1)}, u32[]{:S(2)}, u32[]{:S(2)}) async-start(bf16[128,16,96]{2,1,0:T(8,128)(2,1)} %bitcast.12), calls=%async_computation.3 | async-start | bytes 1048576 | tf_op jit(solution)/shard_map/all_to_all | solution.py:29
  39.5 0.5 convolution_convert_fusion.4
  40.0 1.0 reshape.143
  41.0 16.3 %all-to-all-done.3 = bf16[128,16,96]{2,1,0:T(8,128)(2,1)S(1)} async-done(((bf16[128,16,96]{2,1,0:T(8,128)(2,1)}), bf16[128,16,96]{2,1,0:T(8,128)(2,1)S(1)}, u32[]{:S(2)}, u32[]{:S(2)}) %all-to-all-start.3) | async-done | bytes 393248 | tf_op jit(solution)/shard_map/all_to_all | solution.py:29
  57.3 7.5 %all-to-all-start = ((bf16[128,2,1024]{2,1,0:T(2,128)(2,1)}), bf16[128,2,1024]{2,1,0:T(2,128)(2,1)S(1)}, u32[]{:S(2)}, u32[]{:S(2)}) async-start(bf16[128,2,1024]{2,1,0:T(2,128)(2,1)} %reshape.143), calls=%async_computation | async-start | bytes 1048576 | tf_op jit(solution)/shard_map/all_to_all | solution.py:29
  64.8 0.2 fusion.14
  65.0 16.9 %all-to-all-done = bf16[128,2,1024]{2,1,0:T(2,128)(2,1)S(1)} async-done(((bf16[128,2,1024]{2,1,0:T(2,128)(2,1)}), bf16[128,2,1024]{2,1,0:T(2,128)(2,1)S(1)}, u32[]{:S(2)}, u32[]{:S(2)}) %all-to-all-start) | async-done | bytes 524320 | tf_op jit(solution)/shard_map/all_to_all | solution.py:29
  82.0 0.2 reshape.144
  82.2 4.5 %collective-permute-start.1 = (bf16[256,1024]{1,0:T(8,128)(2,1)S(1)}, bf16[256,1024]{1,0:T(8,128)(2,1)S(1)}, u32[]{:S(2)}, u32[]{:S(2)}) collective-permute-start(bf16[256,1024]{1,0:T(8,128)(2,1)S(1)} %reshape.144), channel_id=1, source_target_pairs={{0,1},{1,0},{2,3},{3,2},{4,5},{5,4},{6,7},{7,6},{8,9},{9,8},{10,11... | collective-permute-start | bytes 1572872 | tf_op jit(solution)/shard_map/ppermute | solution.py:20
  86.7 0.1 fusion.43
  86.8 0.3 fusion.24
  87.1 0.3 fusion.21
  87.4 0.8 collective-permute-done.1
  88.2 0.3 convolution_add_fusion.1
  88.5 0.3 fusion.2
  88.8 0.7 copy-done.4
  89.6 1.1 convolution_convert_fusion.2
  90.7 0.4 collective-permute-start.2
  91.0 0.3 convolution_convert_fusion
  91.4 0.2 collective-permute-start.3
  91.6 1.3 %collective-permute-done.3 = bf16[64,1024]{1,0:T(8,128)(2,1)S(1)} collective-permute-done((bf16[64,1024]{1,0:T(8,128)(2,1)S(1)}, bf16[64,1024]{1,0:T(8,128)(2,1)S(1)}, u32[]{:S(2)}, u32[]{:S(2)}) %collective-permute-start.3) | collective-permute-done | bytes 131104 | tf_op jit(solution)/shard_map/ppermute | solution.py:20
  93.0 0.7 fusion.32
  93.6 3.4 %all-to-all-start.4 = ((bf16[8,8,1024]{2,1,0:T(8,128)(2,1)}), bf16[8,8,1024]{2,1,0:T(8,128)(2,1)S(1)}, u32[]{:S(2)}, u32[]{:S(2)}) async-start(bf16[8,8,1024]{2,1,0:T(8,128)(2,1)} %fusion.32), calls=%async_computation.4 | async-start | bytes 262144 | tf_op jit(solution)/shard_map/all_to_all | solution.py:29
  97.0 0.3 add_convert_fusion
  97.3 1.0 reshape.145
  98.3 6.9 %all-to-all-done.4 = bf16[8,8,1024]{2,1,0:T(8,128)(2,1)S(1)} async-done(((bf16[8,8,1024]{2,1,0:T(8,128)(2,1)}), bf16[8,8,1024]{2,1,0:T(8,128)(2,1)S(1)}, u32[]{:S(2)}, u32[]{:S(2)}) %all-to-all-start.4) | async-done | bytes 131104 | tf_op jit(solution)/shard_map/all_to_all | solution.py:29
  105.2 6.2 %all-to-all-start.1 = ((bf16[128,2,1024]{2,1,0:T(2,128)(2,1)}), bf16[128,2,1024]{2,1,0:T(2,128)(2,1)S(1)}, u32[]{:S(2)}, u32[]{:S(2)}) async-start(bf16[128,2,1024]{2,1,0:T(2,128)(2,1)} %reshape.145), calls=%async_computation.1 | async-start | bytes 1048576 | tf_op jit(solution)/shard_map/all_to_all | solution.py:29
  111.4 0.7 copy-done.7
  112.1 0.1 reduce_sum.77
  112.3 0.1 mul.175
  112.4 0.2 fusion.33
  112.6 0.2 fusion.12
  112.8 16.3 %all-to-all-done.1 = bf16[128,2,1024]{2,1,0:T(2,128)(2,1)S(1)} async-done(((bf16[128,2,1024]{2,1,0:T(2,128)(2,1)}), bf16[128,2,1024]{2,1,0:T(2,128)(2,1)S(1)}, u32[]{:S(2)}, u32[]{:S(2)}) %all-to-all-start.1) | async-done | bytes 524320 | tf_op jit(solution)/shard_map/all_to_all | solution.py:29
  129.1 0.2 reshape.146
  129.3 0.9 fusion.4
  (46 shorter events, 0.5 us)
Async XLA Ops:
  0.0 6.2 %copy-start = (bf16[256,2048]{1,0:T(8,128)(2,1)S(1)}, bf16[256,2048]{1,0:T(8,128)(2,1)}, u32[]{:S(2)}) copy-start(bf16[256,2048]{1,0:T(8,128)(2,1)} %param.31) | copy-start | bytes 3145732
  0.0 1.8 %copy-start.3 = (bf16[8,2048]{1,0:T(8,128)(2,1)S(1)}, bf16[8,2048]{1,0:T(8,128)(2,1)}, u32[]{:S(2)}) copy-start(bf16[8,2048]{1,0:T(8,128)(2,1)} %param.21) | copy-start | bytes 98308
  0.0 4.9 %copy-start.2 = (f32[8,1,128,256]{3,2,1,0:T(8,128)S(1)}, f32[8,1,128,256]{3,2,1,0:T(8,128)}, u32[]{:S(2)}) copy-start(f32[8,1,128,256]{3,2,1,0:T(8,128)} %param.30) | copy-start | bytes 3145732
  0.8 3.7 %copy-start.14 = (bf16[2048,16]{0,1:T(8,128)(2,1)S(1)}, bf16[2048,16]{0,1:T(8,128)(2,1)}, u32[]{:S(2)}) copy-start(bf16[2048,16]{0,1:T(8,128)(2,1)} %param.26) | copy-start | bytes 196612
  0.9 3.7 %copy-start.15 = (bf16[16,128]{1,0:T(8,128)(2,1)S(1)}, bf16[16,128]{1,0:T(8,128)(2,1)}, u32[]{:S(2)}) copy-start(bf16[16,128]{1,0:T(8,128)(2,1)} %param.27) | copy-start | bytes 12292
  0.9 3.7 %copy-start.16 = (f32[128]{0:T(128)S(1)}, f32[128]{0:T(128)}, u32[]{:S(2)}) copy-start(f32[128]{0:T(128)} %param.28) | copy-start | bytes 1540
  1.8 3.4 %copy-start.1 = (bf16[2048,256]{1,0:T(8,128)(2,1)S(1)}, bf16[2048,256]{1,0:T(8,128)(2,1)}, u32[]{:S(2)}) copy-start(bf16[2048,256]{1,0:T(8,128)(2,1)} %param.25) | copy-start | bytes 3145732
  5.6 0.7 copy-start.17
  6.2 3.5 %copy-start.11 = (bf16[2048]{0:T(1024)(128)(2,1)S(1)}, bf16[2048]{0:T(1024)(128)(2,1)}, u32[]{:S(2)}) copy-start(bf16[2048]{0:T(1024)(128)(2,1)} %param.32) | copy-start | bytes 12292
  6.5 4.1 %collective-permute-start = (bf16[8,2048]{1,0:T(8,128)(2,1)S(1)}, bf16[8,2048]{1,0:T(8,128)(2,1)S(1)}, u32[]{:S(2)}, u32[]{:S(2)}) collective-permute-start(bf16[8,2048]{1,0:T(8,128)(2,1)S(1)} %convolution_convert_fusion.1), channel_id=1, source_target_pairs={{0,1},{1,0},{2,3},{3,2},{4,5},{5,4},{6,7},{7,6},{8,9},{9,8},{10,11... | collective-permute-start | bytes 98312 | tf_op jit(solution)/shard_map/ppermute | solution.py:20
  11.5 6.6 %copy-start.8 = (bf16[16,256]{1,0:T(8,128)(2,1)S(1)}, bf16[16,256]{1,0:T(8,128)(2,1)}, u32[]{:S(2)}) copy-start(bf16[16,256]{1,0:T(8,128)(2,1)} %param.38) | copy-start | bytes 24580
  11.5 17.8 %all-to-all-start.2 = ((bf16[8,8,2048]{2,1,0:T(8,128)(2,1)}), bf16[8,8,2048]{2,1,0:T(8,128)(2,1)S(1)}, u32[]{:S(2)}, u32[]{:S(2)}) async-start(bf16[8,8,2048]{2,1,0:T(8,128)(2,1)} %broadcast_in_dim.6), calls=%async_computation.2 | async-start | bytes 524288 | tf_op jit(solution)/shard_map/all_to_all | solution.py:29
  18.3 0.7 copy-start.9
  19.0 0.7 copy-start.10
  20.3 0.7 copy-start.13
  30.2 27.1 %all-to-all-start.3 = ((bf16[128,16,96]{2,1,0:T(8,128)(2,1)}), bf16[128,16,96]{2,1,0:T(8,128)(2,1)S(1)}, u32[]{:S(2)}, u32[]{:S(2)}) async-start(bf16[128,16,96]{2,1,0:T(8,128)(2,1)} %bitcast.12), calls=%async_computation.3 | async-start | bytes 1048576 | tf_op jit(solution)/shard_map/all_to_all | solution.py:29
  57.3 24.7 %all-to-all-start = ((bf16[128,2,1024]{2,1,0:T(2,128)(2,1)}), bf16[128,2,1024]{2,1,0:T(2,128)(2,1)S(1)}, u32[]{:S(2)}, u32[]{:S(2)}) async-start(bf16[128,2,1024]{2,1,0:T(2,128)(2,1)} %reshape.143), calls=%async_computation | async-start | bytes 1048576 | tf_op jit(solution)/shard_map/all_to_all | solution.py:29
  65.0 21.8 %copy-start.5 = (bf16[1,2048,128]{2,1,0:T(8,128)(2,1)S(1)}, bf16[1,2048,128]{2,1,0:T(8,128)(2,1)}, u32[]{:S(2)}) copy-start(bf16[1,2048,128]{2,1,0:T(8,128)(2,1)} %param.35) | copy-start | bytes 1572868
  82.2 4.9 %copy-start.6 = (bf16[1,2048,128]{2,1,0:T(8,128)(2,1)S(1)}, bf16[1,2048,128]{2,1,0:T(8,128)(2,1)}, u32[]{:S(2)}) copy-start(bf16[1,2048,128]{2,1,0:T(8,128)(2,1)} %param.36) | copy-start | bytes 1572868
  82.2 6.1 %collective-permute-start.1 = (bf16[256,1024]{1,0:T(8,128)(2,1)S(1)}, bf16[256,1024]{1,0:T(8,128)(2,1)S(1)}, u32[]{:S(2)}, u32[]{:S(2)}) collective-permute-start(bf16[256,1024]{1,0:T(8,128)(2,1)S(1)} %reshape.144), channel_id=1, source_target_pairs={{0,1},{1,0},{2,3},{3,2},{4,5},{5,4},{6,7},{7,6},{8,9},{9,8},{10,11... | collective-permute-start | bytes 1572872 | tf_op jit(solution)/shard_map/ppermute | solution.py:20
  88.5 1.0 copy-start.4
  90.7 6.4 %collective-permute-start.2 = (bf16[256,1024]{1,0:T(8,128)(2,1)}, bf16[256,1024]{1,0:T(8,128)(2,1)S(1)}, u32[]{:S(2)}, u32[]{:S(2)}) collective-permute-start(bf16[256,1024]{1,0:T(8,128)(2,1)} %convolution_convert_fusion.2), channel_id=1, source_target_pairs={{0,1},{1,0},{2,3},{3,2},{4,5},{5,4},{6,7},{7,6},{8,9},{9,8},{10,11... | collective-permute-start | bytes 1572872 | tf_op jit(solution)/shard_map/ppermute | solution.py:20
  91.4 1.6 %collective-permute-start.3 = (bf16[64,1024]{1,0:T(8,128)(2,1)S(1)}, bf16[64,1024]{1,0:T(8,128)(2,1)S(1)}, u32[]{:S(2)}, u32[]{:S(2)}) collective-permute-start(bf16[64,1024]{1,0:T(8,128)(2,1)S(1)} %constant_dynamic-slice_fusion), channel_id=1, source_target_pairs={{0,1},{1,0},{2,3},{3,2},{4,5},{5,4},{6,7},{7,6},{8,9},{9,8},{10,11... | collective-permute-start | bytes 393224 | tf_op jit(solution)/shard_map/ppermute | solution.py:20
  93.6 11.6 %all-to-all-start.4 = ((bf16[8,8,1024]{2,1,0:T(8,128)(2,1)}), bf16[8,8,1024]{2,1,0:T(8,128)(2,1)S(1)}, u32[]{:S(2)}, u32[]{:S(2)}) async-start(bf16[8,8,1024]{2,1,0:T(8,128)(2,1)} %fusion.32), calls=%async_computation.4 | async-start | bytes 262144 | tf_op jit(solution)/shard_map/all_to_all | solution.py:29
  98.3 13.1 %copy-start.12 = (bf16[2048]{0:T(1024)(128)(2,1)S(1)}, bf16[2048]{0:T(1024)(128)(2,1)}, u32[]{:S(2)}) copy-start(bf16[2048]{0:T(1024)(128)(2,1)} %param.41) | copy-start | bytes 12292
  105.2 23.9 %all-to-all-start.1 = ((bf16[128,2,1024]{2,1,0:T(2,128)(2,1)}), bf16[128,2,1024]{2,1,0:T(2,128)(2,1)S(1)}, u32[]{:S(2)}, u32[]{:S(2)}) async-start(bf16[128,2,1024]{2,1,0:T(2,128)(2,1)} %reshape.145), calls=%async_computation.1 | async-start | bytes 1048576 | tf_op jit(solution)/shard_map/all_to_all | solution.py:29
  111.4 0.7 copy-start.7

commit v2 on v1

--- a/solution.py
+++ b/solution.py
@@ -8,6 +8,8 @@
 DV = 256
 TOPK = 6
 EP = ("ep_0", "ep_1", "ep_2")
+PLANE = ("ep_1", "ep_2")
+CAP = 2
 
 
 EPS = 1e-06
@@ -64,15 +66,36 @@
     rows_dev, width = tokens.shape
     core = lax.axis_index("tp")
     lines = lax.axis_size("ep_0")
-    experts = lax.axis_size(EP)
+    plane = lax.axis_size(PLANE)
+    experts = lines * plane
+    half = width // 2
     rows_own, hidden = dense_gate.shape
     units = hidden // lines
     packed = jnp.stack([dense_gate, dense_up, dense_down.T], axis=1)
     packed = packed.reshape(rows_own, 3, lines, units).transpose(2, 0, 1, 3)
-    packed = packed.reshape(lines, 1, rows_own, 3 * units)
-    packed = jnp.broadcast_to(packed, (lines, experts // lines, rows_own, 3 * units))
-    dense_weights = exchanged(packed.reshape(experts, rows_own, 3 * units), EP).reshape(
-        width, 3 * units
+    packed = packed.reshape(lines, rows_own, 3 * units)
+    shares = route_weights / jnp.sum(route_weights, axis=-1, keepdims=True)
+    named = (expert_ids[:, :, None] == jnp.arange(experts, dtype=jnp.int32)).astype(jnp.float32)
+    chosen = named.sum(axis=1)
+    earlier = jnp.cumsum(chosen, axis=0) - chosen
+    place = chosen * (1.0 + earlier)
+    share = (named * shares[:, :, None]).sum(axis=1)
+    share_high = share.astype(jnp.bfloat16)
+    share_low = (share - share_high.astype(jnp.float32)).astype(jnp.bfloat16)
+
+    def by_line(array):
+        return array.astype(jnp.bfloat16).reshape(rows_dev, lines, plane).transpose(1, 0, 2)
+
+    side = jnp.concatenate(
+        [
+            packed[:, :rows_dev],
+            by_line(place),
+            by_line(share_high),
+            packed[:, rows_dev:],
+            by_line(share_low),
+            jnp.zeros((lines, rows_dev, plane), jnp.bfloat16),
+        ],
+        axis=2,
     )
 
     normed = rms_scale(tokens, first_gain).astype(jnp.bfloat16)
@@ -97,63 +120,52 @@
     attention = partial_value.astype(jnp.float32) + swapped(partial_value).astype(jnp.float32)
     residual = (tokens.astype(jnp.float32) + attention).astype(jnp.bfloat16)
     expert_in = rms_scale(residual, second_gain).astype(jnp.bfloat16)
-    branch = jax.nn.sigmoid(jnp.dot(expert_in, branch_gate, preferred_element_type=jnp.float32))
-
-    capacity = max(2, 2 * rows_dev * TOPK // experts)
-    flat_ids = expert_ids.reshape(-1)
-    choices_dev = flat_ids.shape[0]
-    onehot = (flat_ids[:, None] == jnp.arange(experts, dtype=jnp.int32)[None, :]).astype(
-        jnp.float32
-    )
-    lower = (
-        jnp.arange(choices_dev, dtype=jnp.int32)[:, None]
-        > jnp.arange(choices_dev, dtype=jnp.int32)[None, :]
-    ).astype(jnp.float32)
-    earlier = jnp.dot(lower, onehot, precision=lax.Precision.HIGHEST)
-    slot_ids = jnp.sum(earlier * onehot, axis=1)
-    slot_hot = (slot_ids[:, None] == jnp.arange(capacity, dtype=jnp.float32)[None, :]).astype(
-        jnp.float32
-    )
-    placing = (onehot[:, :, None] * slot_hot[:, None, :]).reshape(choices_dev, experts * capacity)
-    owners = (
-        jnp.arange(choices_dev, dtype=jnp.int32)[:, None] // TOPK
-        == jnp.arange(rows_dev, dtype=jnp.int32)[None, :]
-    ).astype(jnp.float32)
-    send_map = jnp.einsum("rs,rt->st", placing, owners).astype(jnp.bfloat16)
-    shares = route_weights / jnp.sum(route_weights, axis=-1, keepdims=True)
-    weighing = jnp.einsum(
-        "rt,rs->ts", owners, placing * shares.reshape(-1)[:, None], precision=lax.Precision.HIGHEST
-    )
-
-    line_in = exchanged(
-        jnp.broadcast_to(expert_in[None], (lines, rows_dev, width)), "ep_0"
-    ).reshape(lines * rows_dev, width)
-    outgoing = (
-        jnp.dot(send_map, half_of(expert_in, core, 1), preferred_element_type=jnp.float32)
-        .astype(jnp.bfloat16)
-        .reshape(experts, capacity, -1)
-    )
-    arrived = exchanged(outgoing, EP)
-    paired = jnp.dot(line_in, dense_weights, preferred_element_type=jnp.float32)
-    line_hidden = (
-        jax.nn.silu(paired[:, :units]) * paired[:, units : 2 * units]
-    ).astype(jnp.bfloat16)
-    line_part = lax.dot_general(
-        jnp.pad(line_hidden, ((0, 0), (2 * units, 0))),
-        dense_weights,
-        (((1,), (1,)), ((), ())),
-        preferred_element_type=jnp.float32,
-    ).astype(jnp.bfloat16)
-    line_sum = half_of(line_part, core, 1).astype(jnp.float32) + swapped(
-        half_of(line_part, 1 - core, 1)
-    ).astype(jnp.float32)
-    dense = (
-        exchanged(line_sum.astype(jnp.bfloat16).reshape(lines, rows_dev, width // 2), "ep_0")
-        .astype(jnp.float32)
-        .sum(axis=0)
-    )
-
-    mine = arrived.reshape(experts * capacity, -1)
+
+    first = jnp.concatenate(
+        [jnp.broadcast_to(expert_in[None], (lines, rows_dev, width)), side], axis=2
+    )
+    line = exchanged(first, "ep_0").reshape(lines * rows_dev, width + 256)
+    line_in = line[:, :width]
+    line_place = line[:, width + 96 : width + 112]
+    line_high = line[:, width + 112 : width + 128]
+    line_low = line[:, width + 224 : width + 240]
+    slots = plane * lines * CAP
+    row = lax.broadcasted_iota(jnp.int32, (slots, lines * rows_dev), 0)
+    col = lax.broadcasted_iota(jnp.int32, (slots, lines * rows_dev), 1)
+    spread = (
+        lax.broadcasted_iota(jnp.int32, (slots, plane), 0) // (lines * CAP)
+        == lax.broadcasted_iota(jnp.int32, (slots, plane), 1)
+    ).astype(jnp.bfloat16)
+
+    def over_slots(array):
+        return lax.dot_general(
+            spread, array, (((1,), (1,)), ((), ())), preferred_element_type=jnp.float32
+        )
+
+    taken = (over_slots(line_place) == (1 + row % CAP).astype(jnp.float32)) & (
+        row // CAP % lines == col // rows_dev
+    )
+    rows = jnp.dot(
+        taken.astype(jnp.bfloat16), half_of(line_in, core, 1), preferred_element_type=jnp.float32
+    ).astype(jnp.bfloat16)
+    weights = line[:, width:].reshape(4, lines * rows_dev // 4, 256).transpose(1, 0, 2)
+    weights = weights.reshape(1, lines * rows_dev // 4, half)
+    second = jnp.concatenate(
+        [
+            rows.reshape(plane, lines * CAP, half),
+            jnp.broadcast_to(weights, (plane, lines * rows_dev // 4, half)),
+        ],
+        axis=2,
+    )
+    arrived = exchanged(second, PLANE)
+    mine = arrived[:, :, :half].reshape(slots, half)
+    dense_weights = (
+        arrived[:, :, half:]
+        .reshape(plane, 2, rows_dev, 4, 2, 128)
+        .transpose(3, 1, 0, 4, 2, 5)
+        .reshape(width, 128)
+    )
+
     theirs = swapped(mine)
     gate, up, down = expert_gate[0], expert_up[0], expert_down[0]
     gate_pre = jnp.dot(
@@ -172,14 +184,41 @@
     summed = (for_me.astype(jnp.float32) + swapped(for_them).astype(jnp.float32)).astype(
         jnp.bfloat16
     )
-    came_back = exchanged(summed.reshape(experts, capacity, -1), EP)
-    routed = jnp.dot(
-        weighing,
-        came_back.reshape(experts * capacity, -1).astype(jnp.float32),
-        precision=lax.Precision.HIGHEST,
-    )
+    summed, dense_weights = lax.optimization_barrier((summed, dense_weights))
+    with jax.named_scope("return"):
+        came_back = exchanged(summed.reshape(plane, lines * CAP, half), PLANE)
+    with jax.named_scope("dense"):
+        branch = jax.nn.sigmoid(jnp.dot(line_in, branch_gate, preferred_element_type=jnp.float32))
+        paired = jnp.dot(line_in, dense_weights, preferred_element_type=jnp.float32)
+        line_hidden = (jax.nn.silu(paired[:, :units]) * paired[:, units : 2 * units]).astype(
+            jnp.bfloat16
+        )
+        line_part = lax.dot_general(
+            jnp.pad(line_hidden, ((0, 0), (2 * units, 128 - 3 * units))),
+            dense_weights,
+            (((1,), (1,)), ((), ())),
+            preferred_element_type=jnp.float32,
+        ).astype(jnp.bfloat16)
+        dense = branch[:, None] * (
+            half_of(line_part, core, 1).astype(jnp.float32)
+            + swapped(half_of(line_part, 1 - core, 1)).astype(jnp.float32)
+        )
+        weighing = jnp.where(taken, over_slots(line_high) + over_slots(line_low), 0.0)
+        weigh_high = weighing.astype(jnp.bfloat16)
+        weigh_low = (weighing - weigh_high.astype(jnp.float32)).astype(jnp.bfloat16)
+
+    def combined(part):
+        return lax.dot_general(
+            part,
+            came_back.reshape(slots, half),
+            (((0,), (0,)), ((), ())),
+            preferred_element_type=jnp.float32,
+        )
+
+    third = (combined(weigh_high) + combined(weigh_low) + dense).astype(jnp.bfloat16)
+    parts = exchanged(third.reshape(lines, rows_dev, half), "ep_0")
     own_half = half_of(residual, core, 1).astype(jnp.float32)
-    return (own_half + routed + branch[:, None] * dense).astype(jnp.bfloat16)
+    return (own_half + parts.astype(jnp.float32).sum(axis=0)).astype(jnp.bfloat16)
 
 
 def solution(mesh):

time: 133 us -> 90.2 us (0.68); the launches traced: 130 us -> 89.4 us
  waiting for transfers between devices: 67.3 us -> 23.7 us
  blocking collectives: 0 us -> 33.1 us
  starting transfers between devices: 41.2 us -> 16.6 us
  local copies, waits for them, and re-layouts: 8.84 us -> 3.06 us
    all_to_all x5 -> x2, waiting for transfers between devices: 64.2 us -> 22.8 us  [exchanged(): return lax.all_to_all(array, axis, split_axis=0, concat_axis=0, tiled=True)]
    all_to_all x0 -> x2, blocking collectives: none -> 33.1 us  [exchanged(): return lax.all_to_all(array, axis, split_axis=0, concat_axis=0, tiled=True)]
    all_to_all x5 -> x2, starting transfers between devices: 32.8 us -> 10.1 us  [exchanged(): return lax.all_to_all(array, axis, split_axis=0, concat_axis=0, tiled=True)]
    unnamed x37 -> x38, local copies, waits for them, and re-layouts: 4.05 us -> 1.18 us
    reshape x4 -> x1, local copies, waits for them, and re-layouts: 2.38 us -> 0.12 us  [shards(): packed = packed.reshape(lines, rows_own, 3 * units)]
    ppermute x4, waiting for transfers between devices: 3.05 us -> 0.87 us  [swapped(): return lax.ppermute(array, 'tp', SWAP)]
    ppermute x4, starting transfers between devices: 8.34 us -> 6.54 us  [swapped(): return lax.ppermute(array, 'tp', SWAP)]
  transfers between devices with their start and end apart: 9 -> 6, of which waited for: 8 -> 4; matrix products, arithmetic and copies ran while one was open for 5% -> 4% of each run, Pallas kernels for 0% -> 0%
where the time goes in v2:
time: 90.2 us; the launch traced here: 89.4 us
  blocking collectives  33.1 us (37%)
  waiting for transfers between devices  23.7 us (26%)
  starting transfers between devices  16.6 us (18%)
  matrix products  8.7 us (10%)
  other arithmetic  3.61 us (4%)
  local copies, waits for them, and re-layouts  3.06 us (3%)
    all_to_all x2, blocking collectives, exchanged(): return lax.all_to_all(array, axis, split_axis=0, concat_axis=0, tiled=True)  33.1 us
    all_to_all x2, waiting for transfers between devices, exchanged(): return lax.all_to_all(array, axis, split_axis=0, concat_axis=0, tiled=True)  22.8 us
    all_to_all x2, starting transfers between devices, exchanged(): return lax.all_to_all(array, axis, split_axis=0, concat_axis=0, tiled=True)  10.1 us
    ppermute x4, starting transfers between devices, swapped(): return lax.ppermute(array, 'tp', SWAP)  6.54 us
  transfers between devices with their start and end apart: 6, of which 4 were waited for; matrix products, arithmetic and copies ran while one was open for 4% of the time, Pallas kernels for 0%

profile of v2, /device:TPU:1, one launch (start us, length us, event | category | flops | bytes accessed | tf_op | source)
XLA Modules:
  0.0 89.4 jit_solution(12257926813919380896)
XLA Ops:
  0.0 0.8 convert_element_type.122
  0.9 0.9 fusion.39
  1.8 1.4 %convolution_multiply_fusion.2 = f32[8,128]{1,0:T(8,128)S(1)} fusion(bf16[2048,128]{1,0:T(8,128)(2,1)} %param.23, bf16[8,2048]{1,0:T(8,128)(2,1)} %param.21, f32[2048]{0:T(1024)S(1)} %convert_element_type.122, f32[8]{0:T(128)S(1)} %add_rsqrt_fusion.2), kind=kOutput, calls=%fused_computation.25 | convolution fusion | flops 4260864 | bytes 569376 | tf_op jit(solution)/shard_map/dot_general | solution.py:102
  3.2 1.4 %fusion.11 = f32[8]{0:T(128)S(1)} fusion(f32[8,128]{1,0:T(8,128)S(1)} %convolution_multiply_fusion.2, bf16[2048,128]{1,0:T(8,128)(2,1)} %param.24, bf16[8,2048]{1,0:T(8,128)(2,1)} %param.21, f32[2048]{0:T(1024)S(1)} %convert_element_type.122, f32[8]{0:T(128)S(1)} %add_rsqrt_fusion.2), kind=kOutput, calls=%fused_computation.27 | convolution fusion | flops 4261880 | bytes 569408 | tf_op jit(solution)/shard_map/dot_general | solution.py:103
  4.6 0.3 fusion.66
  5.0 0.0 copy-start.17
  5.0 0.2 fusion.16
  5.2 0.0 copy-start.13
  5.2 0.0 copy-start.8
  5.3 0.4 multiply_reduce_fusion
  5.7 0.3 convolution_convert_fusion.1
  6.0 3.2 %collective-permute-start = (bf16[8,2048]{1,0:T(8,128)(2,1)S(1)}, bf16[8,2048]{1,0:T(8,128)(2,1)S(1)}, u32[]{:S(2)}, u32[]{:S(2)}) collective-permute-start(bf16[8,2048]{1,0:T(8,128)(2,1)S(1)} %convolution_convert_fusion.1), channel_id=1, source_target_pairs={{0,1},{1,0},{2,3},{3,2},{4,5},{5,4},{6,7},{7,6},{8,9},{9,8},{10,11... | collective-permute-start | bytes 98312 | tf_op jit(solution)/shard_map/ppermute | solution.py:22
  9.2 0.1 reduce_sum.92
  9.3 0.1 broadcast_divide_fusion
  9.4 0.1 copy.40
  9.5 0.1 copy.39
  9.6 0.1 select_reduce_fusion
  9.7 0.1 reduce_sum.94
  9.8 0.1 stack.12
  9.9 0.1 copy.36
  9.9 0.1 stack.13
  10.0 0.1 copy.37
  10.1 0.1 stack.14
  10.2 0.1 copy.38
  10.2 0.3 maximum_bitcast_fusion
  10.5 0.1 reshape.89
  10.7 0.1 reduce_sum.91
  10.8 0.1 fusion.36
  11.0 0.1 fusion.38
  11.1 0.8 concatenate.7
  11.9 6.5 %all-to-all-start = ((bf16[8,8,2304]{2,1,0:T(8,128)(2,1)}), bf16[8,8,2304]{2,1,0:T(8,128)(2,1)S(1)}, u32[]{:S(2)}, u32[]{:S(2)}) async-start(bf16[8,8,2304]{2,1,0:T(8,128)(2,1)} %concatenate.7), calls=%async_computation | async-start | bytes 589824 | tf_op jit(solution)/shard_map/all_to_all | solution.py:31
  18.5 13.0 %all-to-all-done = bf16[8,8,2304]{2,1,0:T(8,128)(2,1)S(1)} async-done(((bf16[8,8,2304]{2,1,0:T(8,128)(2,1)}), bf16[8,8,2304]{2,1,0:T(8,128)(2,1)S(1)}, u32[]{:S(2)}, u32[]{:S(2)}) %all-to-all-start) | async-done | bytes 294944 | tf_op jit(solution)/shard_map/all_to_all | solution.py:31
  31.5 0.3 fusion.7
  31.8 0.3 convolution_convert_fusion.4
  32.2 0.1 broadcast_in_dim.15
  32.2 0.1 pad_maximum_fusion
  32.3 22.8 %all_to_all.20 = bf16[16,16,2048]{2,1,0:T(8,128)(2,1)S(1)} all-to-all(bf16[16,16,2048]{2,1,0:T(8,128)(2,1)S(1)} %pad_maximum_fusion), channel_id=1, replica_groups=mesh['ep_0'=8,'ep_1'=4,'ep_2'=4,'tp'=2] {'ep_1','ep_2'}, dimensions={0} | all-to-all | bytes 2097152 | tf_op jit(solution)/shard_map/all_to_all | solution.py:31
  55.2 0.1 fusion.90
  55.2 1.9 %collective-permute-start.1 = (bf16[256,1024]{1,0:T(8,128)(2,1)S(1)}, bf16[256,1024]{1,0:T(8,128)(2,1)S(1)}, u32[]{:S(2)}, u32[]{:S(2)}) collective-permute-start(bf16[256,1024]{1,0:T(8,128)(2,1)S(1)} %bitcast.82), channel_id=1, source_target_pairs={{0,1},{1,0},{2,3},{3,2},{4,5},{5,4},{6,7},{7,6},{8,9},{9,8},{10,11... | collective-permute-start | bytes 1572872 | tf_op jit(solution)/shard_map/ppermute | solution.py:22
  57.2 0.3 fusion.25
  57.5 0.7 copy-done.6
  58.3 0.3 fusion.22
  58.6 0.2 collective-permute-done.1
  58.7 0.3 convolution_add_fusion.2
  59.0 0.3 fusion.2
  59.3 0.3 copy-done.4
  59.6 0.3 convolution_convert_fusion.2
  59.9 0.9 %collective-permute-start.2 = (bf16[256,1024]{1,0:T(8,128)(2,1)S(1)}, bf16[256,1024]{1,0:T(8,128)(2,1)S(1)}, u32[]{:S(2)}, u32[]{:S(2)}) collective-permute-start(bf16[256,1024]{1,0:T(8,128)(2,1)S(1)} %convolution_convert_fusion.2), channel_id=1, source_target_pairs={{0,1},{1,0},{2,3},{3,2},{4,5},{5,4},{6,7},{7,6},{8,9},{9,8},{10,11... | collective-permute-start | bytes 1572872 | tf_op jit(solution)/shard_map/ppermute | solution.py:22
  60.8 0.3 fusion.35
  61.1 0.3 fusion.3
  61.4 0.2 fusion.15
  61.6 0.1 copy.45
  61.7 0.7 collective-permute-done.2
  62.4 1.1 %add_convert_fusion = bf16[256,1024]{1,0:T(8,128)(2,1)} fusion(bf16[256,1024]{1,0:T(8,128)(2,1)S(1)} %collective-permute-done.2, bf16[256,128]{1,0:T(8,128)(2,1)S(1)} %fusion.2, bf16[1,128,2048]{2,1,0:T(8,128)(2,1)S(1)} %copy-done.4, s32[]{:T(128)S(6)} %select_n.52), kind=kOutput, calls=%fused_computation.36 | convolution fusion | flops 68419584 | bytes 1376260 | tf_op jit(solution)/shard_map/dot_general | solution.py:181
  63.4 3.6 %all-to-all-start.2 = ((bf16[16,16,1024]{2,1,0:T(8,128)(2,1)}), bf16[16,16,1024]{2,1,0:T(8,128)(2,1)S(1)}, u32[]{:S(2)}, u32[]{:S(2)}) async-start(bf16[16,16,1024]{2,1,0:T(8,128)(2,1)} %bitcast.20), calls=%async_computation.2 | async-start | bytes 1048576 | tf_op jit(solution)/shard_map/return/all_to_all | solution.py:31
  67.0 0.2 fusion.86
  67.2 0.1 fusion.54
  67.3 0.3 convolution_convert_fusion
  67.7 0.5 collective-permute-start.3
  68.2 9.8 %all-to-all-done.2 = bf16[16,16,1024]{2,1,0:T(8,128)(2,1)S(1)} async-done(((bf16[16,16,1024]{2,1,0:T(8,128)(2,1)}), bf16[16,16,1024]{2,1,0:T(8,128)(2,1)S(1)}, u32[]{:S(2)}, u32[]{:S(2)}) %all-to-all-start.2) | async-done | bytes 524320 | tf_op jit(solution)/shard_map/return/all_to_all | solution.py:31
  77.9 0.2 fusion.61
  78.2 0.2 fusion.33
  78.4 10.3 %all_to_all.21 = bf16[8,8,1024]{2,1,0:T(8,128)(2,1)S(1)} all-to-all(bf16[8,8,1024]{2,1,0:T(8,128)(2,1)S(1)} %fusion.33), channel_id=1, replica_groups=mesh['ep_0'=8,'ep_1'=4,'ep_2'=4,'tp'=2] {'ep_0'}, dimensions={0} | all-to-all | bytes 262144 | tf_op jit(solution)/shard_map/all_to_all | solution.py:31
  88.7 0.6 add_convert_fusion.2
  (59 shorter events, 0.3 us)
Async XLA Ops:
  0.0 5.7 %copy-start = (bf16[256,2048]{1,0:T(8,128)(2,1)S(1)}, bf16[256,2048]{1,0:T(8,128)(2,1)}, u32[]{:S(2)}) copy-start(bf16[256,2048]{1,0:T(8,128)(2,1)} %param.31) | copy-start | bytes 3145732
  0.0 4.6 %copy-start.3 = (bf16[8,2048]{1,0:T(8,128)(2,1)S(1)}, bf16[8,2048]{1,0:T(8,128)(2,1)}, u32[]{:S(2)}) copy-start(bf16[8,2048]{1,0:T(8,128)(2,1)} %param.21) | copy-start | bytes 98308
  0.0 4.6 %copy-start.14 = (bf16[2048,16]{0,1:T(8,128)(2,1)S(1)}, bf16[2048,16]{0,1:T(8,128)(2,1)}, u32[]{:S(2)}) copy-start(bf16[2048,16]{0,1:T(8,128)(2,1)} %param.26) | copy-start | bytes 196612
  0.0 4.6 %copy-start.15 = (bf16[16,128]{1,0:T(8,128)(2,1)S(1)}, bf16[16,128]{1,0:T(8,128)(2,1)}, u32[]{:S(2)}) copy-start(bf16[16,128]{1,0:T(8,128)(2,1)} %param.27) | copy-start | bytes 12292
  0.0 4.6 %copy-start.16 = (f32[128]{0:T(128)S(1)}, f32[128]{0:T(128)}, u32[]{:S(2)}) copy-start(f32[128]{0:T(128)} %param.28) | copy-start | bytes 1540
  0.0 4.9 %copy-start.2 = (f32[8,1,128,256]{3,2,1,0:T(8,128)S(1)}, f32[8,1,128,256]{3,2,1,0:T(8,128)}, u32[]{:S(2)}) copy-start(f32[8,1,128,256]{3,2,1,0:T(8,128)} %param.30) | copy-start | bytes 3145732
  1.8 3.4 %copy-start.1 = (bf16[2048,256]{1,0:T(8,128)(2,1)S(1)}, bf16[2048,256]{1,0:T(8,128)(2,1)}, u32[]{:S(2)}) copy-start(bf16[2048,256]{1,0:T(8,128)(2,1)} %param.25) | copy-start | bytes 3145732
  5.0 0.7 copy-start.17
  5.2 4.0 %copy-start.7 = (f32[8,6]{1,0:T(8,128)S(1)}, f32[8,6]{1,0:T(8,128)}, u32[]{:S(2)}) copy-start(f32[8,6]{1,0:T(8,128)} %param.34) | copy-start | bytes 580
  5.2 4.3 %copy-start.13 = (s32[8,6]{1,0:T(8,128)S(1)}, s32[8,6]{1,0:T(8,128)}, u32[]{:S(2)}) copy-start(s32[8,6]{1,0:T(8,128)} %param.33) | copy-start | bytes 580
  5.2 4.5 %copy-start.8 = (bf16[16,256]{1,0:T(8,128)(2,1)S(1)}, bf16[16,256]{1,0:T(8,128)(2,1)}, u32[]{:S(2)}) copy-start(bf16[16,256]{1,0:T(8,128)(2,1)} %param.38) | copy-start | bytes 24580
  5.2 4.7 %copy-start.9 = (bf16[16,256]{1,0:T(8,128)(2,1)S(1)}, bf16[16,256]{1,0:T(8,128)(2,1)}, u32[]{:S(2)}) copy-start(bf16[16,256]{1,0:T(8,128)(2,1)} %param.39) | copy-start | bytes 24580
  5.2 4.8 %copy-start.10 = (bf16[256,16]{0,1:T(8,128)(2,1)S(1)}, bf16[256,16]{0,1:T(8,128)(2,1)}, u32[]{:S(2)}) copy-start(bf16[256,16]{0,1:T(8,128)(2,1)} %param.40) | copy-start | bytes 24580
  5.7 5.1 %copy-start.11 = (bf16[2048]{0:T(1024)(128)(2,1)S(1)}, bf16[2048]{0:T(1024)(128)(2,1)}, u32[]{:S(2)}) copy-start(bf16[2048]{0:T(1024)(128)(2,1)} %param.32) | copy-start | bytes 12292
  6.0 4.8 %collective-permute-start = (bf16[8,2048]{1,0:T(8,128)(2,1)S(1)}, bf16[8,2048]{1,0:T(8,128)(2,1)S(1)}, u32[]{:S(2)}, u32[]{:S(2)}) collective-permute-start(bf16[8,2048]{1,0:T(8,128)(2,1)S(1)} %convolution_convert_fusion.1), channel_id=1, source_target_pairs={{0,1},{1,0},{2,3},{3,2},{4,5},{5,4},{6,7},{7,6},{8,9},{9,8},{10,11... | collective-permute-start | bytes 98312 | tf_op jit(solution)/shard_map/ppermute | solution.py:22
  11.9 19.6 %all-to-all-start = ((bf16[8,8,2304]{2,1,0:T(8,128)(2,1)}), bf16[8,8,2304]{2,1,0:T(8,128)(2,1)S(1)}, u32[]{:S(2)}, u32[]{:S(2)}) async-start(bf16[8,8,2304]{2,1,0:T(8,128)(2,1)} %concatenate.7), calls=%async_computation | async-start | bytes 589824 | tf_op jit(solution)/shard_map/all_to_all | solution.py:31
  55.1 2.0 %copy-start.12 = (bf16[2048]{0:T(1024)(128)(2,1)S(1)}, bf16[2048]{0:T(1024)(128)(2,1)}, u32[]{:S(2)}) copy-start(bf16[2048]{0:T(1024)(128)(2,1)} %param.41) | copy-start | bytes 12292
  55.2 2.0 %copy-start.5 = (bf16[1,2048,128]{2,1,0:T(8,128)(2,1)S(1)}, bf16[1,2048,128]{2,1,0:T(8,128)(2,1)}, u32[]{:S(2)}) copy-start(bf16[1,2048,128]{2,1,0:T(8,128)(2,1)} %param.35) | copy-start | bytes 1572868
  55.2 3.5 %collective-permute-start.1 = (bf16[256,1024]{1,0:T(8,128)(2,1)S(1)}, bf16[256,1024]{1,0:T(8,128)(2,1)S(1)}, u32[]{:S(2)}, u32[]{:S(2)}) collective-permute-start(bf16[256,1024]{1,0:T(8,128)(2,1)S(1)} %bitcast.82), channel_id=1, source_target_pairs={{0,1},{1,0},{2,3},{3,2},{4,5},{5,4},{6,7},{7,6},{8,9},{9,8},{10,11... | collective-permute-start | bytes 1572872 | tf_op jit(solution)/shard_map/ppermute | solution.py:22
  57.2 1.0 %copy-start.6 = (bf16[1,2048,128]{2,1,0:T(8,128)(2,1)S(1)}, bf16[1,2048,128]{2,1,0:T(8,128)(2,1)}, u32[]{:S(2)}) copy-start(bf16[1,2048,128]{2,1,0:T(8,128)(2,1)} %param.36) | copy-start | bytes 1572868
  58.5 1.0 %copy-start.4 = (bf16[1,128,2048]{2,1,0:T(8,128)(2,1)S(1)}, bf16[1,128,2048]{2,1,0:T(8,128)(2,1)}, u32[]{:S(2)}) copy-start(bf16[1,128,2048]{2,1,0:T(8,128)(2,1)} %param.37) | copy-start | bytes 1572868
  59.9 2.5 %collective-permute-start.2 = (bf16[256,1024]{1,0:T(8,128)(2,1)S(1)}, bf16[256,1024]{1,0:T(8,128)(2,1)S(1)}, u32[]{:S(2)}, u32[]{:S(2)}) collective-permute-start(bf16[256,1024]{1,0:T(8,128)(2,1)S(1)} %convolution_convert_fusion.2), channel_id=1, source_target_pairs={{0,1},{1,0},{2,3},{3,2},{4,5},{5,4},{6,7},{7,6},{8,9},{9,8},{10,11... | collective-permute-start | bytes 1572872 | tf_op jit(solution)/shard_map/ppermute | solution.py:22
  63.4 14.5 %all-to-all-start.2 = ((bf16[16,16,1024]{2,1,0:T(8,128)(2,1)}), bf16[16,16,1024]{2,1,0:T(8,128)(2,1)S(1)}, u32[]{:S(2)}, u32[]{:S(2)}) async-start(bf16[16,16,1024]{2,1,0:T(8,128)(2,1)} %bitcast.20), calls=%async_computation.2 | async-start | bytes 1048576 | tf_op jit(solution)/shard_map/return/all_to_all | solution.py:31
  67.7 10.5 %collective-permute-start.3 = (bf16[64,1024]{1,0:T(8,128)(2,1)S(1)}, bf16[64,1024]{1,0:T(8,128)(2,1)S(1)}, u32[]{:S(2)}, u32[]{:S(2)}) collective-permute-start(bf16[64,1024]{1,0:T(8,128)(2,1)S(1)} %constant_dynamic-slice_fusion), channel_id=1, source_target_pairs={{0,1},{1,0},{2,3},{3,2},{4,5},{5,4},{6,7},{7,6},{8,9},{9,8},{10,11... | collective-permute-start | bytes 393224 | tf_op jit(solution)/shard_map/dense/ppermute | solution.py:22

commit v3 on v2

--- a/solution.py
+++ b/solution.py
@@ -4,9 +4,8 @@
 from jax.sharding import Mesh
 from jax.sharding import PartitionSpec as P
 
+
 DK = 128
-DV = 256
-TOPK = 6
 EP = ("ep_0", "ep_1", "ep_2")
 PLANE = ("ep_1", "ep_2")
 CAP = 2
@@ -122,13 +121,27 @@
     expert_in = rms_scale(residual, second_gain).astype(jnp.bfloat16)
 
     first = jnp.concatenate(
-        [jnp.broadcast_to(expert_in[None], (lines, rows_dev, width)), side], axis=2
-    )
-    line = exchanged(first, "ep_0").reshape(lines * rows_dev, width + 256)
-    line_in = line[:, :width]
-    line_place = line[:, width + 96 : width + 112]
-    line_high = line[:, width + 112 : width + 128]
-    line_low = line[:, width + 224 : width + 240]
+        [jnp.broadcast_to(half_of(expert_in, core, 1)[None], (lines, rows_dev, half)), side],
+        axis=2,
+    )
+    first, gate, up, down = lax.optimization_barrier(
+        (first, expert_gate[0], expert_up[0], expert_down[0])
+    )
+    line = exchanged(first, "ep_0")
+    line = line.reshape(lines * rows_dev, half + 256)
+    given = jnp.concatenate([half_of(gate, 1 - core, 0), half_of(up, 1 - core, 0)], axis=1)
+    taken_in = swapped(given)
+    taken_down = swapped(half_of(down, 1 - core, 1))
+    inner = gate.shape[1]
+    weights_in = jnp.concatenate(
+        [half_of(gate, core, 0), taken_in[:, :inner], half_of(up, core, 0), taken_in[:, inner:]],
+        axis=1,
+    )
+    weights_down = jnp.concatenate([half_of(down, core, 1), taken_down], axis=0)
+    line_in = line[:, :half]
+    line_place = line[:, half + 96 : half + 112]
+    line_high = line[:, half + 112 : half + 128]
+    line_low = line[:, half + 224 : half + 240]
     slots = plane * lines * CAP
     row = lax.broadcasted_iota(jnp.int32, (slots, lines * rows_dev), 0)
     col = lax.broadcasted_iota(jnp.int32, (slots, lines * rows_dev), 1)
@@ -146,9 +159,9 @@
         row // CAP % lines == col // rows_dev
     )
     rows = jnp.dot(
-        taken.astype(jnp.bfloat16), half_of(line_in, core, 1), preferred_element_type=jnp.float32
-    ).astype(jnp.bfloat16)
-    weights = line[:, width:].reshape(4, lines * rows_dev // 4, 256).transpose(1, 0, 2)
+        taken.astype(jnp.bfloat16), line_in, preferred_element_type=jnp.float32
+    ).astype(jnp.bfloat16)
+    weights = line[:, half:].reshape(4, lines * rows_dev // 4, 256).transpose(1, 0, 2)
     weights = weights.reshape(1, lines * rows_dev // 4, half)
     second = jnp.concatenate(
         [
@@ -166,46 +179,41 @@
         .reshape(width, 128)
     )
 
-    theirs = swapped(mine)
-    gate, up, down = expert_gate[0], expert_up[0], expert_down[0]
-    gate_pre = jnp.dot(
-        mine, half_of(gate, core, 0), preferred_element_type=jnp.float32
-    ) + jnp.dot(theirs, half_of(gate, 1 - core, 0), preferred_element_type=jnp.float32)
-    up_pre = jnp.dot(
-        mine, half_of(up, core, 0), preferred_element_type=jnp.float32
-    ) + jnp.dot(theirs, half_of(up, 1 - core, 0), preferred_element_type=jnp.float32)
-    activated = (jax.nn.silu(gate_pre) * up_pre).astype(jnp.bfloat16)
-    for_them = jnp.dot(
-        activated, half_of(down, 1 - core, 1), preferred_element_type=jnp.float32
-    ).astype(jnp.bfloat16)
-    for_me = jnp.dot(
-        activated, half_of(down, core, 1), preferred_element_type=jnp.float32
-    ).astype(jnp.bfloat16)
-    summed = (for_me.astype(jnp.float32) + swapped(for_them).astype(jnp.float32)).astype(
+    partial_in = jnp.dot(mine, weights_in, preferred_element_type=jnp.float32)
+    blocks = [partial_in[:, k * inner : (k + 1) * inner] for k in (1, 0, 3, 2)]
+    pre = partial_in + swapped(
+        jnp.concatenate(blocks, axis=1).astype(jnp.bfloat16)
+    ).astype(jnp.float32)
+    activated = (jax.nn.silu(pre[:, : 2 * inner]) * pre[:, 2 * inner :]).astype(jnp.bfloat16)
+    summed = jnp.dot(activated, weights_down, preferred_element_type=jnp.float32).astype(
         jnp.bfloat16
     )
-    summed, dense_weights = lax.optimization_barrier((summed, dense_weights))
-    with jax.named_scope("return"):
-        came_back = exchanged(summed.reshape(plane, lines * CAP, half), PLANE)
-    with jax.named_scope("dense"):
-        branch = jax.nn.sigmoid(jnp.dot(line_in, branch_gate, preferred_element_type=jnp.float32))
-        paired = jnp.dot(line_in, dense_weights, preferred_element_type=jnp.float32)
-        line_hidden = (jax.nn.silu(paired[:, :units]) * paired[:, units : 2 * units]).astype(
-            jnp.bfloat16
-        )
-        line_part = lax.dot_general(
-            jnp.pad(line_hidden, ((0, 0), (2 * units, 128 - 3 * units))),
-            dense_weights,
-            (((1,), (1,)), ((), ())),
-            preferred_element_type=jnp.float32,
-        ).astype(jnp.bfloat16)
-        dense = branch[:, None] * (
-            half_of(line_part, core, 1).astype(jnp.float32)
-            + swapped(half_of(line_part, 1 - core, 1)).astype(jnp.float32)
-        )
-        weighing = jnp.where(taken, over_slots(line_high) + over_slots(line_low), 0.0)
-        weigh_high = weighing.astype(jnp.bfloat16)
-        weigh_low = (weighing - weigh_high.astype(jnp.float32)).astype(jnp.bfloat16)
+    summed, dense_weights, line_in = lax.optimization_barrier((summed, dense_weights, line_in))
+    came_back = exchanged(summed.reshape(plane, lines * CAP, half), PLANE)
+    line_rest = swapped(line_in)
+    pre_gate = jnp.dot(
+        line_in, half_of(branch_gate, core, 0), preferred_element_type=jnp.float32
+    ) + jnp.dot(line_rest, half_of(branch_gate, 1 - core, 0), preferred_element_type=jnp.float32)
+    branch = jax.nn.sigmoid(pre_gate)
+    paired = jnp.dot(
+        line_in, half_of(dense_weights, core, 0), preferred_element_type=jnp.float32
+    ) + jnp.dot(line_rest, half_of(dense_weights, 1 - core, 0), preferred_element_type=jnp.float32)
+    line_hidden = (jax.nn.silu(paired[:, :units]) * paired[:, units : 2 * units]).astype(
+        jnp.bfloat16
+    )
+    line_part = lax.dot_general(
+        jnp.pad(line_hidden, ((0, 0), (2 * units, 128 - 3 * units))),
+        dense_weights,
+        (((1,), (1,)), ((), ())),
+        preferred_element_type=jnp.float32,
+    ).astype(jnp.bfloat16)
+    dense = branch[:, None] * (
+        half_of(line_part, core, 1).astype(jnp.float32)
+        + swapped(half_of(line_part, 1 - core, 1)).astype(jnp.float32)
+    )
+    weighing = jnp.where(taken, over_slots(line_high) + over_slots(line_low), 0.0)
+    weigh_high = weighing.astype(jnp.bfloat16)
+    weigh_low = (weighing - weigh_high.astype(jnp.float32)).astype(jnp.bfloat16)
 
     def combined(part):
         return lax.dot_general(

time: 90.2 us -> 86.4 us (0.958)
  blocking collectives: 33.1 us -> 10.3 us
  starting transfers between devices: 16.6 us -> 27.1 us
  waiting for transfers between devices: 23.7 us -> 29.9 us
  other arithmetic: 3.61 us -> 4.75 us
    all_to_all x2 -> x1, blocking collectives: 33.1 us -> 10.3 us  [exchanged(): return lax.all_to_all(array, axis, split_axis=0, concat_axis=0, tiled=True)]
    all_to_all x2 -> x3, starting transfers between devices: 10.1 us -> 16.9 us  [exchanged(): return lax.all_to_all(array, axis, split_axis=0, concat_axis=0, tiled=True)]
    all_to_all x2 -> x3, waiting for transfers between devices: 22.8 us -> 28.2 us  [exchanged(): return lax.all_to_all(array, axis, split_axis=0, concat_axis=0, tiled=True)]
    ppermute x4 -> x6, starting transfers between devices: 6.54 us -> 10.1 us  [swapped(): return lax.ppermute(array, 'tp', SWAP)]
    concatenate x1, other arithmetic: 0.09 us -> 1.07 us  [shards(): jnp.concatenate([rows.reshape(plane, lines * CAP, half), jnp.broadcast_to...]
    dynamic_slice x1 -> x7, local copies, waits for them, and re-layouts: 0.02 us -> 0.95 us  [half_of(): return lax.dynamic_slice_in_dim(array, index * width, width, dim)]
    dot_general x9 -> x7, matrix products: 3.26 us -> 3.47 us  [the longest x1 2.07 us: shards(): jnp.dot(activated, weights_down, preferred_element_type=jnp.float32)]
  transfers between devices with their start and end apart: 6 -> 9, of which waited for: 4 -> 6; matrix products, arithmetic and copies ran while one was open for 4% -> 6% of each run, Pallas kernels for 0% -> 0%
where the time goes in v3:
time: 86.4 us; the launch traced here: 85.5 us
  waiting for transfers between devices  29.9 us (35%)
  starting transfers between devices  27.1 us (31%)
  blocking collectives  10.3 us (12%)
  matrix products  8.91 us (10%)
  other arithmetic  4.75 us (5%)
  local copies, waits for them, and re-layouts  3.9 us (5%)
    all_to_all x3, waiting for transfers between devices, exchanged(): return lax.all_to_all(array, axis, split_axis=0, concat_axis=0, tiled=True)  28.2 us
    all_to_all x3, starting transfers between devices, exchanged(): return lax.all_to_all(array, axis, split_axis=0, concat_axis=0, tiled=True)  16.9 us
    all_to_all x1, blocking collectives, exchanged(): return lax.all_to_all(array, axis, split_axis=0, concat_axis=0, tiled=True)  10.3 us
    ppermute x6, starting transfers between devices, swapped(): return lax.ppermute(array, 'tp', SWAP)  10.1 us
    dot_general x1, matrix products, shards(): jnp.dot(activated, weights_down, preferred_element_type=jnp.float32)  2.07 us
  transfers between devices with their start and end apart: 9, of which 6 were waited for; matrix products, arithmetic and copies ran while one was open for 6% of the time, Pallas kernels for 0%

profile of v3, /device:TPU:1, one launch (start us, length us, event | category | flops | bytes accessed | tf_op | source)
XLA Modules:
  0.0 85.5 jit_solution(10964361077183653648)
XLA Ops:
  0.0 0.8 convert_element_type.114
  0.9 0.9 %fusion.34 = f32[8]{0:T(128)S(1)} fusion(bf16[8,2048]{1,0:T(8,128)(2,1)} %param.21), kind=kLoop, calls=%fused_computation.67 | loop fusion | flops 49144 | bytes 32800 | tf_op jit(solution)/shard_map/reduce_sum | solution.py:37
  1.8 1.4 %convolution_multiply_fusion.2 = f32[8,128]{1,0:T(8,128)S(1)} fusion(bf16[2048,128]{1,0:T(8,128)(2,1)} %param.23, bf16[8,2048]{1,0:T(8,128)(2,1)} %param.21, f32[2048]{0:T(1024)S(1)} %convert_element_type.114, f32[8]{0:T(128)S(1)} %add_rsqrt_fusion.2), kind=kOutput, calls=%fused_computation.20 | convolution fusion | flops 4260864 | bytes 569376 | tf_op jit(solution)/shard_map/dot_general | solution.py:101
  3.2 1.4 %fusion.8 = f32[8]{0:T(128)S(1)} fusion(f32[8,128]{1,0:T(8,128)S(1)} %convolution_multiply_fusion.2, bf16[2048,128]{1,0:T(8,128)(2,1)} %param.24, bf16[8,2048]{1,0:T(8,128)(2,1)} %param.21, f32[2048]{0:T(1024)S(1)} %convert_element_type.114, f32[8]{0:T(128)S(1)} %add_rsqrt_fusion.2), kind=kOutput, calls=%fused_computation.22 | convolution fusion | flops 4261880 | bytes 569408 | tf_op jit(solution)/shard_map/dot_general | solution.py:102
  4.6 0.3 fusion.63
  5.0 0.2 fusion.22
  5.3 0.4 multiply_reduce_fusion.1
  5.7 0.3 convolution_convert_fusion.1
  6.0 3.2 %collective-permute-start = (bf16[8,2048]{1,0:T(8,128)(2,1)S(1)}, bf16[8,2048]{1,0:T(8,128)(2,1)S(1)}, u32[]{:S(2)}, u32[]{:S(2)}) collective-permute-start(bf16[8,2048]{1,0:T(8,128)(2,1)S(1)} %convolution_convert_fusion.1), channel_id=1, source_target_pairs={{0,1},{1,0},{2,3},{3,2},{4,5},{5,4},{6,7},{7,6},{8,9},{9,8},{10,11... | collective-permute-start | bytes 98312 | tf_op jit(solution)/shard_map/ppermute | solution.py:21
  9.2 0.1 reduce_sum.92
  9.4 0.1 broadcast_divide_fusion
  9.4 0.1 copy.40
  9.5 0.1 copy.39
  9.6 0.1 select_reduce_fusion
  9.7 0.1 reduce_sum.94
  9.8 0.1 stack.12
  9.9 0.1 copy.36
  9.9 0.1 stack.13
  10.0 0.1 copy.37
  10.1 0.1 stack.14
  10.2 0.1 copy.38
  10.3 0.3 maximum_bitcast_fusion
  10.5 0.1 reshape.83
  10.7 0.1 reduce_sum.91
  10.9 0.1 multiply_reduce_fusion
  11.0 0.1 fusion.51
  11.1 0.8 concatenate.20
  11.9 6.5 %all-to-all-start = ((bf16[8,8,1280]{2,1,0:T(8,128)(2,1)}), bf16[8,8,1280]{2,1,0:T(8,128)(2,1)S(1)}, u32[]{:S(2)}, u32[]{:S(2)}) async-start(bf16[8,8,1280]{2,1,0:T(8,128)(2,1)} %concatenate.20), calls=%async_computation | async-start | bytes 327680 | tf_op jit(solution)/shard_map/all_to_all | solution.py:30
  18.4 9.2 %all-to-all-done = bf16[8,8,1280]{2,1,0:T(8,128)(2,1)S(1)} async-done(((bf16[8,8,1280]{2,1,0:T(8,128)(2,1)}), bf16[8,8,1280]{2,1,0:T(8,128)(2,1)S(1)}, u32[]{:S(2)}, u32[]{:S(2)}) %all-to-all-start) | async-done | bytes 163872 | tf_op jit(solution)/shard_map/all_to_all | solution.py:30
  27.6 0.3 fusion.4
  27.9 0.3 convolution_convert_fusion.3
  28.3 1.1 %pad_maximum_fusion = bf16[16,16,2048]{2,1,0:T(8,128)(2,1)} fusion(bf16[16,16,1024]{2,1,0:T(8,128)(2,1)S(1)} %broadcast_in_dim.15, bf16[16,16,1024]{2,1,0:T(8,128)(2,1)S(1)} %bitcast.70), kind=kLoop, calls=%fused_computation.30 | loop fusion | flops 2097152 | bytes 2097152 | tf_op jit(solution)/shard_map/concatenate | solution.py:166
  29.4 6.9 %all-to-all-start.1 = ((bf16[16,16,2048]{2,1,0:T(8,128)(2,1)}), bf16[16,16,2048]{2,1,0:T(8,128)(2,1)S(1)}, u32[]{:S(2)}, u32[]{:S(2)}) async-start(bf16[16,16,2048]{2,1,0:T(8,128)(2,1)} %pad_maximum_fusion), calls=%async_computation.1 | async-start | bytes 2097152 | tf_op jit(solution)/shard_map/all_to_all | solution.py:30
  36.3 0.9 %constant_dynamic-slice_fusion.3 = (bf16[1024,128]{1,0:T(8,128)(2,1)}, bf16[1024,128]{1,0:T(8,128)(2,1)S(1)}, bf16[1024,128]{1,0:T(8,128)(2,1)S(1)}, bf16[1024,128]{1,0:T(8,128)(2,1)}) fusion(bf16[2048,128]{1,0:T(8,128)(2,1)S(1)} %bitcast.78, s32[]{:T(128)S(6)} %select_n.56, s32[]{:T(128)S(6)} %select_n.63, bf16[2048,128]{1,0:T(8,128)(2,1)S(1)} %bitcast.79), kind=kLoop, calls=%fused_computation.117 | loop fusion | bytes 2097160 | tf_op jit(solution)/shard_map/dynamic_slice | solution.py:26
  37.2 0.1 pad_maximum_fusion.1
  37.2 1.9 %collective-permute-start.1 = (bf16[1024,256]{1,0:T(8,128)(2,1)S(1)}, bf16[1024,256]{1,0:T(8,128)(2,1)S(1)}, u32[]{:S(2)}, u32[]{:S(2)}) collective-permute-start(bf16[1024,256]{1,0:T(8,128)(2,1)S(1)} %pad_maximum_fusion.1), channel_id=1, source_target_pairs={{0,1},{1,0},{2,3},{3,2},{4,5},{5,4},{6,7},{7,6},{8,9},{9,8},{10,11... | collective-permute-start | bytes 1572872 | tf_op jit(solution)/shard_map/ppermute | solution.py:21
  39.2 0.9 %collective-permute-start.3 = (bf16[128,1024]{1,0:T(8,128)(2,1)S(1)}, bf16[128,1024]{1,0:T(8,128)(2,1)}, u32[]{:S(2)}, u32[]{:S(2)}) collective-permute-start(bf16[128,1024]{1,0:T(8,128)(2,1)S(1)} %get-tuple-element.32), channel_id=1, source_target_pairs={{0,1},{1,0},{2,3},{3,2},{4,5},{5,4},{6,7},{7,6},{8,9},{9,8},{10,11... | collective-permute-start | bytes 786440 | tf_op jit(solution)/shard_map/ppermute | solution.py:21
  40.1 0.5 collective-permute-done.1
  40.7 10.8 %all-to-all-done.1 = bf16[16,16,2048]{2,1,0:T(8,128)(2,1)S(1)} async-done(((bf16[16,16,2048]{2,1,0:T(8,128)(2,1)}), bf16[16,16,2048]{2,1,0:T(8,128)(2,1)S(1)}, u32[]{:S(2)}, u32[]{:S(2)}) %all-to-all-start.1) | async-done | bytes 1048608 | tf_op jit(solution)/shard_map/all_to_all | solution.py:30
  51.5 0.1 fusion.83
  51.6 0.9 copy-done.7
  52.5 0.1 copy-done.8
  52.6 0.4 fusion.88
  53.1 3.2 %collective-permute-start.2 = (bf16[256,512]{1,0:T(8,128)(2,1)S(1)}, bf16[256,512]{1,0:T(8,128)(2,1)S(1)}, u32[]{:S(2)}, u32[]{:S(2)}) collective-permute-start(bf16[256,512]{1,0:T(8,128)(2,1)S(1)} %pad_maximum_fusion.2), channel_id=1, source_target_pairs={{0,1},{1,0},{2,3},{3,2},{4,5},{5,4},{6,7},{7,6},{8,9},{9,8},{10,11... | collective-permute-start | bytes 786440 | tf_op jit(solution)/shard_map/ppermute | solution.py:21
  56.3 0.3 fusion.33
  56.6 0.3 fusion
  56.9 0.5 collective-permute-done.2
  57.4 0.1 convert_add_fusion
  57.5 2.1 %convolution_convert_fusion.2 = bf16[256,1024]{1,0:T(8,128)(2,1)} fusion(bf16[128,1024]{1,0:T(8,128)(2,1)} %collective-permute-done.3, bf16[128,1024]{1,0:T(8,128)(2,1)S(1)} %get-tuple-element.31, f32[256,512]{1,0:T(8,128)S(1)} %convert_add_fusion), kind=kOutput, calls=%fused_computation.2 | convolution fusion | flops 135921664 | bytes 1572864 | tf_op jit(solution)/shard_map/dot_general | solution.py:188
  59.6 3.6 %all-to-all-start.2 = ((bf16[16,16,1024]{2,1,0:T(8,128)(2,1)}), bf16[16,16,1024]{2,1,0:T(8,128)(2,1)S(1)}, u32[]{:S(2)}, u32[]{:S(2)}) async-start(bf16[16,16,1024]{2,1,0:T(8,128)(2,1)} %bitcast.17), calls=%async_computation.2 | async-start | bytes 1048576 | tf_op jit(solution)/shard_map/all_to_all | solution.py:30
  63.2 0.5 collective-permute-start.4
  63.6 0.2 fusion.28
  63.8 0.1 convolution_bitcast_fusion.1
  64.0 0.7 collective-permute-done.4
  64.6 0.2 convolution_add_fusion.2
  64.8 0.1 fusion.49
  64.9 0.3 convolution_convert_fusion
  65.3 0.4 collective-permute-start.5
  65.7 0.1 fusion.13
  65.9 8.2 %all-to-all-done.2 = bf16[16,16,1024]{2,1,0:T(8,128)(2,1)S(1)} async-done(((bf16[16,16,1024]{2,1,0:T(8,128)(2,1)}), bf16[16,16,1024]{2,1,0:T(8,128)(2,1)S(1)}, u32[]{:S(2)}, u32[]{:S(2)}) %all-to-all-start.2) | async-done | bytes 524320 | tf_op jit(solution)/shard_map/all_to_all | solution.py:30
  74.1 0.2 fusion.58
  74.3 0.2 fusion.30
  74.5 10.3 %all_to_all.20 = bf16[8,8,1024]{2,1,0:T(8,128)(2,1)S(1)} all-to-all(bf16[8,8,1024]{2,1,0:T(8,128)(2,1)S(1)} %fusion.30), channel_id=1, replica_groups=mesh['ep_0'=8,'ep_1'=4,'ep_2'=4,'tp'=2] {'ep_0'}, dimensions={0} | all-to-all | bytes 262144 | tf_op jit(solution)/shard_map/all_to_all | solution.py:30
  84.9 0.6 add_convert_fusion.1
  (76 shorter events, 0.6 us)
Async XLA Ops:
  0.0 5.7 %copy-start = (bf16[256,2048]{1,0:T(8,128)(2,1)S(1)}, bf16[256,2048]{1,0:T(8,128)(2,1)}, u32[]{:S(2)}) copy-start(bf16[256,2048]{1,0:T(8,128)(2,1)} %param.31) | copy-start | bytes 3145732
  0.0 4.6 %copy-start.3 = (bf16[8,2048]{1,0:T(8,128)(2,1)S(1)}, bf16[8,2048]{1,0:T(8,128)(2,1)}, u32[]{:S(2)}) copy-start(bf16[8,2048]{1,0:T(8,128)(2,1)} %param.21) | copy-start | bytes 98308
  0.0 4.6 %copy-start.16 = (bf16[2048,16]{0,1:T(8,128)(2,1)S(1)}, bf16[2048,16]{0,1:T(8,128)(2,1)}, u32[]{:S(2)}) copy-start(bf16[2048,16]{0,1:T(8,128)(2,1)} %param.26) | copy-start | bytes 196612
  0.0 4.6 %copy-start.17 = (bf16[16,128]{1,0:T(8,128)(2,1)S(1)}, bf16[16,128]{1,0:T(8,128)(2,1)}, u32[]{:S(2)}) copy-start(bf16[16,128]{1,0:T(8,128)(2,1)} %param.27) | copy-start | bytes 12292
  0.0 4.6 %copy-start.18 = (f32[128]{0:T(128)S(1)}, f32[128]{0:T(128)}, u32[]{:S(2)}) copy-start(f32[128]{0:T(128)} %param.28) | copy-start | bytes 1540
  0.0 4.9 %copy-start.2 = (f32[8,1,128,256]{3,2,1,0:T(8,128)S(1)}, f32[8,1,128,256]{3,2,1,0:T(8,128)}, u32[]{:S(2)}) copy-start(f32[8,1,128,256]{3,2,1,0:T(8,128)} %param.30) | copy-start | bytes 3145732
  1.8 3.4 %copy-start.1 = (bf16[2048,256]{1,0:T(8,128)(2,1)S(1)}, bf16[2048,256]{1,0:T(8,128)(2,1)}, u32[]{:S(2)}) copy-start(bf16[2048,256]{1,0:T(8,128)(2,1)} %param.25) | copy-start | bytes 3145732
  5.0 0.7 copy-start.19
  5.2 4.0 %copy-start.9 = (f32[8,6]{1,0:T(8,128)S(1)}, f32[8,6]{1,0:T(8,128)}, u32[]{:S(2)}) copy-start(f32[8,6]{1,0:T(8,128)} %param.34) | copy-start | bytes 580
  5.2 4.3 %copy-start.13 = (s32[8,6]{1,0:T(8,128)S(1)}, s32[8,6]{1,0:T(8,128)}, u32[]{:S(2)}) copy-start(s32[8,6]{1,0:T(8,128)} %param.33) | copy-start | bytes 580
  5.2 4.6 %copy-start.10 = (bf16[16,256]{1,0:T(8,128)(2,1)S(1)}, bf16[16,256]{1,0:T(8,128)(2,1)}, u32[]{:S(2)}) copy-start(bf16[16,256]{1,0:T(8,128)(2,1)} %param.38) | copy-start | bytes 24580
  5.2 4.7 %copy-start.11 = (bf16[16,256]{1,0:T(8,128)(2,1)S(1)}, bf16[16,256]{1,0:T(8,128)(2,1)}, u32[]{:S(2)}) copy-start(bf16[16,256]{1,0:T(8,128)(2,1)} %param.39) | copy-start | bytes 24580
  5.2 4.9 %copy-start.12 = (bf16[256,16]{0,1:T(8,128)(2,1)S(1)}, bf16[256,16]{0,1:T(8,128)(2,1)}, u32[]{:S(2)}) copy-start(bf16[256,16]{0,1:T(8,128)(2,1)} %param.40) | copy-start | bytes 24580
  5.7 5.1 %copy-start.14 = (bf16[2048]{0:T(1024)(128)(2,1)S(1)}, bf16[2048]{0:T(1024)(128)(2,1)}, u32[]{:S(2)}) copy-start(bf16[2048]{0:T(1024)(128)(2,1)} %param.32) | copy-start | bytes 12292
  6.0 4.9 %collective-permute-start = (bf16[8,2048]{1,0:T(8,128)(2,1)S(1)}, bf16[8,2048]{1,0:T(8,128)(2,1)S(1)}, u32[]{:S(2)}, u32[]{:S(2)}) collective-permute-start(bf16[8,2048]{1,0:T(8,128)(2,1)S(1)} %convolution_convert_fusion.1), channel_id=1, source_target_pairs={{0,1},{1,0},{2,3},{3,2},{4,5},{5,4},{6,7},{7,6},{8,9},{9,8},{10,11... | collective-permute-start | bytes 98312 | tf_op jit(solution)/shard_map/ppermute | solution.py:21
  11.9 15.7 %all-to-all-start = ((bf16[8,8,1280]{2,1,0:T(8,128)(2,1)}), bf16[8,8,1280]{2,1,0:T(8,128)(2,1)S(1)}, u32[]{:S(2)}, u32[]{:S(2)}) async-start(bf16[8,8,1280]{2,1,0:T(8,128)(2,1)} %concatenate.20), calls=%async_computation | async-start | bytes 327680 | tf_op jit(solution)/shard_map/all_to_all | solution.py:30
  29.4 6.9 %copy-start.5 = (bf16[1,2048,128]{2,1,0:T(8,128)(2,1)S(1)}, bf16[1,2048,128]{2,1,0:T(8,128)(2,1)}, u32[]{:S(2)}) copy-start(bf16[1,2048,128]{2,1,0:T(8,128)(2,1)} %param.36) | copy-start | bytes 1572868
  29.4 6.9 %copy-start.6 = (bf16[1,2048,128]{2,1,0:T(8,128)(2,1)S(1)}, bf16[1,2048,128]{2,1,0:T(8,128)(2,1)}, u32[]{:S(2)}) copy-start(bf16[1,2048,128]{2,1,0:T(8,128)(2,1)} %param.35) | copy-start | bytes 1572868
  29.4 22.2 %all-to-all-start.1 = ((bf16[16,16,2048]{2,1,0:T(8,128)(2,1)}), bf16[16,16,2048]{2,1,0:T(8,128)(2,1)S(1)}, u32[]{:S(2)}, u32[]{:S(2)}) async-start(bf16[16,16,2048]{2,1,0:T(8,128)(2,1)} %pad_maximum_fusion), calls=%async_computation.1 | async-start | bytes 2097152 | tf_op jit(solution)/shard_map/all_to_all | solution.py:30
  37.2 2.0 %copy-start.15 = (bf16[2048]{0:T(1024)(128)(2,1)S(1)}, bf16[2048]{0:T(1024)(128)(2,1)}, u32[]{:S(2)}) copy-start(bf16[2048]{0:T(1024)(128)(2,1)} %param.41) | copy-start | bytes 12292
  37.2 2.0 %copy-start.4 = (bf16[1,128,2048]{2,1,0:T(8,128)(2,1)S(1)}, bf16[1,128,2048]{2,1,0:T(8,128)(2,1)}, u32[]{:S(2)}) copy-start(bf16[1,128,2048]{2,1,0:T(8,128)(2,1)} %param.37) | copy-start | bytes 1572868
  37.2 3.4 %collective-permute-start.1 = (bf16[1024,256]{1,0:T(8,128)(2,1)S(1)}, bf16[1024,256]{1,0:T(8,128)(2,1)S(1)}, u32[]{:S(2)}, u32[]{:S(2)}) collective-permute-start(bf16[1024,256]{1,0:T(8,128)(2,1)S(1)} %pad_maximum_fusion.1), channel_id=1, source_target_pairs={{0,1},{1,0},{2,3},{3,2},{4,5},{5,4},{6,7},{7,6},{8,9},{9,8},{10,11... | collective-permute-start | bytes 1572872 | tf_op jit(solution)/shard_map/ppermute | solution.py:21
  39.2 18.3 %collective-permute-start.3 = (bf16[128,1024]{1,0:T(8,128)(2,1)S(1)}, bf16[128,1024]{1,0:T(8,128)(2,1)}, u32[]{:S(2)}, u32[]{:S(2)}) collective-permute-start(bf16[128,1024]{1,0:T(8,128)(2,1)S(1)} %get-tuple-element.32), channel_id=1, source_target_pairs={{0,1},{1,0},{2,3},{3,2},{4,5},{5,4},{6,7},{7,6},{8,9},{9,8},{10,11... | collective-permute-start | bytes 786440 | tf_op jit(solution)/shard_map/ppermute | solution.py:21
  51.5 1.0 %copy-start.7 = (bf16[1024,128]{1,0:T(8,128)(2,1)S(1)}, bf16[1024,128]{1,0:T(8,128)(2,1)}, u32[]{:S(2)}) copy-start(bf16[1024,128]{1,0:T(8,128)(2,1)} %get-tuple-element.29) | copy-start | bytes 786436
  51.5 1.0 %copy-start.8 = (bf16[1024,128]{1,0:T(8,128)(2,1)S(1)}, bf16[1024,128]{1,0:T(8,128)(2,1)}, u32[]{:S(2)}) copy-start(bf16[1024,128]{1,0:T(8,128)(2,1)} %get-tuple-element.50) | copy-start | bytes 786436
  53.1 4.3 %collective-permute-start.2 = (bf16[256,512]{1,0:T(8,128)(2,1)S(1)}, bf16[256,512]{1,0:T(8,128)(2,1)S(1)}, u32[]{:S(2)}, u32[]{:S(2)}) collective-permute-start(bf16[256,512]{1,0:T(8,128)(2,1)S(1)} %pad_maximum_fusion.2), channel_id=1, source_target_pairs={{0,1},{1,0},{2,3},{3,2},{4,5},{5,4},{6,7},{7,6},{8,9},{9,8},{10,11... | collective-permute-start | bytes 786440 | tf_op jit(solution)/shard_map/ppermute | solution.py:21
  59.6 14.5 %all-to-all-start.2 = ((bf16[16,16,1024]{2,1,0:T(8,128)(2,1)}), bf16[16,16,1024]{2,1,0:T(8,128)(2,1)S(1)}, u32[]{:S(2)}, u32[]{:S(2)}) async-start(bf16[16,16,1024]{2,1,0:T(8,128)(2,1)} %bitcast.17), calls=%async_computation.2 | async-start | bytes 1048576 | tf_op jit(solution)/shard_map/all_to_all | solution.py:30
  63.2 1.5 %collective-permute-start.4 = (bf16[64,1024]{1,0:T(8,128)(2,1)S(1)}, bf16[64,1024]{1,0:T(8,128)(2,1)S(1)}, u32[]{:S(2)}, u32[]{:S(2)}) collective-permute-start(bf16[64,1024]{1,0:T(8,128)(2,1)S(1)} %slice.85), channel_id=1, source_target_pairs={{0,1},{1,0},{2,3},{3,2},{4,5},{5,4},{6,7},{7,6},{8,9},{9,8},{10,11... | collective-permute-start | bytes 393224 | tf_op jit(solution)/shard_map/ppermute | solution.py:21
  65.3 9.0 %collective-permute-start.5 = (bf16[64,1024]{1,0:T(8,128)(2,1)S(1)}, bf16[64,1024]{1,0:T(8,128)(2,1)S(1)}, u32[]{:S(2)}, u32[]{:S(2)}) collective-permute-start(bf16[64,1024]{1,0:T(8,128)(2,1)S(1)} %constant_dynamic-slice_fusion), channel_id=1, source_target_pairs={{0,1},{1,0},{2,3},{3,2},{4,5},{5,4},{6,7},{7,6},{8,9},{9,8},{10,11... | collective-permute-start | bytes 393224 | tf_op jit(solution)/shard_map/ppermute | solution.py:21

commit v4 on v3

v4 whole, which is shorter than its diff:
```python
import jax
import jax.numpy as jnp
from jax import lax
from jax.sharding import Mesh
from jax.sharding import PartitionSpec as P

from jax.experimental import pallas as pl
from jax.experimental.pallas import tpu as pltpu

DK = 128
TOPK = 6
EP = ("ep_0", "ep_1", "ep_2")
PLANE = ("ep_1", "ep_2")
CAP = 2


EPS = 1e-06


SWAP = [(0, 1), (1, 0)]


def swapped(array):
    return lax.ppermute(array, "tp", SWAP)


def half_of(array, index, dim):
    width = array.shape[dim] // 2
    return lax.dynamic_slice_in_dim(array, index * width, width, dim)


def exchanged(array, axis):
    return lax.all_to_all(array, axis, split_axis=0, concat_axis=0, tiled=True)


def rms_scale(values_in, gain):
    widened = values_in.astype(jnp.float32)
    return (
        widened
        * lax.rsqrt(jnp.mean(widened * widened, axis=-1, keepdims=True) + EPS)
        * gain.astype(jnp.float32)
    )


def dot(a, b, dims=((1,), (0,))):
    return lax.dot_general(a, b, (dims, ((), ())), preferred_element_type=jnp.float32)


FAR = pl.BlockSpec(memory_space=pl.ANY)
NEAR = pl.BlockSpec(memory_space=pltpu.VMEM)


def in_vmem(array):
    return pltpu.with_memory_space_constraint(array, pltpu.VMEM)


def placed_lanes(tile, lane, source, target, size):
    shift = (target - source) % 128
    turned = tile if shift == 0 else pltpu.roll(tile, shift, 1)
    return jnp.where((lane >= target) & (lane < target + size), turned, 0.0)


def attend(*refs):
    far, result, side, near, done = refs[:16], refs[16], refs[17], refs[18:34], refs[34]
    copies = [pltpu.make_async_copy(far[k], near[k], done.at[k]) for k in range(16)]
    for copy in copies:
        copy.start()
    (
        tokens, gain, query_weight, decay_down, key_weight, decay_up, decay_bias, value_weight,
        ids, weights, dense_gate, dense_up, dense_down, state, head_gain, out_weight,
    ) = near
    count = tokens.shape[0]
    copies[0].wait()
    copies[1].wait()
    normed = rms_scale(tokens[...], gain[...][None, :]).astype(jnp.bfloat16)
    copies[2].wait()
    query = dot(normed, query_weight[...]) * DK ** (-0.5)
    copies[3].wait()
    decay_low = dot(normed, decay_down[...], ((1,), (1,))).astype(jnp.bfloat16)
    copies[4].wait()
    keys = dot(normed, key_weight[...])
    copies[5].wait()
    copies[6].wait()
    decay_pre = dot(decay_low, decay_up[...]) + decay_bias[...][None, :]
    log_decay = jnp.minimum(decay_pre, 0.0) - jnp.log1p(jnp.exp(-jnp.abs(decay_pre)))
    columns = jnp.transpose(query * jnp.exp(log_decay / 16.0))
    copies[7].wait()
    values = dot(normed, value_weight[...])

    for k in range(8, 13):
        copies[k].wait()
    lane = lax.broadcasted_iota(jnp.int32, (8, 128), 1)
    line = lax.broadcasted_iota(jnp.int32, (8, 128), 0)
    shares = weights[...] / jnp.sum(weights[...], axis=1, keepdims=True)
    chosen = jnp.zeros((8, 128), jnp.float32)
    share = jnp.zeros((8, 128), jnp.float32)
    for k in range(TOPK):
        named = ids[:, k : k + 1] == lane
        chosen = chosen + jnp.where(named, 1.0, 0.0)
        share = share + jnp.where(named, shares[:, k : k + 1], 0.0)
    place = jnp.where(chosen > 0.0, 1.0, 0.0)
    for k in range(1, count):
        place = place + jnp.where(line >= k, pltpu.roll(chosen, k, 0), 0.0)
    place = place * chosen
    share_high = share.astype(jnp.bfloat16).astype(jnp.float32)
    share_low = share - share_high
    for z in range(8):
        tiles = []
        for part in range(2):
            tile = jnp.zeros((8, 128), jnp.float32)
            for m, matrix in enumerate((dense_gate, dense_up, dense_down)):
                start = 128 * (z // 4)
                piece = matrix[...].astype(jnp.float32)[8 * part : 8 * part + 8, start : start + 128]
                tile = tile + placed_lanes(piece, lane, 32 * (z % 4), 32 * m, 32)
            tiles.append(tile)
        tiles[0] = tiles[0] + placed_lanes(place, lane, 16 * z, 96, 16)
        tiles[0] = tiles[0] + placed_lanes(share_high, lane, 16 * z, 112, 16)
        tiles[1] = tiles[1] + placed_lanes(share_low, lane, 16 * z, 96, 16)
        side[z] = jnp.concatenate(tiles, axis=1).astype(jnp.bfloat16)

    copies[13].wait()
    read = [
        jnp.sum(columns[:, k : k + 1] * state[k], axis=0, keepdims=True) for k in range(count)
    ]
    head = jnp.concatenate(read, axis=0) + jnp.sum(query * keys, axis=1, keepdims=True) * values
    copies[14].wait()
    head = rms_scale(head, head_gain[...][None, :]).astype(jnp.bfloat16)
    copies[15].wait()
    result[...] = dot(head, out_weight[...]).astype(jnp.bfloat16)


def attended(*held):
    tokens = held[0]
    return pl.pallas_call(
        attend,
        out_shape=(
            pltpu.VMEM(tokens.shape, jnp.bfloat16),
            pltpu.VMEM((8, 8, 256), jnp.bfloat16),
        ),
        in_specs=[FAR] * 16,
        out_specs=(NEAR, NEAR),
        scratch_shapes=[pltpu.VMEM(a.shape, a.dtype) for a in held]
        + [pltpu.SemaphoreType.DMA((16,))],
        name="attend",
    )(*held)


def assemble(core, tokens, mine, theirs, gain, side, first, own, block, done):
    sides = pltpu.make_async_copy(side, first.at[:, :, pl.ds(1024, 256)], done.at[8])
    sides.start()
    both = mine[...].astype(jnp.float32) + theirs[...].astype(jnp.float32)
    residual = (tokens[...].astype(jnp.float32) + both).astype(jnp.bfloat16)
    normed = rms_scale(residual, gain[...][None, :])
    half = normed.shape[1] // 2
    first_half = core[0] == 0
    block[...] = jnp.where(first_half, normed[:, :half], normed[:, half:]).astype(jnp.bfloat16)
    copies = [
        pltpu.make_async_copy(block, first.at[z, :, pl.ds(0, 1024)], done.at[z]) for z in range(8)
    ]
    for copy in copies:
        copy.start()
    wide = residual.astype(jnp.float32)
    own[...] = jnp.where(first_half, wide[:, :half], wide[:, half:])
    for copy in copies:
        copy.wait()
    sides.wait()


def assembled(core, tokens, mine, theirs, gain, side):
    rows, width = tokens.shape
    return pl.pallas_call(
        assemble,
        out_shape=(
            jax.ShapeDtypeStruct((8, rows, width // 2 + 256), jnp.bfloat16),
            pltpu.VMEM((rows, width // 2), jnp.float32),
        ),
        in_specs=[pl.BlockSpec(memory_space=pltpu.SMEM)] + [NEAR] * 5,
        out_specs=(FAR, NEAR),
        scratch_shapes=[
            pltpu.VMEM((rows, width // 2), jnp.bfloat16),
            pltpu.SemaphoreType.DMA((9,)),
        ],
        name="assemble",
    )(
        core.reshape(1).astype(jnp.int32), in_vmem(tokens), in_vmem(mine), in_vmem(theirs),
        in_vmem(gain), in_vmem(side),
    )


def route(line, second, rows, weights, done):
    planes, depth, _ = second.shape
    half = line.shape[1] - 256
    tiles = [
        line[:, half + 128 * k : half + 128 * (k + 1)].astype(jnp.float32) for k in range(2)
    ]
    lane = lax.broadcasted_iota(jnp.int32, (8, 128), 1)
    for which in range(3):
        for parity in range(2):
            parts = []
            for tile in tiles:
                part = jnp.zeros((8, 128), jnp.float32)
                for quarter in range(4):
                    z = 2 * quarter + parity
                    part = part + placed_lanes(
                        tile[8 * z : 8 * z + 8], lane, 32 * which, 32 * quarter, 32
                    )
                parts.append(part)
            start = 256 * which + 128 * parity
            weights[:, start : start + 128] = jnp.concatenate(parts, axis=0).astype(jnp.bfloat16)
    copies = [
        pltpu.make_async_copy(weights, second.at[k, :, pl.ds(1024, 768)], done.at[k])
        for k in range(planes)
    ]
    for copy in copies:
        copy.start()
    marks = line[:, half : half + 128]
    group = planes // 4
    count = group * depth
    for step in range(4):
        row = lax.broadcasted_iota(jnp.int32, (count, 128), 0) + step * count
        lane = lax.broadcasted_iota(jnp.int32, (count, 128), 1)
        spread = jnp.where(lane == 96 + row // depth, 1.0, 0.0).astype(jnp.bfloat16)
        place = dot(spread, marks, ((1,), (1,)))
        row, lane = row[:, : line.shape[0]], lane[:, : line.shape[0]]
        taken = (place == (1 + row % CAP).astype(jnp.float32)) & (row // CAP % 8 == lane // 8)
        taken = jnp.where(taken, 1.0, 0.0).astype(jnp.bfloat16)
        rows[pl.ds(step * group, group)] = (
            dot(taken, line[:, :half]).astype(jnp.bfloat16).reshape(group, depth, half)
        )
        copy = pltpu.make_async_copy(
            rows.at[pl.ds(step * group, group)],
            second.at[pl.ds(step * group, group), :, pl.ds(0, 1024)],
            done.at[planes + step],
        )
        copy.start()
        copies.append(copy)
    for copy in copies:
        copy.wait()


def routed_rows(line, planes):
    half = line.shape[1] - 256
    return pl.pallas_call(
        route,
        out_shape=jax.ShapeDtypeStruct((planes, 16, half + 768), jnp.bfloat16),
        in_specs=[NEAR],
        out_specs=FAR,
        scratch_shapes=[
            pltpu.VMEM((planes, 16, half), jnp.bfloat16),
            pltpu.VMEM((16, 768), jnp.bfloat16),
            pltpu.SemaphoreType.DMA((planes + 4,)),
        ],
        name="route",
    )(in_vmem(line))


def shards(
    tokens,
    first_gain,
    query_weight,
    key_weight,
    value_weight,
    decay_down,
    decay_up,
    decay_bias,
    head_gain,
    recurrent_state,
    out_weight,
    second_gain,
    expert_ids,
    route_weights,
    expert_gate,
    expert_up,
    expert_down,
    dense_gate,
    dense_up,
    dense_down,
    branch_gate,
):
    rows_dev, width = tokens.shape
    core = lax.axis_index("tp")
    lines = lax.axis_size("ep_0")
    plane = lax.axis_size(PLANE)
    half = width // 2
    rows_own, hidden = dense_gate.shape
    units = hidden // lines
    partial_value, side = attended(
        tokens, first_gain, query_weight, decay_down.T, key_weight, decay_up, decay_bias,
        value_weight, expert_ids, route_weights, dense_gate, dense_up, dense_down.T,
        recurrent_state[:, 0], head_gain, out_weight,
    )
    first, own_half = assembled(
        core, tokens, partial_value, swapped(partial_value), second_gain, side
    )
    first, gate, up, down = lax.optimization_barrier(
        (first, expert_gate[0], expert_up[0], expert_down[0])
    )
    line = exchanged(first, "ep_0")
    line = line.reshape(lines * rows_dev, half + 256)
    given = jnp.concatenate([half_of(gate, 1 - core, 0), half_of(up, 1 - core, 0)], axis=1)
    taken_in = swapped(given)
    taken_down = swapped(half_of(down, 1 - core, 1))
    inner = gate.shape[1]
    weights_in = jnp.concatenate(
        [half_of(gate, core, 0), taken_in[:, :inner], half_of(up, core, 0), taken_in[:, inner:]],
        axis=1,
    )
    weights_down = jnp.concatenate([half_of(down, core, 1), taken_down], axis=0)
    arrived = exchanged(routed_rows(line, plane), PLANE)
    slots = plane * lines * CAP
    mine = arrived[:, :, :half].reshape(slots, half)
    partial_in = jnp.dot(mine, weights_in, preferred_element_type=jnp.float32)
    blocks = [partial_in[:, k * inner : (k + 1) * inner] for k in (1, 0, 3, 2)]
    pre = partial_in + swapped(
        jnp.concatenate(blocks, axis=1).astype(jnp.bfloat16)
    ).astype(jnp.float32)
    activated = (jax.nn.silu(pre[:, : 2 * inner]) * pre[:, 2 * inner :]).astype(jnp.bfloat16)
    summed = jnp.dot(activated, weights_down, preferred_element_type=jnp.float32).astype(
        jnp.bfloat16
    )
    summed, arrived, line = lax.optimization_barrier((summed, arrived, line))
    came_back = exchanged(summed.reshape(plane, lines * CAP, half), PLANE)
    line_in = line[:, :half]
    line_rest = swapped(line_in)
    pre_gate = jnp.dot(
        line_in, half_of(branch_gate, core, 0), preferred_element_type=jnp.float32
    ) + jnp.dot(line_rest, half_of(branch_gate, 1 - core, 0), preferred_element_type=jnp.float32)
    branch = jax.nn.sigmoid(pre_gate)
    matrices = [
        jnp.concatenate(
            [
                arrived[:, :, half + 256 * m + 128 * p : half + 256 * m + 128 * (p + 1)].reshape(
                    plane * rows_own, 128
                )
                for p in range(2)
            ],
            axis=0,
        )
        for m in range(3)
    ]
    quarter = width // 4
    group = jnp.arange(128, dtype=jnp.int32)[None, :] // units
    low = jnp.where(core == 0, line_in, line_rest)
    high = jnp.where(core == 0, line_rest, line_in)

    def through(matrix):
        total = jnp.zeros((lines * rows_dev, 128), jnp.float32)
        for q in range(4):
            part = (low, high)[q // 2][:, q % 2 * quarter : (q % 2 + 1) * quarter]
            total = total + jnp.where(
                group == q, jnp.dot(part, matrix, preferred_element_type=jnp.float32), 0.0
            )
        return sum(jnp.roll(total, units * q, axis=1) for q in range(4))

    line_hidden = (jax.nn.silu(through(matrices[0])) * through(matrices[1])).astype(jnp.bfloat16)
    line_part = jnp.concatenate(
        [dot(jnp.where(group == q, line_hidden, 0), matrices[2], ((1,), (1,))) for q in range(4)],
        axis=1,
    ).astype(jnp.bfloat16)
    dense = branch[:, None] * (
        half_of(line_part, core, 1).astype(jnp.float32)
        + swapped(half_of(line_part, 1 - core, 1)).astype(jnp.float32)
    )
    row = lax.broadcasted_iota(jnp.int32, (slots, lines * rows_dev), 0)
    col = lax.broadcasted_iota(jnp.int32, (slots, lines * rows_dev), 1)
    spread = (
        lax.broadcasted_iota(jnp.int32, (slots, plane), 0) // (lines * CAP)
        == lax.broadcasted_iota(jnp.int32, (slots, plane), 1)
    ).astype(jnp.bfloat16)

    def over_slots(start):
        return dot(spread, line[:, half + start : half + start + plane], ((1,), (1,)))

    taken = (over_slots(96) == (1 + row % CAP).astype(jnp.float32)) & (
        row // CAP % lines == col // rows_dev
    )
    weighing = jnp.where(taken, over_slots(112) + over_slots(224), 0.0)
    weigh_high = weighing.astype(jnp.bfloat16)
    weigh_low = (weighing - weigh_high.astype(jnp.float32)).astype(jnp.bfloat16)

    def combined(part):
        return lax.dot_general(
            part,
            came_back.reshape(slots, half),
            (((0,), (0,)), ((), ())),
            preferred_element_type=jnp.float32,
        )

    third = (combined(weigh_high) + combined(weigh_low) + dense).astype(jnp.bfloat16)
    parts = exchanged(third.reshape(lines, rows_dev, half), "ep_0")
    return (own_half + parts.astype(jnp.float32).sum(axis=0)).astype(jnp.bfloat16)


def solution(mesh):
    split = Mesh(mesh.devices.reshape(8, 4, 4, mesh.shape["tp"]), ("ep_0", "ep_1", "ep_2", "tp"))
    placed = (
        P(EP, None),
        P(),
        P(None, "tp"),
        P(None, "tp"),
        P(None, "tp"),
        P(),
        P(None, "tp"),
        P("tp"),
        P(),
        P(EP, "tp", None, None),
        P("tp", None),
        P(),
        P(EP, None),
        P(EP, None),
        P(EP, None, "tp"),
        P(EP, None, "tp"),
        P(EP, "tp", None),
        P(EP, "tp"),
        P(EP, "tp"),
        P("tp", EP),
        P(),
    )
    return jax.shard_map(
        shards, mesh=split, in_specs=placed, out_specs=P(EP, "tp"), check_vma=False
    )
```

time: 86.4 us -> 79.9 us (0.925)
  Pallas kernels: 0 us -> 5.97 us
  matrix products: 8.91 us -> 5.12 us
  other arithmetic: 4.75 us -> 1.05 us
  local copies, waits for them, and re-layouts: 3.9 us -> 0.86 us
  waiting for transfers between devices: 29.9 us -> 27.8 us
    pallas_call x0 -> x3, Pallas kernels: none -> 5.97 us  [the longest x1 3.49 us: attended(): pl.pallas_call(attend, out_shape=(pltpu.VMEM(tokens.shape, jnp.bfloat16),...]
    all_to_all x3, waiting for transfers between devices: 28.2 us -> 24.4 us  [exchanged(): return lax.all_to_all(array, axis, split_axis=0, concat_axis=0, tiled=True)]
    dot_general x12 -> x15, matrix products: 5.71 us -> 2.88 us  [the longest x7 1.59 us: dot(): lax.dot_general(a, b, (dims, ((), ())), preferred_element_type=jnp.float32)]
    ppermute x6, waiting for transfers between devices: 1.68 us -> 3.39 us  [swapped(): return lax.ppermute(array, 'tp', SWAP)]
    reduce_sum x5 -> x0, other arithmetic: 1.44 us -> none  [the longest x2 1.02 us: rms_scale(): jnp.mean(widened * widened, axis=-1, keepdims=True) + EPS]
    unnamed x41 -> x12, local copies, waits for them, and re-layouts: 1.1 us -> 0.03 us
    concatenate x1, other arithmetic: 1.07 us -> 0.02 us  [shards(): jnp.concatenate([dot(jnp.where(group == q, line_hidden, 0), matrices[2],...]
    dot_general x1, matrix products: 2.07 us -> 1.11 us  [shards(): jnp.dot(activated, weights_down, preferred_element_type=jnp.float32)]
  transfers between devices with their start and end apart: 9 -> 9, of which waited for: 6 -> 7; matrix products, arithmetic and copies ran while one was open for 6% -> 6% of each run, Pallas kernels for 0% -> 0%
where the time goes in v4:
time: 79.9 us; the launch traced here: 78.9 us
  waiting for transfers between devices  27.8 us (35%)
  starting transfers between devices  27.5 us (34%)
  blocking collectives  10.3 us (13%)
  Pallas kernels  5.97 us (7%)
  matrix products  5.12 us (6%)
  other arithmetic  1.05 us (1%)
  local copies, waits for them, and re-layouts  0.86 us (1%)
    all_to_all x3, waiting for transfers between devices, exchanged(): return lax.all_to_all(array, axis, split_axis=0, concat_axis=0, tiled=True)  24.4 us
    all_to_all x3, starting transfers between devices, exchanged(): return lax.all_to_all(array, axis, split_axis=0, concat_axis=0, tiled=True)  16.8 us
    ppermute x6, starting transfers between devices, swapped(): return lax.ppermute(array, 'tp', SWAP)  10.7 us
    all_to_all x1, blocking collectives, exchanged(): return lax.all_to_all(array, axis, split_axis=0, concat_axis=0, tiled=True)  10.3 us
    pallas_call x1, Pallas kernels, attended(): pl.pallas_call(attend, out_shape=(pltpu.VMEM(tokens.shape, jnp.bfloat16),...  3.49 us
    ppermute x6, waiting for transfers between devices, swapped(): return lax.ppermute(array, 'tp', SWAP)  3.39 us
    pallas_call x1, Pallas kernels, routed_rows(): pl.pallas_call(route, out_shape=jax.ShapeDtypeStruct((planes, 16, half +...  1.63 us
  transfers between devices with their start and end apart: 9, of which 7 were waited for; matrix products, arithmetic and copies ran while one was open for 6% of the time, Pallas kernels for 0%

profile of v4, /device:TPU:1, one launch (start us, length us, event | category | flops | bytes accessed | tf_op | source)
XLA Modules:
  0.0 78.9 jit_solution(8171911053862586762)
XLA Ops:
  0.0 0.0 copy-start.4
  0.0 3.5 %attend.1 = (bf16[8,2048]{1,0:T(8,128)(2,1)S(1)}, bf16[8,8,256]{2,1,0:T(8,128)(2,1)S(1)}) custom-call(bf16[8,2048]{1,0:T(8,128)(2,1)} %tokens.1, bf16[2048]{0:T(1024)(128)(2,1)} %refs_1_.1, bf16[2048,128]{1,0:T(8,128)(2,1)} %refs_2_.1, bf16[16,2048]{1,0:T(8,128)(2,1)} %bitcast.69, bf16[2048,128]{1,0:T(8,128)(2,1)} %refs_4_.1, bf16[16,128]{1,0:T(8,128)(2,1)} %refs_5_.1, ...), custom_call_target="tpu_custom_call" | custom-call | tf_op jit(solution)/shard_map/attend/pallas_call | solution.py:134
  3.5 3.3 %collective-permute-start = (bf16[8,2048]{1,0:T(8,128)(2,1)S(1)}, bf16[8,2048]{1,0:T(8,128)(2,1)S(1)}, u32[]{:S(2)}, u32[]{:S(2)}) collective-permute-start(bf16[8,2048]{1,0:T(8,128)(2,1)S(1)} %get-tuple-element.16.mine), channel_id=1, source_target_pairs={{0,1},{1,0},{2,3},{3,2},{4,5},{5,4},{6,7},{7,6},{8,9},{9,8},{10,11... | collective-permute-start | bytes 98312 | tf_op jit(solution)/shard_map/ppermute | solution.py:24
  6.8 0.9 %collective-permute-done.theirs = bf16[8,2048]{1,0:T(8,128)(2,1)S(1)} collective-permute-done((bf16[8,2048]{1,0:T(8,128)(2,1)S(1)}, bf16[8,2048]{1,0:T(8,128)(2,1)S(1)}, u32[]{:S(2)}, u32[]{:S(2)}) %collective-permute-start) | collective-permute-done | bytes 32800 | tf_op jit(solution)/shard_map/ppermute | solution.py:24
  7.7 0.0 copy-done
  7.7 0.0 copy-done.1
  7.7 0.8 %assemble.1 = (bf16[8,8,1280]{2,1,0:T(8,128)(2,1)}, f32[8,1024]{1,0:T(8,128)S(1)}) custom-call(s32[1]{0:T(128)} %bitcast.core, bf16[8,2048]{1,0:T(8,128)(2,1)S(1)} %copy-done, bf16[8,2048]{1,0:T(8,128)(2,1)S(1)} %get-tuple-element.16.mine, bf16[8,2048]{1,0:T(8,128)(2,1)S(1)} %collective-permute-done.theirs, bf16[2048]{0:T(1024)(128)(2,1)S(1)} %copy-done.1, ...), custom_call_target="tpu_custom_call" | custom-call | tf_op jit(solution)/shard_map/assemble/pallas_call | solution.py:171
  8.5 6.5 %all-to-all-start = ((bf16[8,8,1280]{2,1,0:T(8,128)(2,1)}), bf16[8,8,1280]{2,1,0:T(8,128)(2,1)S(1)}, u32[]{:S(2)}, u32[]{:S(2)}) async-start(bf16[8,8,1280]{2,1,0:T(8,128)(2,1)} %get-tuple-element.20), calls=%async_computation | async-start | bytes 327680 | tf_op jit(solution)/shard_map/all_to_all | solution.py:33
  15.0 0.0 copy-done.3
  15.1 0.0 copy-done.4
  15.1 0.1 constant_dynamic-slice_fusion.3
  15.2 8.5 %all-to-all-done = bf16[8,8,1280]{2,1,0:T(8,128)(2,1)S(1)} async-done(((bf16[8,8,1280]{2,1,0:T(8,128)(2,1)}), bf16[8,8,1280]{2,1,0:T(8,128)(2,1)S(1)}, u32[]{:S(2)}, u32[]{:S(2)}) %all-to-all-start) | async-done | bytes 163872 | tf_op jit(solution)/shard_map/all_to_all | solution.py:33
  23.7 1.6 %route.1 = bf16[16,16,1792]{2,1,0:T(8,128)(2,1)} custom-call(bf16[64,1280]{1,0:T(8,128)(2,1)S(1)} %bitcast.39), custom_call_target="tpu_custom_call" | custom-call | tf_op jit(solution)/shard_map/route/pallas_call | solution.py:243
  25.3 0.0 copy-start.5
  25.4 6.8 %all-to-all-start.1 = ((bf16[16,16,1792]{2,1,0:T(8,128)(2,1)}), bf16[16,16,1792]{2,1,0:T(8,128)(2,1)S(1)}, u32[]{:S(2)}, u32[]{:S(2)}) async-start(bf16[16,16,1792]{2,1,0:T(8,128)(2,1)} %route.1), calls=%async_computation.1 | async-start | bytes 1835008 | tf_op jit(solution)/shard_map/all_to_all | solution.py:33
  32.1 0.1 pad_maximum_fusion
  32.2 2.4 %collective-permute-start.1 = (bf16[1024,256]{1,0:T(8,128)(2,1)S(1)}, bf16[1024,256]{1,0:T(8,128)(2,1)S(1)}, u32[]{:S(2)}, u32[]{:S(2)}) collective-permute-start(bf16[1024,256]{1,0:T(8,128)(2,1)S(1)} %pad_maximum_fusion), channel_id=1, source_target_pairs={{0,1},{1,0},{2,3},{3,2},{4,5},{5,4},{6,7},{7,6},{8,9},{9,8},{10,11... | collective-permute-start | bytes 1572872 | tf_op jit(solution)/shard_map/ppermute | solution.py:24
  34.6 0.0 copy-done.5
  34.7 1.5 %collective-permute-done.1 = bf16[1024,256]{1,0:T(8,128)(2,1)S(1)} collective-permute-done((bf16[1024,256]{1,0:T(8,128)(2,1)S(1)}, bf16[1024,256]{1,0:T(8,128)(2,1)S(1)}, u32[]{:S(2)}, u32[]{:S(2)}) %collective-permute-start.1) | collective-permute-done | bytes 524320 | tf_op jit(solution)/shard_map/ppermute | solution.py:24
  36.2 9.6 %all-to-all-done.1 = bf16[16,16,1792]{2,1,0:T(8,128)(2,1)S(1)} async-done(((bf16[16,16,1792]{2,1,0:T(8,128)(2,1)}), bf16[16,16,1792]{2,1,0:T(8,128)(2,1)S(1)}, u32[]{:S(2)}, u32[]{:S(2)}) %all-to-all-start.1) | async-done | bytes 917536 | tf_op jit(solution)/shard_map/all_to_all | solution.py:33
  45.8 0.1 slice.154
  45.9 0.4 fusion.94
  46.3 0.0 copy-start.2
  46.4 3.3 %collective-permute-start.2 = (bf16[256,512]{1,0:T(8,128)(2,1)S(1)}, bf16[256,512]{1,0:T(8,128)(2,1)S(1)}, u32[]{:S(2)}, u32[]{:S(2)}) collective-permute-start(bf16[256,512]{1,0:T(8,128)(2,1)S(1)} %pad_maximum_fusion.1), channel_id=1, source_target_pairs={{0,1},{1,0},{2,3},{3,2},{4,5},{5,4},{6,7},{7,6},{8,9},{9,8},{10,11... | collective-permute-start | bytes 786440 | tf_op jit(solution)/shard_map/ppermute | solution.py:24
  49.8 0.9 %collective-permute-start.3 = (bf16[128,1024]{1,0:T(8,128)(2,1)S(1)}, bf16[128,1024]{1,0:T(8,128)(2,1)S(1)}, u32[]{:S(2)}, u32[]{:S(2)}) collective-permute-start(bf16[128,1024]{1,0:T(8,128)(2,1)S(1)} %get-tuple-element.40), channel_id=1, source_target_pairs={{0,1},{1,0},{2,3},{3,2},{4,5},{5,4},{6,7},{7,6},{8,9},{9,8},{10,11... | collective-permute-start | bytes 786440 | tf_op jit(solution)/shard_map/ppermute | solution.py:24
  50.8 0.2 collective-permute-done.2
  50.9 0.1 convert_add_fusion
  51.0 0.9 %collective-permute-done.3 = bf16[128,1024]{1,0:T(8,128)(2,1)S(1)} collective-permute-done((bf16[128,1024]{1,0:T(8,128)(2,1)S(1)}, bf16[128,1024]{1,0:T(8,128)(2,1)S(1)}, u32[]{:S(2)}, u32[]{:S(2)}) %collective-permute-start.3) | collective-permute-done | bytes 262176 | tf_op jit(solution)/shard_map/ppermute | solution.py:24
  51.9 1.1 %convolution_convert_fusion = bf16[256,1024]{1,0:T(8,128)(2,1)} fusion(bf16[128,1024]{1,0:T(8,128)(2,1)S(1)} %collective-permute-done.3, bf16[128,1024]{1,0:T(8,128)(2,1)S(1)} %get-tuple-element.39, f32[256,512]{1,0:T(8,128)S(1)} %convert_add_fusion), kind=kOutput, calls=%fused_computation | convolution fusion | flops 135921664 | bytes 1572864 | tf_op jit(solution)/shard_map/dot_general | solution.py:318
  53.0 3.6 %all-to-all-start.2 = ((bf16[16,16,1024]{2,1,0:T(8,128)(2,1)}), bf16[16,16,1024]{2,1,0:T(8,128)(2,1)S(1)}, u32[]{:S(2)}, u32[]{:S(2)}) async-start(bf16[16,16,1024]{2,1,0:T(8,128)(2,1)} %bitcast.9), calls=%async_computation.2 | async-start | bytes 1048576 | tf_op jit(solution)/shard_map/all_to_all | solution.py:33
  56.6 0.5 collective-permute-start.4
  57.1 0.1 fusion.84
  57.1 0.3 fusion.28
  57.4 0.3 fusion.7
  57.7 0.3 fusion
  58.0 0.1 convolution_bitcast_fusion.1
  58.2 0.0 collective-permute-done.4
  58.2 0.2 convolution_select_fusion.5
  58.4 0.2 convolution_select_fusion.4
  58.5 0.2 convolution_select_fusion.6
  58.7 0.2 fusion.6
  58.9 0.1 fusion.87
  58.9 0.1 fusion.88
  59.0 0.1 fusion.89
  59.1 0.2 convolution_select_fusion.2
  59.3 0.2 convolution_select_fusion.1
  59.4 0.2 convolution_select_fusion
  59.6 0.2 fusion.3
  59.7 0.1 fusion.90
  59.8 0.1 fusion.91
  59.9 0.1 fusion.92
  60.0 0.1 fusion.53
  60.1 0.2 convolution_convert_fusion.4
  60.3 0.2 convolution_convert_fusion.3
  60.5 0.2 convolution_convert_fusion.2
  60.6 0.2 convolution_convert_fusion.1
  60.9 0.3 collective-permute-start.5
  61.2 0.1 fusion.12
  61.3 6.2 %all-to-all-done.2 = bf16[16,16,1024]{2,1,0:T(8,128)(2,1)S(1)} async-done(((bf16[16,16,1024]{2,1,0:T(8,128)(2,1)}), bf16[16,16,1024]{2,1,0:T(8,128)(2,1)S(1)}, u32[]{:S(2)}, u32[]{:S(2)}) %all-to-all-start.2) | async-done | bytes 524320 | tf_op jit(solution)/shard_map/all_to_all | solution.py:33
  67.5 0.2 fusion.59
  67.7 0.0 collective-permute-done.5
  67.7 0.2 fusion.25
  68.0 10.3 %all_to_all.20 = bf16[8,8,1024]{2,1,0:T(8,128)(2,1)S(1)} all-to-all(bf16[8,8,1024]{2,1,0:T(8,128)(2,1)S(1)} %fusion.25), channel_id=1, replica_groups=mesh['ep_0'=8,'ep_1'=4,'ep_2'=4,'tp'=2] {'ep_0'}, dimensions={0} | all-to-all | bytes 262144 | tf_op jit(solution)/shard_map/all_to_all | solution.py:33
  78.3 0.6 add_convert_fusion.1
  (26 shorter events, 0.4 us)
Async XLA Ops:
  0.0 7.7 %copy-start = (bf16[8,2048]{1,0:T(8,128)(2,1)S(1)}, bf16[8,2048]{1,0:T(8,128)(2,1)}, u32[]{:S(2)}) copy-start(bf16[8,2048]{1,0:T(8,128)(2,1)} %tokens.1) | copy-start | bytes 98308
  0.0 7.7 %copy-start.1 = (bf16[2048]{0:T(1024)(128)(2,1)S(1)}, bf16[2048]{0:T(1024)(128)(2,1)}, u32[]{:S(2)}) copy-start(bf16[2048]{0:T(1024)(128)(2,1)} %gain.1) | copy-start | bytes 12292
  0.0 15.0 %copy-start.3 = (bf16[1,2048,128]{2,1,0:T(8,128)(2,1)S(1)}, bf16[1,2048,128]{2,1,0:T(8,128)(2,1)}, u32[]{:S(2)}) copy-start(bf16[1,2048,128]{2,1,0:T(8,128)(2,1)} %param.36) | copy-start | bytes 1572868
  0.0 15.0 %copy-start.4 = (bf16[1,2048,128]{2,1,0:T(8,128)(2,1)S(1)}, bf16[1,2048,128]{2,1,0:T(8,128)(2,1)}, u32[]{:S(2)}) copy-start(bf16[1,2048,128]{2,1,0:T(8,128)(2,1)} %param.35) | copy-start | bytes 1572868
  3.5 4.1 %collective-permute-start = (bf16[8,2048]{1,0:T(8,128)(2,1)S(1)}, bf16[8,2048]{1,0:T(8,128)(2,1)S(1)}, u32[]{:S(2)}, u32[]{:S(2)}) collective-permute-start(bf16[8,2048]{1,0:T(8,128)(2,1)S(1)} %get-tuple-element.16.mine), channel_id=1, source_target_pairs={{0,1},{1,0},{2,3},{3,2},{4,5},{5,4},{6,7},{7,6},{8,9},{9,8},{10,11... | collective-permute-start | bytes 98312 | tf_op jit(solution)/shard_map/ppermute | solution.py:24
  8.5 15.2 %all-to-all-start = ((bf16[8,8,1280]{2,1,0:T(8,128)(2,1)}), bf16[8,8,1280]{2,1,0:T(8,128)(2,1)S(1)}, u32[]{:S(2)}, u32[]{:S(2)}) async-start(bf16[8,8,1280]{2,1,0:T(8,128)(2,1)} %get-tuple-element.20), calls=%async_computation | async-start | bytes 327680 | tf_op jit(solution)/shard_map/all_to_all | solution.py:33
  25.3 9.3 %copy-start.5 = (bf16[2048]{0:T(1024)(128)(2,1)S(1)}, bf16[2048]{0:T(1024)(128)(2,1)}, u32[]{:S(2)}) copy-start(bf16[2048]{0:T(1024)(128)(2,1)} %param.41) | copy-start | bytes 12292
  25.4 20.5 %all-to-all-start.1 = ((bf16[16,16,1792]{2,1,0:T(8,128)(2,1)}), bf16[16,16,1792]{2,1,0:T(8,128)(2,1)S(1)}, u32[]{:S(2)}, u32[]{:S(2)}) async-start(bf16[16,16,1792]{2,1,0:T(8,128)(2,1)} %route.1), calls=%async_computation.1 | async-start | bytes 1835008 | tf_op jit(solution)/shard_map/all_to_all | solution.py:33
  32.2 4.0 %collective-permute-start.1 = (bf16[1024,256]{1,0:T(8,128)(2,1)S(1)}, bf16[1024,256]{1,0:T(8,128)(2,1)S(1)}, u32[]{:S(2)}, u32[]{:S(2)}) collective-permute-start(bf16[1024,256]{1,0:T(8,128)(2,1)S(1)} %pad_maximum_fusion), channel_id=1, source_target_pairs={{0,1},{1,0},{2,3},{3,2},{4,5},{5,4},{6,7},{7,6},{8,9},{9,8},{10,11... | collective-permute-start | bytes 1572872 | tf_op jit(solution)/shard_map/ppermute | solution.py:24
  46.3 3.4 %copy-start.2 = (bf16[1,128,2048]{2,1,0:T(8,128)(2,1)S(1)}, bf16[1,128,2048]{2,1,0:T(8,128)(2,1)}, u32[]{:S(2)}) copy-start(bf16[1,128,2048]{2,1,0:T(8,128)(2,1)} %param.37) | copy-start | bytes 1572868
  46.4 4.5 %collective-permute-start.2 = (bf16[256,512]{1,0:T(8,128)(2,1)S(1)}, bf16[256,512]{1,0:T(8,128)(2,1)S(1)}, u32[]{:S(2)}, u32[]{:S(2)}) collective-permute-start(bf16[256,512]{1,0:T(8,128)(2,1)S(1)} %pad_maximum_fusion.1), channel_id=1, source_target_pairs={{0,1},{1,0},{2,3},{3,2},{4,5},{5,4},{6,7},{7,6},{8,9},{9,8},{10,11... | collective-permute-start | bytes 786440 | tf_op jit(solution)/shard_map/ppermute | solution.py:24
  49.8 2.1 %collective-permute-start.3 = (bf16[128,1024]{1,0:T(8,128)(2,1)S(1)}, bf16[128,1024]{1,0:T(8,128)(2,1)S(1)}, u32[]{:S(2)}, u32[]{:S(2)}) collective-permute-start(bf16[128,1024]{1,0:T(8,128)(2,1)S(1)} %get-tuple-element.40), channel_id=1, source_target_pairs={{0,1},{1,0},{2,3},{3,2},{4,5},{5,4},{6,7},{7,6},{8,9},{9,8},{10,11... | collective-permute-start | bytes 786440 | tf_op jit(solution)/shard_map/ppermute | solution.py:24
  53.0 14.5 %all-to-all-start.2 = ((bf16[16,16,1024]{2,1,0:T(8,128)(2,1)}), bf16[16,16,1024]{2,1,0:T(8,128)(2,1)S(1)}, u32[]{:S(2)}, u32[]{:S(2)}) async-start(bf16[16,16,1024]{2,1,0:T(8,128)(2,1)} %bitcast.9), calls=%async_computation.2 | async-start | bytes 1048576 | tf_op jit(solution)/shard_map/all_to_all | solution.py:33
  56.6 1.6 %collective-permute-start.4 = (bf16[64,1024]{1,0:T(8,128)(2,1)S(1)}, bf16[64,1024]{1,0:T(8,128)(2,1)S(1)}, u32[]{:S(2)}, u32[]{:S(2)}) collective-permute-start(bf16[64,1024]{1,0:T(8,128)(2,1)S(1)} %slice.131), channel_id=1, source_target_pairs={{0,1},{1,0},{2,3},{3,2},{4,5},{5,4},{6,7},{7,6},{8,9},{9,8},{10,11... | collective-permute-start | bytes 393224 | tf_op jit(solution)/shard_map/ppermute | solution.py:24
  60.9 6.9 %collective-permute-start.5 = (bf16[64,1024]{1,0:T(8,128)(2,1)S(1)}, bf16[64,1024]{1,0:T(8,128)(2,1)S(1)}, u32[]{:S(2)}, u32[]{:S(2)}) collective-permute-start(bf16[64,1024]{1,0:T(8,128)(2,1)S(1)} %constant_dynamic-slice_fusion), channel_id=1, source_target_pairs={{0,1},{1,0},{2,3},{3,2},{4,5},{5,4},{6,7},{7,6},{8,9},{9,8},{10,11... | collective-permute-start | bytes 393224 | tf_op jit(solution)/shard_map/ppermute | solution.py:24

commit v5 on v4

--- a/solution.py
+++ b/solution.py
@@ -48,6 +48,7 @@
 
 FAR = pl.BlockSpec(memory_space=pl.ANY)
 NEAR = pl.BlockSpec(memory_space=pltpu.VMEM)
+SMALL = pltpu.CompilerParams(vmem_limit_bytes=32 * 2**20)
 
 
 def in_vmem(array):
@@ -180,14 +181,15 @@
             pltpu.VMEM((rows, width // 2), jnp.bfloat16),
             pltpu.SemaphoreType.DMA((9,)),
         ],
+        compiler_params=SMALL,
         name="assemble",
     )(
-        core.reshape(1).astype(jnp.int32), in_vmem(tokens), in_vmem(mine), in_vmem(theirs),
+        core, in_vmem(tokens), in_vmem(mine), in_vmem(theirs),
         in_vmem(gain), in_vmem(side),
     )
 
 
-def route(line, second, rows, weights, done):
+def route(line, second, weights):
     planes, depth, _ = second.shape
     half = line.shape[1] - 256
     tiles = [
@@ -207,51 +209,97 @@
                 parts.append(part)
             start = 256 * which + 128 * parity
             weights[:, start : start + 128] = jnp.concatenate(parts, axis=0).astype(jnp.bfloat16)
-    copies = [
-        pltpu.make_async_copy(weights, second.at[k, :, pl.ds(1024, 768)], done.at[k])
-        for k in range(planes)
-    ]
-    for copy in copies:
-        copy.start()
+    second[:, :, half:] = jnp.broadcast_to(weights[...][None], (planes, depth, 768))
     marks = line[:, half : half + 128]
+    count = planes * depth
+    row = lax.broadcasted_iota(jnp.int32, (count, 128), 0)
+    lane = lax.broadcasted_iota(jnp.int32, (count, 128), 1)
+    spread = jnp.where(lane == 96 + row // depth, 1.0, 0.0).astype(jnp.bfloat16)
+    place = dot(spread, marks, ((1,), (1,)))
+    row, lane = row[:, : line.shape[0]], lane[:, : line.shape[0]]
+    taken = (place == (1 + row % CAP).astype(jnp.float32)) & (row // CAP % 8 == lane // 8)
+    taken = jnp.where(taken, 1.0, 0.0).astype(jnp.bfloat16)
+    second[:, :, :half] = (
+        dot(taken, line[:, :half]).astype(jnp.bfloat16).reshape(planes, depth, half)
+    )
+
+
+def routed_rows(line, planes):
+    half = line.shape[1] - 256
+    return pl.pallas_call(
+        route,
+        out_shape=pltpu.VMEM((planes, 16, half + 768), jnp.bfloat16),
+        in_specs=[NEAR],
+        out_specs=NEAR,
+        scratch_shapes=[pltpu.VMEM((16, 768), jnp.bfloat16)],
+        compiler_params=SMALL,
+        name="route",
+    )(in_vmem(line))
+
+
+def widen(core, arrived, gate, up, far, pre, sent):
+    planes, depth, _ = arrived.shape
+    half, wide = far.shape
+    units = wide // 2
+    rows = arrived[:, :, :half].reshape(planes * depth, half)
+    start = pl.multiple_of(core[0] * half, half)
+    there = dot(rows, far[...])
+    here = [dot(rows, matrix[pl.ds(start, half), :]) for matrix in (gate, up)]
+    parts = (here[0], there[:, :units], here[1], there[:, units:])
+    for k in range(4):
+        pre[:, k * units : (k + 1) * units] = parts[k]
+        sent[:, k * units : (k + 1) * units] = parts[k ^ 1].astype(jnp.bfloat16)
+
+
+def widened(core, arrived, gate, up, far):
+    slots, wide = arrived.shape[0] * arrived.shape[1], 2 * far.shape[1]
+    return pl.pallas_call(
+        widen,
+        out_shape=(
+            pltpu.VMEM((slots, wide), jnp.float32),
+            pltpu.VMEM((slots, wide), jnp.bfloat16),
+        ),
+        in_specs=[pl.BlockSpec(memory_space=pltpu.SMEM)] + [NEAR] * 4,
+        out_specs=(NEAR, NEAR),
+        compiler_params=SMALL,
+        name="widen",
+    )(core, *[in_vmem(a) for a in (arrived, gate, up, far)])
+
+
+def narrow(core, pre, came, down, far, result, rows, done):
+    units = far.shape[0]
+    planes, depth, half = result.shape
+    start = pl.multiple_of(core[0] * half, half)
+    near = down[:, pl.ds(start, half)]
     group = planes // 4
     count = group * depth
+    copies = []
     for step in range(4):
-        row = lax.broadcasted_iota(jnp.int32, (count, 128), 0) + step * count
-        lane = lax.broadcasted_iota(jnp.int32, (count, 128), 1)
-        spread = jnp.where(lane == 96 + row // depth, 1.0, 0.0).astype(jnp.bfloat16)
-        place = dot(spread, marks, ((1,), (1,)))
-        row, lane = row[:, : line.shape[0]], lane[:, : line.shape[0]]
-        taken = (place == (1 + row % CAP).astype(jnp.float32)) & (row // CAP % 8 == lane // 8)
-        taken = jnp.where(taken, 1.0, 0.0).astype(jnp.bfloat16)
-        rows[pl.ds(step * group, group)] = (
-            dot(taken, line[:, :half]).astype(jnp.bfloat16).reshape(group, depth, half)
-        )
-        copy = pltpu.make_async_copy(
-            rows.at[pl.ds(step * group, group)],
-            second.at[pl.ds(step * group, group), :, pl.ds(0, 1024)],
-            done.at[planes + step],
-        )
+        part = slice(step * count, (step + 1) * count)
+        total = pre[part, :] + came[part, :].astype(jnp.float32)
+        gate = total[:, : 2 * units]
+        hidden = (gate / (1.0 + jnp.exp(-gate)) * total[:, 2 * units :]).astype(jnp.bfloat16)
+        out = dot(hidden[:, :units], near) + dot(hidden[:, units:], far[...])
+        here = pl.ds(step * group, group)
+        rows[here] = out.astype(jnp.bfloat16).reshape(group, depth, half)
+        copy = pltpu.make_async_copy(rows.at[here], result.at[here], done.at[step])
         copy.start()
         copies.append(copy)
     for copy in copies:
         copy.wait()
 
 
-def routed_rows(line, planes):
-    half = line.shape[1] - 256
+def narrowed(core, pre, came, down, far, planes):
+    shape = (planes, pre.shape[0] // planes, far.shape[1])
     return pl.pallas_call(
-        route,
-        out_shape=jax.ShapeDtypeStruct((planes, 16, half + 768), jnp.bfloat16),
-        in_specs=[NEAR],
+        narrow,
+        out_shape=jax.ShapeDtypeStruct(shape, jnp.bfloat16),
+        in_specs=[pl.BlockSpec(memory_space=pltpu.SMEM)] + [NEAR] * 4,
         out_specs=FAR,
-        scratch_shapes=[
-            pltpu.VMEM((planes, 16, half), jnp.bfloat16),
-            pltpu.VMEM((16, 768), jnp.bfloat16),
-            pltpu.SemaphoreType.DMA((planes + 4,)),
-        ],
-        name="route",
-    )(in_vmem(line))
+        scratch_shapes=[pltpu.VMEM(shape, jnp.bfloat16), pltpu.SemaphoreType.DMA((4,))],
+        compiler_params=SMALL,
+        name="narrow",
+    )(core, *[in_vmem(a) for a in (pre, came, down, far)])
 
 
 def shards(
@@ -289,8 +337,9 @@
         value_weight, expert_ids, route_weights, dense_gate, dense_up, dense_down.T,
         recurrent_state[:, 0], head_gain, out_weight,
     )
+    which = core.reshape(1).astype(jnp.int32)
     first, own_half = assembled(
-        core, tokens, partial_value, swapped(partial_value), second_gain, side
+        which, tokens, partial_value, swapped(partial_value), second_gain, side
     )
     first, gate, up, down = lax.optimization_barrier(
         (first, expert_gate[0], expert_up[0], expert_down[0])
@@ -298,28 +347,17 @@
     line = exchanged(first, "ep_0")
     line = line.reshape(lines * rows_dev, half + 256)
     given = jnp.concatenate([half_of(gate, 1 - core, 0), half_of(up, 1 - core, 0)], axis=1)
-    taken_in = swapped(given)
-    taken_down = swapped(half_of(down, 1 - core, 1))
-    inner = gate.shape[1]
-    weights_in = jnp.concatenate(
-        [half_of(gate, core, 0), taken_in[:, :inner], half_of(up, core, 0), taken_in[:, inner:]],
-        axis=1,
-    )
-    weights_down = jnp.concatenate([half_of(down, core, 1), taken_down], axis=0)
+    far_in = swapped(given)
+    far_down = swapped(half_of(down, 1 - core, 1))
+    line, far_in, far_down, gate, up, down = lax.optimization_barrier(
+        (line, far_in, far_down, gate, up, down)
+    )
     arrived = exchanged(routed_rows(line, plane), PLANE)
     slots = plane * lines * CAP
-    mine = arrived[:, :, :half].reshape(slots, half)
-    partial_in = jnp.dot(mine, weights_in, preferred_element_type=jnp.float32)
-    blocks = [partial_in[:, k * inner : (k + 1) * inner] for k in (1, 0, 3, 2)]
-    pre = partial_in + swapped(
-        jnp.concatenate(blocks, axis=1).astype(jnp.bfloat16)
-    ).astype(jnp.float32)
-    activated = (jax.nn.silu(pre[:, : 2 * inner]) * pre[:, 2 * inner :]).astype(jnp.bfloat16)
-    summed = jnp.dot(activated, weights_down, preferred_element_type=jnp.float32).astype(
-        jnp.bfloat16
-    )
+    pre, sent = widened(which, arrived, gate, up, far_in)
+    summed = narrowed(which, pre, swapped(sent), down, far_down, plane)
     summed, arrived, line = lax.optimization_barrier((summed, arrived, line))
-    came_back = exchanged(summed.reshape(plane, lines * CAP, half), PLANE)
+    came_back = exchanged(summed, PLANE)
     line_in = line[:, :half]
     line_rest = swapped(line_in)
     pre_gate = jnp.dot(

time: 79.9 us -> 82.6 us (1.034)
  waiting for transfers between devices: 27.8 us -> 30.7 us
  starting transfers between devices: 27.5 us -> 24.8 us
  Pallas kernels: 5.97 us -> 8.1 us
  matrix products: 5.12 us -> 3.58 us
  local copies, waits for them, and re-layouts: 0.86 us -> 2.34 us
    all_to_all x3, waiting for transfers between devices: 24.4 us -> 27.4 us  [exchanged(): return lax.all_to_all(array, axis, split_axis=0, concat_axis=0, tiled=True)]
    ppermute x6, starting transfers between devices: 10.7 us -> 7.95 us  [swapped(): return lax.ppermute(array, 'tp', SWAP)]
    pallas_call x1 -> x3, Pallas kernels: 1.63 us -> 3.76 us  [the longest x1 1.36 us: routed_rows(): pl.pallas_call(route, out_shape=pltpu.VMEM((planes, 16, half + 768), jnp....]
    unnamed x12 -> x16, local copies, waits for them, and re-layouts: 0.03 us -> 1.7 us
    dot_general x2 -> x0, matrix products: 1.55 us -> none  [the longest x1 1.11 us: shards(): jnp.dot(activated, weights_down, preferred_element_type=jnp.float32)]
  transfers between devices with their start and end apart: 9 -> 9, of which waited for: 7 -> 6; matrix products, arithmetic and copies ran while one was open for 6% -> 5% of each run, Pallas kernels for 0% -> 0%
where the time goes in v5:
time: 82.6 us; the launch traced here: 81.9 us
  waiting for transfers between devices  30.7 us (37%)
  starting transfers between devices  24.8 us (30%)
  blocking collectives  10.4 us (13%)
  Pallas kernels  8.1 us (10%)
  matrix products  3.58 us (4%)
  local copies, waits for them, and re-layouts  2.34 us (3%)
  other arithmetic  1.74 us (2%)
    all_to_all x3, waiting for transfers between devices, exchanged(): return lax.all_to_all(array, axis, split_axis=0, concat_axis=0, tiled=True)  27.4 us
    all_to_all x3, starting transfers between devices, exchanged(): return lax.all_to_all(array, axis, split_axis=0, concat_axis=0, tiled=True)  16.8 us
    all_to_all x1, blocking collectives, exchanged(): return lax.all_to_all(array, axis, split_axis=0, concat_axis=0, tiled=True)  10.4 us
    ppermute x6, starting transfers between devices, swapped(): return lax.ppermute(array, 'tp', SWAP)  7.95 us
    pallas_call x1, Pallas kernels, attended(): pl.pallas_call(attend, out_shape=(pltpu.VMEM(tokens.shape, jnp.bfloat16),...  3.49 us
    ppermute x6, waiting for transfers between devices, swapped(): return lax.ppermute(array, 'tp', SWAP)  3.35 us
    unnamed x16, local copies, waits for them, and re-layouts  1.7 us
  transfers between devices with their start and end apart: 9, of which 6 were waited for; matrix products, arithmetic and copies ran while one was open for 5% of the time, Pallas kernels for 0%

profile of v5, /device:TPU:1, one launch (start us, length us, event | category | flops | bytes accessed | tf_op | source)
XLA Modules:
  0.0 81.9 jit_solution(10210333612465842068)
XLA Ops:
  0.0 0.0 copy-start.5
  0.0 3.5 %attend.1 = (bf16[8,2048]{1,0:T(8,128)(2,1)S(1)}, bf16[8,8,256]{2,1,0:T(8,128)(2,1)S(1)}) custom-call(bf16[8,2048]{1,0:T(8,128)(2,1)} %tokens.1, bf16[2048]{0:T(1024)(128)(2,1)} %refs_1_.1, bf16[2048,128]{1,0:T(8,128)(2,1)} %refs_2_.1, bf16[16,2048]{1,0:T(8,128)(2,1)} %bitcast.68, bf16[2048,128]{1,0:T(8,128)(2,1)} %refs_4_.1, bf16[16,128]{1,0:T(8,128)(2,1)} %refs_5_.1, ...), custom_call_target="tpu_custom_call" | custom-call | tf_op jit(solution)/shard_map/attend/pallas_call | solution.py:135
  3.5 3.3 %collective-permute-start = (bf16[8,2048]{1,0:T(8,128)(2,1)S(1)}, bf16[8,2048]{1,0:T(8,128)(2,1)S(1)}, u32[]{:S(2)}, u32[]{:S(2)}) collective-permute-start(bf16[8,2048]{1,0:T(8,128)(2,1)S(1)} %get-tuple-element.24.mine), channel_id=1, source_target_pairs={{0,1},{1,0},{2,3},{3,2},{4,5},{5,4},{6,7},{7,6},{8,9},{9,8},{10,11... | collective-permute-start | bytes 98312 | tf_op jit(solution)/shard_map/ppermute | solution.py:24
  6.8 0.9 %collective-permute-done.theirs = bf16[8,2048]{1,0:T(8,128)(2,1)S(1)} collective-permute-done((bf16[8,2048]{1,0:T(8,128)(2,1)S(1)}, bf16[8,2048]{1,0:T(8,128)(2,1)S(1)}, u32[]{:S(2)}, u32[]{:S(2)}) %collective-permute-start) | collective-permute-done | bytes 32800 | tf_op jit(solution)/shard_map/ppermute | solution.py:24
  7.6 0.0 copy-done.5
  7.7 0.0 copy-done.6
  7.7 0.9 %assemble.1 = (bf16[8,8,1280]{2,1,0:T(8,128)(2,1)}, f32[8,1024]{1,0:T(8,128)S(1)}) custom-call(s32[1]{0:T(128)} %bitcast.core, bf16[8,2048]{1,0:T(8,128)(2,1)S(1)} %copy-done.5, bf16[8,2048]{1,0:T(8,128)(2,1)S(1)} %get-tuple-element.24.mine, bf16[8,2048]{1,0:T(8,128)(2,1)S(1)} %collective-permute-done.theirs, bf16[2048]{0:T(1024)(128)(2,1)S(1)} %copy-done.6, ...), custom_call_target="tpu_custom_call" | custom-call | tf_op jit(solution)/shard_map/assemble/pallas_call | solution.py:172
  8.5 0.0 copy-done.1
  8.5 0.0 copy-done.2
  8.6 0.0 copy-start
  8.6 0.9 %pad_maximum_fusion = bf16[1024,256]{1,0:T(8,128)(2,1)} fusion(bf16[1024,128]{1,0:T(8,128)(2,1)S(1)} %get-tuple-element.71, bf16[1024,128]{1,0:T(8,128)(2,1)S(1)} %get-tuple-element.72), kind=kLoop, calls=%fused_computation.30 | loop fusion | flops 1048576 | bytes 1048576 | tf_op jit(solution)/shard_map/concatenate | solution.py:349
  9.5 0.3 collective-permute-start.1
  9.8 6.5 %all-to-all-start = ((bf16[8,8,1280]{2,1,0:T(8,128)(2,1)}), bf16[8,8,1280]{2,1,0:T(8,128)(2,1)S(1)}, u32[]{:S(2)}, u32[]{:S(2)}) async-start(bf16[8,8,1280]{2,1,0:T(8,128)(2,1)} %get-tuple-element.28), calls=%async_computation | async-start | bytes 327680 | tf_op jit(solution)/shard_map/all_to_all | solution.py:33
  16.3 0.0 copy-done
  16.3 0.5 collective-permute-start.2
  16.9 1.2 %collective-permute-done.2.far = bf16[128,1024]{1,0:T(8,128)(2,1)S(1)} collective-permute-done((bf16[128,1024]{1,0:T(8,128)(2,1)S(1)}, bf16[128,1024]{1,0:T(8,128)(2,1)S(1)}, u32[]{:S(2)}, u32[]{:S(2)}) %collective-permute-start.2) | collective-permute-done | bytes 262176 | tf_op jit(solution)/shard_map/ppermute | solution.py:24
  18.0 7.3 %all-to-all-done = bf16[8,8,1280]{2,1,0:T(8,128)(2,1)S(1)} async-done(((bf16[8,8,1280]{2,1,0:T(8,128)(2,1)}), bf16[8,8,1280]{2,1,0:T(8,128)(2,1)S(1)}, u32[]{:S(2)}, u32[]{:S(2)}) %all-to-all-start) | async-done | bytes 163872 | tf_op jit(solution)/shard_map/all_to_all | solution.py:33
  25.3 0.0 collective-permute-done.1.far
  25.3 1.4 %route.1 = bf16[16,16,1792]{2,1,0:T(8,128)(2,1)} custom-call(bf16[64,1280]{1,0:T(8,128)(2,1)S(1)} %bitcast.36), custom_call_target="tpu_custom_call" | custom-call | tf_op jit(solution)/shard_map/route/pallas_call | solution.py:229
  26.6 0.0 copy-done.3
  26.6 6.8 %all-to-all-start.1 = ((bf16[16,16,1792]{2,1,0:T(8,128)(2,1)}), bf16[16,16,1792]{2,1,0:T(8,128)(2,1)S(1)}, u32[]{:S(2)}, u32[]{:S(2)}) async-start(bf16[16,16,1792]{2,1,0:T(8,128)(2,1)} %route.1), calls=%async_computation.1 | async-start | bytes 1835008 | tf_op jit(solution)/shard_map/all_to_all | solution.py:33
  33.5 0.0 copy-start.7
  33.5 0.6 copy-done.7
  34.1 13.1 %all-to-all-done.1.arrived = bf16[16,16,1792]{2,1,0:T(8,128)(2,1)S(1)} async-done(((bf16[16,16,1792]{2,1,0:T(8,128)(2,1)}), bf16[16,16,1792]{2,1,0:T(8,128)(2,1)S(1)}, u32[]{:S(2)}, u32[]{:S(2)}) %all-to-all-start.1) | async-done | bytes 917536 | tf_op jit(solution)/shard_map/all_to_all | solution.py:33
  47.2 1.0 %copy-done.4 = bf16[1024,256]{1,0:T(8,128)(2,1)S(1)} copy-done((bf16[1024,256]{1,0:T(8,128)(2,1)S(1)}, bf16[1024,256]{1,0:T(8,128)(2,1)}, u32[]{:S(2)}) %copy-start.4) | copy-done | bytes 524312
  48.2 1.3 %widen.1 = (f32[256,512]{1,0:T(8,128)S(1)}, bf16[256,512]{1,0:T(8,128)(2,1)}) custom-call(s32[1]{0:T(128)} %bitcast.core, bf16[16,16,1792]{2,1,0:T(8,128)(2,1)S(1)} %all-to-all-done.1.arrived, bf16[2048,128]{1,0:T(8,128)(2,1)S(1)} %bitcast.46, bf16[2048,128]{1,0:T(8,128)(2,1)S(1)} %bitcast.48, bf16[1024,256]{1,0:T(8,128)(2,1)S(1)} %copy-done.4), custom_call_target="tpu_custom_call" | custom-call | tf_op jit(solution)/shard_map/widen/pallas_call | solution.py:256
  49.5 3.1 %collective-permute-start.3 = (bf16[256,512]{1,0:T(8,128)(2,1)}, bf16[256,512]{1,0:T(8,128)(2,1)S(1)}, u32[]{:S(2)}, u32[]{:S(2)}) collective-permute-start(bf16[256,512]{1,0:T(8,128)(2,1)} %get-tuple-element.37), channel_id=1, source_target_pairs={{0,1},{1,0},{2,3},{3,2},{4,5},{5,4},{6,7},{7,6},{8,9},{9,8},{10,11... | collective-permute-start | bytes 786440 | tf_op jit(solution)/shard_map/ppermute | solution.py:24
  52.7 1.3 %collective-permute-done.3.came = bf16[256,512]{1,0:T(8,128)(2,1)S(1)} collective-permute-done((bf16[256,512]{1,0:T(8,128)(2,1)}, bf16[256,512]{1,0:T(8,128)(2,1)S(1)}, u32[]{:S(2)}, u32[]{:S(2)}) %collective-permute-start.3) | collective-permute-done | bytes 262176 | tf_op jit(solution)/shard_map/ppermute | solution.py:24
  54.0 1.1 %narrow.1 = bf16[16,16,1024]{2,1,0:T(8,128)(2,1)} custom-call(s32[1]{0:T(128)} %bitcast.core, f32[256,512]{1,0:T(8,128)S(1)} %get-tuple-element.36.pre, bf16[256,512]{1,0:T(8,128)(2,1)S(1)} %collective-permute-done.3.came, bf16[128,2048]{1,0:T(8,128)(2,1)S(1)} %bitcast.44, bf16[128,1024]{1,0:T(8,128)(2,1)S(1)} %collective-permute-done.2.far), custom_call_target="tpu_custom_call" | custom-call | tf_op jit(solution)/shard_map/narrow/pallas_call | solution.py:294
  55.2 0.5 collective-permute-start.4
  55.6 0.1 fusion.67
  55.7 3.6 %all-to-all-start.2 = ((bf16[16,16,1024]{2,1,0:T(8,128)(2,1)}), bf16[16,16,1024]{2,1,0:T(8,128)(2,1)S(1)}, u32[]{:S(2)}, u32[]{:S(2)}) async-start(bf16[16,16,1024]{2,1,0:T(8,128)(2,1)} %narrow.1), calls=%async_computation.2 | async-start | bytes 1048576 | tf_op jit(solution)/shard_map/all_to_all | solution.py:33
  59.3 0.3 fusion.14
  59.6 0.3 fusion.7
  59.9 0.3 fusion
  60.2 0.1 convolution_bitcast_fusion.1
  60.3 0.0 collective-permute-done.4
  60.4 0.2 convolution_select_fusion
  60.5 0.2 convolution_select_fusion.1
  60.7 0.2 convolution_select_fusion.2
  60.9 0.2 fusion.3
  61.0 0.1 fusion.71
  61.1 0.1 fusion.72
  61.2 0.1 fusion.73
  61.2 0.2 convolution_select_fusion.4
  61.4 0.2 convolution_select_fusion.5
  61.6 0.2 convolution_select_fusion.6
  61.7 0.2 fusion.6
  61.9 0.1 fusion.68
  62.0 0.1 fusion.69
  62.1 0.1 fusion.70
  62.1 0.1 fusion.39
  62.3 0.2 convolution_convert_fusion
  62.4 0.2 convolution_convert_fusion.1
  62.6 0.2 convolution_convert_fusion.2
  62.8 0.2 convolution_convert_fusion.3
  63.0 0.2 collective-permute-start.5
  63.2 0.1 fusion.12
  63.4 7.1 %all-to-all-done.2 = bf16[16,16,1024]{2,1,0:T(8,128)(2,1)S(1)} async-done(((bf16[16,16,1024]{2,1,0:T(8,128)(2,1)}), bf16[16,16,1024]{2,1,0:T(8,128)(2,1)S(1)}, u32[]{:S(2)}, u32[]{:S(2)}) %all-to-all-start.2) | async-done | bytes 524320 | tf_op jit(solution)/shard_map/all_to_all | solution.py:33
  70.4 0.2 fusion.45
  70.7 0.0 collective-permute-done.5
  70.7 0.2 fusion.13
  70.9 10.4 %all_to_all.20 = bf16[8,8,1024]{2,1,0:T(8,128)(2,1)S(1)} all-to-all(bf16[8,8,1024]{2,1,0:T(8,128)(2,1)S(1)} %fusion.13), channel_id=1, replica_groups=mesh['ep_0'=8,'ep_1'=4,'ep_2'=4,'tp'=2] {'ep_0'}, dimensions={0} | all-to-all | bytes 262144 | tf_op jit(solution)/shard_map/all_to_all | solution.py:33
  81.3 0.6 add_convert_fusion.1
  (25 shorter events, 0.3 us)
Async XLA Ops:
  0.0 7.7 %copy-start.5 = (bf16[8,2048]{1,0:T(8,128)(2,1)S(1)}, bf16[8,2048]{1,0:T(8,128)(2,1)}, u32[]{:S(2)}) copy-start(bf16[8,2048]{1,0:T(8,128)(2,1)} %tokens.1) | copy-start | bytes 98308
  0.0 8.5 %copy-start.1 = (bf16[1,2048,128]{2,1,0:T(8,128)(2,1)S(1)}, bf16[1,2048,128]{2,1,0:T(8,128)(2,1)}, u32[]{:S(2)}) copy-start(bf16[1,2048,128]{2,1,0:T(8,128)(2,1)} %param.35) | copy-start | bytes 1572868
  0.0 8.5 %copy-start.2 = (bf16[1,2048,128]{2,1,0:T(8,128)(2,1)S(1)}, bf16[1,2048,128]{2,1,0:T(8,128)(2,1)}, u32[]{:S(2)}) copy-start(bf16[1,2048,128]{2,1,0:T(8,128)(2,1)} %param.36) | copy-start | bytes 1572868
  3.5 4.1 %collective-permute-start = (bf16[8,2048]{1,0:T(8,128)(2,1)S(1)}, bf16[8,2048]{1,0:T(8,128)(2,1)S(1)}, u32[]{:S(2)}, u32[]{:S(2)}) collective-permute-start(bf16[8,2048]{1,0:T(8,128)(2,1)S(1)} %get-tuple-element.24.mine), channel_id=1, source_target_pairs={{0,1},{1,0},{2,3},{3,2},{4,5},{5,4},{6,7},{7,6},{8,9},{9,8},{10,11... | collective-permute-start | bytes 98312 | tf_op jit(solution)/shard_map/ppermute | solution.py:24
  6.8 0.9 %copy-start.6 = (bf16[2048]{0:T(1024)(128)(2,1)S(1)}, bf16[2048]{0:T(1024)(128)(2,1)}, u32[]{:S(2)}) copy-start(bf16[2048]{0:T(1024)(128)(2,1)} %gain.1) | copy-start | bytes 12292
  8.6 7.7 %copy-start = (bf16[1,128,2048]{2,1,0:T(8,128)(2,1)S(1)}, bf16[1,128,2048]{2,1,0:T(8,128)(2,1)}, u32[]{:S(2)}) copy-start(bf16[1,128,2048]{2,1,0:T(8,128)(2,1)} %param.37) | copy-start | bytes 1572868
  9.5 15.8 %collective-permute-start.1 = (bf16[1024,256]{1,0:T(8,128)(2,1)}, bf16[1024,256]{1,0:T(8,128)(2,1)S(1)}, u32[]{:S(2)}, u32[]{:S(2)}) collective-permute-start(bf16[1024,256]{1,0:T(8,128)(2,1)} %pad_maximum_fusion), channel_id=1, source_target_pairs={{0,1},{1,0},{2,3},{3,2},{4,5},{5,4},{6,7},{7,6},{8,9},{9,8},{10,11... | collective-permute-start | bytes 1572872 | tf_op jit(solution)/shard_map/ppermute | solution.py:24
  9.8 15.5 %all-to-all-start = ((bf16[8,8,1280]{2,1,0:T(8,128)(2,1)}), bf16[8,8,1280]{2,1,0:T(8,128)(2,1)S(1)}, u32[]{:S(2)}, u32[]{:S(2)}) async-start(bf16[8,8,1280]{2,1,0:T(8,128)(2,1)} %get-tuple-element.28), calls=%async_computation | async-start | bytes 327680 | tf_op jit(solution)/shard_map/all_to_all | solution.py:33
  16.3 1.7 %collective-permute-start.2 = (bf16[128,1024]{1,0:T(8,128)(2,1)S(1)}, bf16[128,1024]{1,0:T(8,128)(2,1)S(1)}, u32[]{:S(2)}, u32[]{:S(2)}) collective-permute-start(bf16[128,1024]{1,0:T(8,128)(2,1)S(1)} %constant_dynamic-slice_fusion.1), channel_id=1, source_target_pairs={{0,1},{1,0},{2,3},{3,2},{4,5},{5,4},{6,7},{7,6},{8,9},{9,8},{10,11... | collective-permute-start | bytes 786440 | tf_op jit(solution)/shard_map/ppermute | solution.py:24
  25.3 1.4 %copy-start.3 = (bf16[1024,256]{1,0:T(8,128)(2,1)}, bf16[1024,256]{1,0:T(8,128)(2,1)S(1)}, u32[]{:S(2)}) copy-start(bf16[1024,256]{1,0:T(8,128)(2,1)S(1)} %collective-permute-done.1.far) | copy-start | bytes 1572868
  26.6 20.6 %all-to-all-start.1 = ((bf16[16,16,1792]{2,1,0:T(8,128)(2,1)}), bf16[16,16,1792]{2,1,0:T(8,128)(2,1)S(1)}, u32[]{:S(2)}, u32[]{:S(2)}) async-start(bf16[16,16,1792]{2,1,0:T(8,128)(2,1)} %route.1), calls=%async_computation.1 | async-start | bytes 1835008 | tf_op jit(solution)/shard_map/all_to_all | solution.py:33
  33.5 0.7 copy-start.7
  47.2 1.0 %copy-start.4 = (bf16[1024,256]{1,0:T(8,128)(2,1)S(1)}, bf16[1024,256]{1,0:T(8,128)(2,1)}, u32[]{:S(2)}) copy-start(bf16[1024,256]{1,0:T(8,128)(2,1)} %copy-done.3) | copy-start | bytes 1572868
  49.5 4.5 %collective-permute-start.3 = (bf16[256,512]{1,0:T(8,128)(2,1)}, bf16[256,512]{1,0:T(8,128)(2,1)S(1)}, u32[]{:S(2)}, u32[]{:S(2)}) collective-permute-start(bf16[256,512]{1,0:T(8,128)(2,1)} %get-tuple-element.37), channel_id=1, source_target_pairs={{0,1},{1,0},{2,3},{3,2},{4,5},{5,4},{6,7},{7,6},{8,9},{9,8},{10,11... | collective-permute-start | bytes 786440 | tf_op jit(solution)/shard_map/ppermute | solution.py:24
  55.2 5.2 %collective-permute-start.4 = (bf16[64,1024]{1,0:T(8,128)(2,1)S(1)}, bf16[64,1024]{1,0:T(8,128)(2,1)S(1)}, u32[]{:S(2)}, u32[]{:S(2)}) collective-permute-start(bf16[64,1024]{1,0:T(8,128)(2,1)S(1)} %slice.91), channel_id=1, source_target_pairs={{0,1},{1,0},{2,3},{3,2},{4,5},{5,4},{6,7},{7,6},{8,9},{9,8},{10,11... | collective-permute-start | bytes 393224 | tf_op jit(solution)/shard_map/ppermute | solution.py:24
  55.7 14.8 %all-to-all-start.2 = ((bf16[16,16,1024]{2,1,0:T(8,128)(2,1)}), bf16[16,16,1024]{2,1,0:T(8,128)(2,1)S(1)}, u32[]{:S(2)}, u32[]{:S(2)}) async-start(bf16[16,16,1024]{2,1,0:T(8,128)(2,1)} %narrow.1), calls=%async_computation.2 | async-start | bytes 1048576 | tf_op jit(solution)/shard_map/all_to_all | solution.py:33
  63.0 7.6 %collective-permute-start.5 = (bf16[64,1024]{1,0:T(8,128)(2,1)S(1)}, bf16[64,1024]{1,0:T(8,128)(2,1)S(1)}, u32[]{:S(2)}, u32[]{:S(2)}) collective-permute-start(bf16[64,1024]{1,0:T(8,128)(2,1)S(1)} %constant_dynamic-slice_fusion), channel_id=1, source_target_pairs={{0,1},{1,0},{2,3},{3,2},{4,5},{5,4},{6,7},{7,6},{8,9},{9,8},{10,11... | collective-permute-start | bytes 393224 | tf_op jit(solution)/shard_map/ppermute | solution.py:24

commit v6 on v5

--- a/solution.py
+++ b/solution.py
@@ -189,7 +189,7 @@
     )
 
 
-def route(line, second, weights):
+def route(line, second, copy, weights):
     planes, depth, _ = second.shape
     half = line.shape[1] - 256
     tiles = [
@@ -210,6 +210,7 @@
             start = 256 * which + 128 * parity
             weights[:, start : start + 128] = jnp.concatenate(parts, axis=0).astype(jnp.bfloat16)
     second[:, :, half:] = jnp.broadcast_to(weights[...][None], (planes, depth, 768))
+    copy[...] = line[:, :half]
     marks = line[:, half : half + 128]
     count = planes * depth
     row = lax.broadcasted_iota(jnp.int32, (count, 128), 0)
@@ -228,9 +229,12 @@
     half = line.shape[1] - 256
     return pl.pallas_call(
         route,
-        out_shape=pltpu.VMEM((planes, 16, half + 768), jnp.bfloat16),
+        out_shape=(
+            pltpu.VMEM((planes, 16, half + 768), jnp.bfloat16),
+            pltpu.VMEM((line.shape[0], half), jnp.bfloat16),
+        ),
         in_specs=[NEAR],
-        out_specs=NEAR,
+        out_specs=(NEAR, NEAR),
         scratch_shapes=[pltpu.VMEM((16, 768), jnp.bfloat16)],
         compiler_params=SMALL,
         name="route",
@@ -266,40 +270,100 @@
     )(core, *[in_vmem(a) for a in (arrived, gate, up, far)])
 
 
-def narrow(core, pre, came, down, far, result, rows, done):
+def narrow(core, pre, came, down, far, result):
     units = far.shape[0]
     planes, depth, half = result.shape
     start = pl.multiple_of(core[0] * half, half)
     near = down[:, pl.ds(start, half)]
-    group = planes // 4
-    count = group * depth
-    copies = []
-    for step in range(4):
-        part = slice(step * count, (step + 1) * count)
-        total = pre[part, :] + came[part, :].astype(jnp.float32)
-        gate = total[:, : 2 * units]
-        hidden = (gate / (1.0 + jnp.exp(-gate)) * total[:, 2 * units :]).astype(jnp.bfloat16)
-        out = dot(hidden[:, :units], near) + dot(hidden[:, units:], far[...])
-        here = pl.ds(step * group, group)
-        rows[here] = out.astype(jnp.bfloat16).reshape(group, depth, half)
-        copy = pltpu.make_async_copy(rows.at[here], result.at[here], done.at[step])
-        copy.start()
-        copies.append(copy)
-    for copy in copies:
-        copy.wait()
+    total = pre[...] + came[...].astype(jnp.float32)
+    gate = total[:, : 2 * units]
+    hidden = (gate / (1.0 + jnp.exp(-gate)) * total[:, 2 * units :]).astype(jnp.bfloat16)
+    out = dot(hidden[:, :units], near) + dot(hidden[:, units:], far[...])
+    result[...] = out.astype(jnp.bfloat16).reshape(planes, depth, half)
 
 
 def narrowed(core, pre, came, down, far, planes):
     shape = (planes, pre.shape[0] // planes, far.shape[1])
     return pl.pallas_call(
         narrow,
-        out_shape=jax.ShapeDtypeStruct(shape, jnp.bfloat16),
+        out_shape=pltpu.VMEM(shape, jnp.bfloat16),
         in_specs=[pl.BlockSpec(memory_space=pltpu.SMEM)] + [NEAR] * 4,
-        out_specs=FAR,
-        scratch_shapes=[pltpu.VMEM(shape, jnp.bfloat16), pltpu.SemaphoreType.DMA((4,))],
+        out_specs=NEAR,
         compiler_params=SMALL,
         name="narrow",
     )(core, *[in_vmem(a) for a in (pre, came, down, far)])
+
+
+def branch_out(core, arrived, line, rest, mark_own, mark_rest, keep, sent, high, low):
+    planes, depth, _ = arrived.shape
+    count, half = rest.shape
+    quarter = half // 2
+
+    def matrix(m):
+        starts = [half + 256 * m + 128 * p for p in range(2)]
+        blocks = [arrived[:, :, at : at + 128].reshape(planes * depth, 128) for at in starts]
+        return jnp.concatenate(blocks, axis=0)
+
+    group = lax.broadcasted_iota(jnp.int32, (count, 128), 1) // 32
+    both = jnp.concatenate([matrix(0), matrix(1)], axis=1)
+    gate = jnp.zeros((count, 128), jnp.float32)
+    up = jnp.zeros((count, 128), jnp.float32)
+    pre = jnp.zeros((count, 1), jnp.float32)
+    for source, marks, first in (
+        (line[:, :half], mark_own, 2 * core[0]),
+        (rest[...], mark_rest, 2 - 2 * core[0]),
+    ):
+        wide = source.astype(jnp.float32) * marks[...].astype(jnp.float32)[None, :]
+        pre = pre + jnp.sum(wide, axis=1, keepdims=True)
+        for k in range(2):
+            part = dot(source[:, k * quarter : (k + 1) * quarter], both)
+            gate = gate + jnp.where(group == first + k, part[:, :128], 0.0)
+            up = up + jnp.where(group == first + k, part[:, 128:], 0.0)
+
+    def folded(total):
+        return total + sum(pltpu.roll(total, 32 * k, 1) for k in range(1, 4))
+
+    gate = folded(gate)
+    hidden = gate / (1.0 + jnp.exp(-gate)) * folded(up)
+    branch = 1.0 / (1.0 + jnp.exp(-pre))
+    down = matrix(2)
+    for target, first in ((sent, 2 - 2 * core[0]), (keep, 2 * core[0])):
+        for k in range(2):
+            units = jnp.where(group == first + k, hidden, 0.0).astype(jnp.bfloat16)
+            target[:, k * quarter : (k + 1) * quarter] = (
+                branch * dot(units, down, ((1,), (1,)))
+            ).astype(jnp.bfloat16)
+
+    slots = planes * depth
+    row = lax.broadcasted_iota(jnp.int32, (slots, 128), 0)
+    lane = lax.broadcasted_iota(jnp.int32, (slots, 128), 1)
+
+    def over_slots(start, tile):
+        spread = jnp.where(lane == start + row // depth, 1.0, 0.0).astype(jnp.bfloat16)
+        return dot(spread, line[:, half + 128 * tile : half + 128 * (tile + 1)], ((1,), (1,)))
+
+    place, share = over_slots(96, 0), over_slots(112, 0) + over_slots(96, 1)
+    row, lane = row[:, :count], lane[:, :count]
+    taken = (place == (1 + row % CAP).astype(jnp.float32)) & (row // CAP % 8 == lane // 8)
+    weighing = jnp.where(taken, share, 0.0)
+    upper = weighing.astype(jnp.bfloat16)
+    high[...] = upper
+    low[...] = (weighing - upper.astype(jnp.float32)).astype(jnp.bfloat16)
+
+
+def branched_out(core, arrived, line, rest, mark_own, mark_rest):
+    slots = arrived.shape[0] * arrived.shape[1]
+    return pl.pallas_call(
+        branch_out,
+        out_shape=tuple(
+            pltpu.VMEM(shape, jnp.bfloat16)
+            for shape in (rest.shape, rest.shape, (slots, line.shape[0]), (slots, line.shape[0]))
+        ),
+        in_specs=[pl.BlockSpec(memory_space=pltpu.SMEM)] + [NEAR] * 5,
+        out_specs=(NEAR,) * 4,
+        compiler_params=SMALL,
+        name="branch_out",
+    )(core, *[in_vmem(a) for a in (arrived, line, rest, mark_own, mark_rest)])
 
 
 def shards(
@@ -330,8 +394,6 @@
     lines = lax.axis_size("ep_0")
     plane = lax.axis_size(PLANE)
     half = width // 2
-    rows_own, hidden = dense_gate.shape
-    units = hidden // lines
     partial_value, side = attended(
         tokens, first_gain, query_weight, decay_down.T, key_weight, decay_up, decay_bias,
         value_weight, expert_ids, route_weights, dense_gate, dense_up, dense_down.T,
@@ -348,73 +410,29 @@
     line = line.reshape(lines * rows_dev, half + 256)
     given = jnp.concatenate([half_of(gate, 1 - core, 0), half_of(up, 1 - core, 0)], axis=1)
     far_in = swapped(given)
+    mark_own = half_of(branch_gate, core, 0)
+    mark_rest = half_of(branch_gate, 1 - core, 0)
     far_down = swapped(half_of(down, 1 - core, 1))
-    line, far_in, far_down, gate, up, down = lax.optimization_barrier(
-        (line, far_in, far_down, gate, up, down)
-    )
-    arrived = exchanged(routed_rows(line, plane), PLANE)
+    line, far_in, far_down, gate, up, down, mark_own, mark_rest = lax.optimization_barrier(
+        (line, far_in, far_down, gate, up, down, mark_own, mark_rest)
+    )
+    second, line_half = routed_rows(line, plane)
+    arrived = exchanged(second, PLANE)
+    arrived, line_half = lax.optimization_barrier((arrived, line_half))
     slots = plane * lines * CAP
+    rest = swapped(line_half)
     pre, sent = widened(which, arrived, gate, up, far_in)
-    summed = narrowed(which, pre, swapped(sent), down, far_down, plane)
-    summed, arrived, line = lax.optimization_barrier((summed, arrived, line))
+    came = swapped(sent)
+    keep, given_part, weigh_high, weigh_low = branched_out(
+        which, arrived, line, rest, mark_own, mark_rest
+    )
+    given_part = swapped(given_part)
+    summed = narrowed(which, pre, came, down, far_down, plane)
+    dense = keep.astype(jnp.float32) + given_part.astype(jnp.float32)
+    summed, dense, weigh_high, weigh_low = lax.optimization_barrier(
+        (summed, dense, weigh_high, weigh_low)
+    )
     came_back = exchanged(summed, PLANE)
-    line_in = line[:, :half]
-    line_rest = swapped(line_in)
-    pre_gate = jnp.dot(
-        line_in, half_of(branch_gate, core, 0), preferred_element_type=jnp.float32
-    ) + jnp.dot(line_rest, half_of(branch_gate, 1 - core, 0), preferred_element_type=jnp.float32)
-    branch = jax.nn.sigmoid(pre_gate)
-    matrices = [
-        jnp.concatenate(
-            [
-                arrived[:, :, half + 256 * m + 128 * p : half + 256 * m + 128 * (p + 1)].reshape(
-                    plane * rows_own, 128
-                )
-                for p in range(2)
-            ],
-            axis=0,
-        )
-        for m in range(3)
-    ]
-    quarter = width // 4
-    group = jnp.arange(128, dtype=jnp.int32)[None, :] // units
-    low = jnp.where(core == 0, line_in, line_rest)
-    high = jnp.where(core == 0, line_rest, line_in)
-
-    def through(matrix):
-        total = jnp.zeros((lines * rows_dev, 128), jnp.float32)
-        for q in range(4):
-            part = (low, high)[q // 2][:, q % 2 * quarter : (q % 2 + 1) * quarter]
-            total = total + jnp.where(
-                group == q, jnp.dot(part, matrix, preferred_element_type=jnp.float32), 0.0
-            )
-        return sum(jnp.roll(total, units * q, axis=1) for q in range(4))
-
-    line_hidden = (jax.nn.silu(through(matrices[0])) * through(matrices[1])).astype(jnp.bfloat16)
-    line_part = jnp.concatenate(
-        [dot(jnp.where(group == q, line_hidden, 0), matrices[2], ((1,), (1,))) for q in range(4)],
-        axis=1,
-    ).astype(jnp.bfloat16)
-    dense = branch[:, None] * (
-        half_of(line_part, core, 1).astype(jnp.float32)
-        + swapped(half_of(line_part, 1 - core, 1)).astype(jnp.float32)
-    )
-    row = lax.broadcasted_iota(jnp.int32, (slots, lines * rows_dev), 0)
-    col = lax.broadcasted_iota(jnp.int32, (slots, lines * rows_dev), 1)
-    spread = (
-        lax.broadcasted_iota(jnp.int32, (slots, plane), 0) // (lines * CAP)
-        == lax.broadcasted_iota(jnp.int32, (slots, plane), 1)
-    ).astype(jnp.bfloat16)
-
-    def over_slots(start):
-        return dot(spread, line[:, half + start : half + start + plane], ((1,), (1,)))
-
-    taken = (over_slots(96) == (1 + row % CAP).astype(jnp.float32)) & (
-        row // CAP % lines == col // rows_dev
-    )
-    weighing = jnp.where(taken, over_slots(112) + over_slots(224), 0.0)
-    weigh_high = weighing.astype(jnp.bfloat16)
-    weigh_low = (weighing - weigh_high.astype(jnp.float32)).astype(jnp.bfloat16)
 
     def combined(part):
         return lax.dot_general(

time: 82.6 us -> 78.8 us (0.954)
  blocking collectives: 10.4 us -> 44.4 us
  waiting for transfers between devices: 30.7 us -> 11.5 us
  starting transfers between devices: 24.8 us -> 14.3 us
  matrix products: 3.58 us -> 0.45 us
  local copies, waits for them, and re-layouts: 2.34 us -> 0.25 us
  Pallas kernels: 8.1 us -> 6.5 us
  other arithmetic: 1.74 us -> 0.72 us
    all_to_all x1 -> x3, blocking collectives: 10.4 us -> 44.4 us  [exchanged(): return lax.all_to_all(array, axis, split_axis=0, concat_axis=0, tiled=True)]
    all_to_all x3 -> x1, waiting for transfers between devices: 27.4 us -> 7.24 us  [exchanged(): return lax.all_to_all(array, axis, split_axis=0, concat_axis=0, tiled=True)]
    all_to_all x3 -> x1, starting transfers between devices: 16.8 us -> 6.49 us  [exchanged(): return lax.all_to_all(array, axis, split_axis=0, concat_axis=0, tiled=True)]
    dot_general x17 -> x0, matrix products: 3.16 us -> none  [the longest x7 1.59 us: dot(): lax.dot_general(a, b, (dims, ((), ())), preferred_element_type=jnp.float32)]
    unnamed x16 -> x12, local copies, waits for them, and re-layouts: 1.7 us -> 0.17 us
    pallas_call x2 -> x3, Pallas kernels: 2.5 us -> 1.59 us  [the longest x1 0.73 us: branched_out(): pl.pallas_call(branch_out, out_shape=tuple((pltpu.VMEM(shape, jnp.bfloat1...]
    ppermute x6, waiting for transfers between devices: 3.35 us -> 4.21 us  [swapped(): return lax.ppermute(array, 'tp', SWAP)]
  transfers between devices with their start and end apart: 9 -> 7, of which waited for: 6 -> 6; matrix products, arithmetic and copies ran while one was open for 5% -> 0% of each run, Pallas kernels for 0% -> 1%
where the time goes in v6:
time: 78.8 us; the launch traced here: 78.2 us
  blocking collectives  44.4 us (56%)
  starting transfers between devices  14.3 us (18%)
  waiting for transfers between devices  11.5 us (15%)
  Pallas kernels  6.5 us (8%)
    all_to_all x3, blocking collectives, exchanged(): return lax.all_to_all(array, axis, split_axis=0, concat_axis=0, tiled=True)  44.4 us
    ppermute x6, starting transfers between devices, swapped(): return lax.ppermute(array, 'tp', SWAP)  7.8 us
    all_to_all x1, waiting for transfers between devices, exchanged(): return lax.all_to_all(array, axis, split_axis=0, concat_axis=0, tiled=True)  7.24 us
    all_to_all x1, starting transfers between devices, exchanged(): return lax.all_to_all(array, axis, split_axis=0, concat_axis=0, tiled=True)  6.49 us
    ppermute x6, waiting for transfers between devices, swapped(): return lax.ppermute(array, 'tp', SWAP)  4.21 us
    pallas_call x1, Pallas kernels, attended(): pl.pallas_call(attend, out_shape=(pltpu.VMEM(tokens.shape, jnp.bfloat16),...  3.49 us
  transfers between devices with their start and end apart: 7, of which 6 were waited for; matrix products, arithmetic and copies ran while one was open for 0% of the time, Pallas kernels for 1%

profile of v6, /device:TPU:1, one launch (start us, length us, event | category | flops | bytes accessed | tf_op | source)
XLA Modules:
  0.0 78.2 jit_solution(3448417320761232047)
XLA Ops:
  0.0 0.0 copy-start.3
  0.0 0.0 copy-start.1
  0.0 0.0 copy-start.2
  0.0 3.5 %attend.1 = (bf16[8,2048]{1,0:T(8,128)(2,1)S(1)}, bf16[8,8,256]{2,1,0:T(8,128)(2,1)S(1)}) custom-call(bf16[8,2048]{1,0:T(8,128)(2,1)} %tokens.1, bf16[2048]{0:T(1024)(128)(2,1)} %refs_1_.1, bf16[2048,128]{1,0:T(8,128)(2,1)} %refs_2_.1, bf16[16,2048]{1,0:T(8,128)(2,1)} %bitcast.26, bf16[2048,128]{1,0:T(8,128)(2,1)} %refs_4_.1, bf16[16,128]{1,0:T(8,128)(2,1)} %refs_5_.1, ...), custom_call_target="tpu_custom_call" | custom-call | tf_op jit(solution)/shard_map/attend/pallas_call | solution.py:135
  3.5 3.3 %collective-permute-start = (bf16[8,2048]{1,0:T(8,128)(2,1)S(1)}, bf16[8,2048]{1,0:T(8,128)(2,1)S(1)}, u32[]{:S(2)}, u32[]{:S(2)}) collective-permute-start(bf16[8,2048]{1,0:T(8,128)(2,1)S(1)} %get-tuple-element.35.mine), channel_id=1, source_target_pairs={{0,1},{1,0},{2,3},{3,2},{4,5},{5,4},{6,7},{7,6},{8,9},{9,8},{10,11... | collective-permute-start | bytes 98312 | tf_op jit(solution)/shard_map/ppermute | solution.py:24
  6.8 0.0 copy-start.4
  6.8 0.9 %collective-permute-done.theirs = bf16[8,2048]{1,0:T(8,128)(2,1)S(1)} collective-permute-done((bf16[8,2048]{1,0:T(8,128)(2,1)S(1)}, bf16[8,2048]{1,0:T(8,128)(2,1)S(1)}, u32[]{:S(2)}, u32[]{:S(2)}) %collective-permute-start) | collective-permute-done | bytes 32800 | tf_op jit(solution)/shard_map/ppermute | solution.py:24
  7.6 0.0 copy-done.3
  7.7 0.0 copy-done.4
  7.7 0.9 %assemble.1 = (bf16[8,8,1280]{2,1,0:T(8,128)(2,1)}, f32[8,1024]{1,0:T(8,128)S(1)}) custom-call(s32[1]{0:T(128)} %bitcast.core, bf16[8,2048]{1,0:T(8,128)(2,1)S(1)} %copy-done.3, bf16[8,2048]{1,0:T(8,128)(2,1)S(1)} %get-tuple-element.35.mine, bf16[8,2048]{1,0:T(8,128)(2,1)S(1)} %collective-permute-done.theirs, bf16[2048]{0:T(1024)(128)(2,1)S(1)} %copy-done.4, ...), custom_call_target="tpu_custom_call" | custom-call | tf_op jit(solution)/shard_map/assemble/pallas_call | solution.py:172
  8.5 0.0 copy-done.1
  8.5 0.0 copy-done.2
  8.6 0.0 copy-start
  8.6 0.1 pad_maximum_fusion
  8.7 0.4 collective-permute-start.1
  9.1 6.5 %all-to-all-start = ((bf16[8,8,1280]{2,1,0:T(8,128)(2,1)}), bf16[8,8,1280]{2,1,0:T(8,128)(2,1)S(1)}, u32[]{:S(2)}, u32[]{:S(2)}) async-start(bf16[8,8,1280]{2,1,0:T(8,128)(2,1)} %get-tuple-element.39), calls=%async_computation | async-start | bytes 327680 | tf_op jit(solution)/shard_map/all_to_all | solution.py:33
  15.6 0.0 copy-done
  15.6 0.0 copy-start.5
  15.6 0.5 collective-permute-start.2
  16.2 0.1 copy-done.5
  16.3 1.0 %collective-permute-done.2.far = bf16[128,1024]{1,0:T(8,128)(2,1)S(1)} collective-permute-done((bf16[128,1024]{1,0:T(8,128)(2,1)S(1)}, bf16[128,1024]{1,0:T(8,128)(2,1)S(1)}, u32[]{:S(2)}, u32[]{:S(2)}) %collective-permute-start.2) | collective-permute-done | bytes 262176 | tf_op jit(solution)/shard_map/ppermute | solution.py:24
  17.3 7.2 %all-to-all-done = bf16[8,8,1280]{2,1,0:T(8,128)(2,1)S(1)} async-done(((bf16[8,8,1280]{2,1,0:T(8,128)(2,1)}), bf16[8,8,1280]{2,1,0:T(8,128)(2,1)S(1)}, u32[]{:S(2)}, u32[]{:S(2)}) %all-to-all-start) | async-done | bytes 163872 | tf_op jit(solution)/shard_map/all_to_all | solution.py:33
  24.6 0.0 collective-permute-done.1.far
  24.6 0.4 route.1
  25.0 20.5 %all_to_all.20.arrived = bf16[16,16,1792]{2,1,0:T(8,128)(2,1)S(1)} all-to-all(bf16[16,16,1792]{2,1,0:T(8,128)(2,1)S(1)} %get-tuple-element.44), channel_id=1, replica_groups=mesh['ep_0'=8,'ep_1'=4,'ep_2'=4,'tp'=2] {'ep_1','ep_2'}, dimensions={0} | all-to-all | bytes 1835008 | tf_op jit(solution)/shard_map/all_to_all | solution.py:33
  45.5 2.9 %collective-permute-start.4 = (bf16[64,1024]{1,0:T(8,128)(2,1)S(1)}, bf16[64,1024]{1,0:T(8,128)(2,1)S(1)}, u32[]{:S(2)}, u32[]{:S(2)}) collective-permute-start(bf16[64,1024]{1,0:T(8,128)(2,1)S(1)} %get-tuple-element.54), channel_id=1, source_target_pairs={{0,1},{1,0},{2,3},{3,2},{4,5},{5,4},{6,7},{7,6},{8,9},{9,8},{10,11... | collective-permute-start | bytes 393224 | tf_op jit(solution)/shard_map/ppermute | solution.py:24
  48.4 1.0 %collective-permute-done.4.rest = bf16[64,1024]{1,0:T(8,128)(2,1)S(1)} collective-permute-done((bf16[64,1024]{1,0:T(8,128)(2,1)S(1)}, bf16[64,1024]{1,0:T(8,128)(2,1)S(1)}, u32[]{:S(2)}, u32[]{:S(2)}) %collective-permute-start.4) | collective-permute-done | bytes 131104 | tf_op jit(solution)/shard_map/ppermute | solution.py:24
  49.3 0.7 branch_out.1
  50.1 0.4 collective-permute-start.5
  50.5 0.6 widen.1
  51.1 0.2 collective-permute-start.3
  51.3 0.2 collective-permute-done.5
  51.6 1.2 %collective-permute-done.3.came = bf16[256,512]{1,0:T(8,128)(2,1)S(1)} collective-permute-done((bf16[256,512]{1,0:T(8,128)(2,1)S(1)}, bf16[256,512]{1,0:T(8,128)(2,1)S(1)}, u32[]{:S(2)}, u32[]{:S(2)}) %collective-permute-start.3) | collective-permute-done | bytes 262176 | tf_op jit(solution)/shard_map/ppermute | solution.py:24
  52.7 0.4 narrow.1
  53.2 13.6 %all_to_all.21 = bf16[16,16,1024]{2,1,0:T(8,128)(2,1)S(1)} all-to-all(bf16[16,16,1024]{2,1,0:T(8,128)(2,1)S(1)} %narrow.1), channel_id=1, replica_groups=mesh['ep_0'=8,'ep_1'=4,'ep_2'=4,'tp'=2] {'ep_1','ep_2'}, dimensions={0} | all-to-all | bytes 1048576 | tf_op jit(solution)/shard_map/all_to_all | solution.py:33
  66.8 0.2 fusion.4
  67.0 0.2 fusion.2
  67.3 10.3 %all_to_all.22 = bf16[8,8,1024]{2,1,0:T(8,128)(2,1)S(1)} all-to-all(bf16[8,8,1024]{2,1,0:T(8,128)(2,1)S(1)} %fusion.2), channel_id=1, replica_groups=mesh['ep_0'=8,'ep_1'=4,'ep_2'=4,'tp'=2] {'ep_0'}, dimensions={0} | all-to-all | bytes 262144 | tf_op jit(solution)/shard_map/all_to_all | solution.py:33
  77.6 0.6 add_convert_fusion
  (5 shorter events, 0.1 us)
Async XLA Ops:
  0.0 7.7 %copy-start.3 = (bf16[8,2048]{1,0:T(8,128)(2,1)S(1)}, bf16[8,2048]{1,0:T(8,128)(2,1)}, u32[]{:S(2)}) copy-start(bf16[8,2048]{1,0:T(8,128)(2,1)} %tokens.1) | copy-start | bytes 98308
  0.0 8.5 %copy-start.1 = (bf16[1,2048,128]{2,1,0:T(8,128)(2,1)S(1)}, bf16[1,2048,128]{2,1,0:T(8,128)(2,1)}, u32[]{:S(2)}) copy-start(bf16[1,2048,128]{2,1,0:T(8,128)(2,1)} %param.35) | copy-start | bytes 1572868
  0.0 8.5 %copy-start.2 = (bf16[1,2048,128]{2,1,0:T(8,128)(2,1)S(1)}, bf16[1,2048,128]{2,1,0:T(8,128)(2,1)}, u32[]{:S(2)}) copy-start(bf16[1,2048,128]{2,1,0:T(8,128)(2,1)} %param.36) | copy-start | bytes 1572868
  3.5 4.1 %collective-permute-start = (bf16[8,2048]{1,0:T(8,128)(2,1)S(1)}, bf16[8,2048]{1,0:T(8,128)(2,1)S(1)}, u32[]{:S(2)}, u32[]{:S(2)}) collective-permute-start(bf16[8,2048]{1,0:T(8,128)(2,1)S(1)} %get-tuple-element.35.mine), channel_id=1, source_target_pairs={{0,1},{1,0},{2,3},{3,2},{4,5},{5,4},{6,7},{7,6},{8,9},{9,8},{10,11... | collective-permute-start | bytes 98312 | tf_op jit(solution)/shard_map/ppermute | solution.py:24
  6.8 0.9 %copy-start.4 = (bf16[2048]{0:T(1024)(128)(2,1)S(1)}, bf16[2048]{0:T(1024)(128)(2,1)}, u32[]{:S(2)}) copy-start(bf16[2048]{0:T(1024)(128)(2,1)} %gain.1) | copy-start | bytes 12292
  8.6 7.0 %copy-start = (bf16[1,128,2048]{2,1,0:T(8,128)(2,1)S(1)}, bf16[1,128,2048]{2,1,0:T(8,128)(2,1)}, u32[]{:S(2)}) copy-start(bf16[1,128,2048]{2,1,0:T(8,128)(2,1)} %param.37) | copy-start | bytes 1572868
  8.7 15.9 %collective-permute-start.1 = (bf16[1024,256]{1,0:T(8,128)(2,1)S(1)}, bf16[1024,256]{1,0:T(8,128)(2,1)S(1)}, u32[]{:S(2)}, u32[]{:S(2)}) collective-permute-start(bf16[1024,256]{1,0:T(8,128)(2,1)S(1)} %pad_maximum_fusion), channel_id=1, source_target_pairs={{0,1},{1,0},{2,3},{3,2},{4,5},{5,4},{6,7},{7,6},{8,9},{9,8},{10,11... | collective-permute-start | bytes 1572872 | tf_op jit(solution)/shard_map/ppermute | solution.py:24
  9.1 15.5 %all-to-all-start = ((bf16[8,8,1280]{2,1,0:T(8,128)(2,1)}), bf16[8,8,1280]{2,1,0:T(8,128)(2,1)S(1)}, u32[]{:S(2)}, u32[]{:S(2)}) async-start(bf16[8,8,1280]{2,1,0:T(8,128)(2,1)} %get-tuple-element.39), calls=%async_computation | async-start | bytes 327680 | tf_op jit(solution)/shard_map/all_to_all | solution.py:33
  15.6 0.7 copy-start.5
  15.6 1.7 %collective-permute-start.2 = (bf16[128,1024]{1,0:T(8,128)(2,1)S(1)}, bf16[128,1024]{1,0:T(8,128)(2,1)S(1)}, u32[]{:S(2)}, u32[]{:S(2)}) collective-permute-start(bf16[128,1024]{1,0:T(8,128)(2,1)S(1)} %constant_dynamic-slice_fusion), channel_id=1, source_target_pairs={{0,1},{1,0},{2,3},{3,2},{4,5},{5,4},{6,7},{7,6},{8,9},{9,8},{10,11... | collective-permute-start | bytes 786440 | tf_op jit(solution)/shard_map/ppermute | solution.py:24
  45.5 3.9 %collective-permute-start.4 = (bf16[64,1024]{1,0:T(8,128)(2,1)S(1)}, bf16[64,1024]{1,0:T(8,128)(2,1)S(1)}, u32[]{:S(2)}, u32[]{:S(2)}) collective-permute-start(bf16[64,1024]{1,0:T(8,128)(2,1)S(1)} %get-tuple-element.54), channel_id=1, source_target_pairs={{0,1},{1,0},{2,3},{3,2},{4,5},{5,4},{6,7},{7,6},{8,9},{9,8},{10,11... | collective-permute-start | bytes 393224 | tf_op jit(solution)/shard_map/ppermute | solution.py:24
  50.1 1.4 %collective-permute-start.5 = (bf16[64,1024]{1,0:T(8,128)(2,1)S(1)}, bf16[64,1024]{1,0:T(8,128)(2,1)S(1)}, u32[]{:S(2)}, u32[]{:S(2)}) collective-permute-start(bf16[64,1024]{1,0:T(8,128)(2,1)S(1)} %get-tuple-element.58), channel_id=1, source_target_pairs={{0,1},{1,0},{2,3},{3,2},{4,5},{5,4},{6,7},{7,6},{8,9},{9,8},{10,11... | collective-permute-start | bytes 393224 | tf_op jit(solution)/shard_map/ppermute | solution.py:24
  51.1 1.6 %collective-permute-start.3 = (bf16[256,512]{1,0:T(8,128)(2,1)S(1)}, bf16[256,512]{1,0:T(8,128)(2,1)S(1)}, u32[]{:S(2)}, u32[]{:S(2)}) collective-permute-start(bf16[256,512]{1,0:T(8,128)(2,1)S(1)} %get-tuple-element.51), channel_id=1, source_target_pairs={{0,1},{1,0},{2,3},{3,2},{4,5},{5,4},{6,7},{7,6},{8,9},{9,8},{10,11... | collective-permute-start | bytes 786440 | tf_op jit(solution)/shard_map/ppermute | solution.py:24

commit v7 on v6

--- a/solution.py
+++ b/solution.py
@@ -294,45 +294,34 @@
     )(core, *[in_vmem(a) for a in (pre, came, down, far)])
 
 
-def branch_out(core, arrived, line, rest, mark_own, mark_rest, keep, sent, high, low):
+def matrix_of(arrived, m, half):
     planes, depth, _ = arrived.shape
-    count, half = rest.shape
+    starts = [half + 256 * m + 128 * p for p in range(2)]
+    blocks = [arrived[:, :, at : at + 128].reshape(planes * depth, 128) for at in starts]
+    return jnp.concatenate(blocks, axis=0)
+
+
+def added(source, marks, arrived, first, gate, up, pre):
+    count, half = source.shape
     quarter = half // 2
-
-    def matrix(m):
-        starts = [half + 256 * m + 128 * p for p in range(2)]
-        blocks = [arrived[:, :, at : at + 128].reshape(planes * depth, 128) for at in starts]
-        return jnp.concatenate(blocks, axis=0)
-
     group = lax.broadcasted_iota(jnp.int32, (count, 128), 1) // 32
-    both = jnp.concatenate([matrix(0), matrix(1)], axis=1)
-    gate = jnp.zeros((count, 128), jnp.float32)
-    up = jnp.zeros((count, 128), jnp.float32)
-    pre = jnp.zeros((count, 1), jnp.float32)
-    for source, marks, first in (
-        (line[:, :half], mark_own, 2 * core[0]),
-        (rest[...], mark_rest, 2 - 2 * core[0]),
-    ):
-        wide = source.astype(jnp.float32) * marks[...].astype(jnp.float32)[None, :]
-        pre = pre + jnp.sum(wide, axis=1, keepdims=True)
-        for k in range(2):
-            part = dot(source[:, k * quarter : (k + 1) * quarter], both)
-            gate = gate + jnp.where(group == first + k, part[:, :128], 0.0)
-            up = up + jnp.where(group == first + k, part[:, 128:], 0.0)
-
-    def folded(total):
-        return total + sum(pltpu.roll(total, 32 * k, 1) for k in range(1, 4))
-
-    gate = folded(gate)
-    hidden = gate / (1.0 + jnp.exp(-gate)) * folded(up)
-    branch = 1.0 / (1.0 + jnp.exp(-pre))
-    down = matrix(2)
-    for target, first in ((sent, 2 - 2 * core[0]), (keep, 2 * core[0])):
-        for k in range(2):
-            units = jnp.where(group == first + k, hidden, 0.0).astype(jnp.bfloat16)
-            target[:, k * quarter : (k + 1) * quarter] = (
-                branch * dot(units, down, ((1,), (1,)))
-            ).astype(jnp.bfloat16)
+    both = jnp.concatenate([matrix_of(arrived, m, half) for m in range(2)], axis=1)
+    wide = source.astype(jnp.float32) * marks[...].astype(jnp.float32)[None, :]
+    pre = pre + jnp.sum(wide, axis=1, keepdims=True)
+    for k in range(2):
+        part = dot(source[:, k * quarter : (k + 1) * quarter], both)
+        gate = gate + jnp.where(group == first + k, part[:, :128], 0.0)
+        up = up + jnp.where(group == first + k, part[:, 128:], 0.0)
+    return gate, up, pre
+
+
+def branch_in(core, arrived, line, marks, gate, up, pre, high, low):
+    planes, depth, _ = arrived.shape
+    count, half = line.shape[0], line.shape[1] - 256
+    zero = jnp.zeros((count, 128), jnp.float32)
+    gate[...], up[...], pre[...] = added(
+        line[:, :half], marks, arrived, 2 * core[0], zero, zero, zero
+    )
 
     slots = planes * depth
     row = lax.broadcasted_iota(jnp.int32, (slots, 128), 0)
@@ -351,19 +340,37 @@
     low[...] = (weighing - upper.astype(jnp.float32)).astype(jnp.bfloat16)
 
 
-def branched_out(core, arrived, line, rest, mark_own, mark_rest):
-    slots = arrived.shape[0] * arrived.shape[1]
-    return pl.pallas_call(
-        branch_out,
-        out_shape=tuple(
-            pltpu.VMEM(shape, jnp.bfloat16)
-            for shape in (rest.shape, rest.shape, (slots, line.shape[0]), (slots, line.shape[0]))
-        ),
-        in_specs=[pl.BlockSpec(memory_space=pltpu.SMEM)] + [NEAR] * 5,
-        out_specs=(NEAR,) * 4,
+def branch_out(core, arrived, rest, marks, gate_own, up_own, pre_own, keep, sent):
+    count, half = rest.shape
+    quarter = half // 2
+    group = lax.broadcasted_iota(jnp.int32, (count, 128), 1) // 32
+    gate, up, pre = added(
+        rest[...], marks, arrived, 2 - 2 * core[0], gate_own[...], up_own[...], pre_own[...]
+    )
+
+    def folded(total):
+        return total + sum(pltpu.roll(total, 32 * k, 1) for k in range(1, 4))
+
+    gate = folded(gate)
+    hidden = gate / (1.0 + jnp.exp(-gate)) * folded(up)
+    branch = 1.0 / (1.0 + jnp.exp(-pre[:, :1]))
+    down = matrix_of(arrived, 2, half)
+    for target, first in ((sent, 2 - 2 * core[0]), (keep, 2 * core[0])):
+        for k in range(2):
+            units = jnp.where(group == first + k, hidden, 0.0).astype(jnp.bfloat16)
+            target[:, k * quarter : (k + 1) * quarter] = (
+                branch * dot(units, down, ((1,), (1,)))
+            ).astype(jnp.bfloat16)
+
+
+def on_core(kernel, shapes, core, *arrays):
+    return pl.pallas_call(
+        kernel,
+        out_shape=tuple(pltpu.VMEM(shape, kind) for shape, kind in shapes),
+        in_specs=[pl.BlockSpec(memory_space=pltpu.SMEM)] + [NEAR] * len(arrays),
+        out_specs=(NEAR,) * len(shapes),
         compiler_params=SMALL,
-        name="branch_out",
-    )(core, *[in_vmem(a) for a in (arrived, line, rest, mark_own, mark_rest)])
+    )(core, *[in_vmem(a) for a in arrays])
 
 
 def shards(
@@ -423,8 +430,15 @@
     rest = swapped(line_half)
     pre, sent = widened(which, arrived, gate, up, far_in)
     came = swapped(sent)
-    keep, given_part, weigh_high, weigh_low = branched_out(
-        which, arrived, line, rest, mark_own, mark_rest
+    count = lines * rows_dev
+    *sums, weigh_high, weigh_low = on_core(
+        branch_in,
+        [((count, 128), jnp.float32)] * 3 + [((slots, count), jnp.bfloat16)] * 2,
+        which, arrived, line, mark_own,
+    )
+    keep, given_part = on_core(
+        branch_out, [((count, half), jnp.bfloat16)] * 2,
+        which, arrived, rest, mark_rest, *sums,
     )
     given_part = swapped(given_part)
     summed = narrowed(which, pre, came, down, far_down, plane)

time: 78.8 us -> 78.6 us (level)
  no operation moved by 1% of the time
where the time goes in v7:
time: 78.6 us; the launch traced here: 78 us
  blocking collectives  44.4 us (56%)
  starting transfers between devices  14.3 us (18%)
  waiting for transfers between devices  11.1 us (14%)
  Pallas kernels  6.62 us (8%)
    all_to_all x3, blocking collectives, exchanged(): return lax.all_to_all(array, axis, split_axis=0, concat_axis=0, tiled=True)  44.4 us
    ppermute x6, starting transfers between devices, swapped(): return lax.ppermute(array, 'tp', SWAP)  7.8 us
    all_to_all x1, waiting for transfers between devices, exchanged(): return lax.all_to_all(array, axis, split_axis=0, concat_axis=0, tiled=True)  7.24 us
    all_to_all x1, starting transfers between devices, exchanged(): return lax.all_to_all(array, axis, split_axis=0, concat_axis=0, tiled=True)  6.49 us
    ppermute x6, waiting for transfers between devices, swapped(): return lax.ppermute(array, 'tp', SWAP)  3.89 us
    pallas_call x1, Pallas kernels, attended(): pl.pallas_call(attend, out_shape=(pltpu.VMEM(tokens.shape, jnp.bfloat16),...  3.49 us
  transfers between devices with their start and end apart: 7, of which 6 were waited for; matrix products, arithmetic and copies ran while one was open for 0% of the time, Pallas kernels for 1%

profile of v7, /device:TPU:1, one launch (start us, length us, event | category | flops | bytes accessed | tf_op | source)
XLA Modules:
  0.0 78.0 jit_solution(1010851641617950196)
XLA Ops:
  0.0 0.0 copy-start.3
  0.0 0.0 copy-start.1
  0.0 0.0 copy-start.2
  0.0 3.5 %attend.1 = (bf16[8,2048]{1,0:T(8,128)(2,1)S(1)}, bf16[8,8,256]{2,1,0:T(8,128)(2,1)S(1)}) custom-call(bf16[8,2048]{1,0:T(8,128)(2,1)} %tokens.1, bf16[2048]{0:T(1024)(128)(2,1)} %refs_1_.1, bf16[2048,128]{1,0:T(8,128)(2,1)} %refs_2_.1, bf16[16,2048]{1,0:T(8,128)(2,1)} %bitcast.26, bf16[2048,128]{1,0:T(8,128)(2,1)} %refs_4_.1, bf16[16,128]{1,0:T(8,128)(2,1)} %refs_5_.1, ...), custom_call_target="tpu_custom_call" | custom-call | tf_op jit(solution)/shard_map/attend/pallas_call | solution.py:135
  3.5 3.3 %collective-permute-start = (bf16[8,2048]{1,0:T(8,128)(2,1)S(1)}, bf16[8,2048]{1,0:T(8,128)(2,1)S(1)}, u32[]{:S(2)}, u32[]{:S(2)}) collective-permute-start(bf16[8,2048]{1,0:T(8,128)(2,1)S(1)} %get-tuple-element.38.mine), channel_id=1, source_target_pairs={{0,1},{1,0},{2,3},{3,2},{4,5},{5,4},{6,7},{7,6},{8,9},{9,8},{10,11... | collective-permute-start | bytes 98312 | tf_op jit(solution)/shard_map/ppermute | solution.py:24
  6.8 0.0 copy-start.4
  6.8 0.9 %collective-permute-done.theirs = bf16[8,2048]{1,0:T(8,128)(2,1)S(1)} collective-permute-done((bf16[8,2048]{1,0:T(8,128)(2,1)S(1)}, bf16[8,2048]{1,0:T(8,128)(2,1)S(1)}, u32[]{:S(2)}, u32[]{:S(2)}) %collective-permute-start) | collective-permute-done | bytes 32800 | tf_op jit(solution)/shard_map/ppermute | solution.py:24
  7.6 0.0 copy-done.3
  7.7 0.0 copy-done.4
  7.7 0.9 %assemble.1 = (bf16[8,8,1280]{2,1,0:T(8,128)(2,1)}, f32[8,1024]{1,0:T(8,128)S(1)}) custom-call(s32[1]{0:T(128)} %bitcast.core, bf16[8,2048]{1,0:T(8,128)(2,1)S(1)} %copy-done.3, bf16[8,2048]{1,0:T(8,128)(2,1)S(1)} %get-tuple-element.38.mine, bf16[8,2048]{1,0:T(8,128)(2,1)S(1)} %collective-permute-done.theirs, bf16[2048]{0:T(1024)(128)(2,1)S(1)} %copy-done.4, ...), custom_call_target="tpu_custom_call" | custom-call | tf_op jit(solution)/shard_map/assemble/pallas_call | solution.py:172
  8.5 0.0 copy-done.1
  8.5 0.0 copy-done.2
  8.6 0.0 copy-start
  8.6 0.1 pad_maximum_fusion
  8.7 0.4 collective-permute-start.1
  9.1 6.5 %all-to-all-start = ((bf16[8,8,1280]{2,1,0:T(8,128)(2,1)}), bf16[8,8,1280]{2,1,0:T(8,128)(2,1)S(1)}, u32[]{:S(2)}, u32[]{:S(2)}) async-start(bf16[8,8,1280]{2,1,0:T(8,128)(2,1)} %get-tuple-element.42), calls=%async_computation | async-start | bytes 327680 | tf_op jit(solution)/shard_map/all_to_all | solution.py:33
  15.6 0.0 copy-done
  15.6 0.0 copy-start.5
  15.6 0.5 collective-permute-start.2
  16.2 0.1 copy-done.5
  16.3 1.0 %collective-permute-done.2.far = bf16[128,1024]{1,0:T(8,128)(2,1)S(1)} collective-permute-done((bf16[128,1024]{1,0:T(8,128)(2,1)S(1)}, bf16[128,1024]{1,0:T(8,128)(2,1)S(1)}, u32[]{:S(2)}, u32[]{:S(2)}) %collective-permute-start.2) | collective-permute-done | bytes 262176 | tf_op jit(solution)/shard_map/ppermute | solution.py:24
  17.3 7.2 %all-to-all-done = bf16[8,8,1280]{2,1,0:T(8,128)(2,1)S(1)} async-done(((bf16[8,8,1280]{2,1,0:T(8,128)(2,1)}), bf16[8,8,1280]{2,1,0:T(8,128)(2,1)S(1)}, u32[]{:S(2)}, u32[]{:S(2)}) %all-to-all-start) | async-done | bytes 163872 | tf_op jit(solution)/shard_map/all_to_all | solution.py:33
  24.6 0.0 collective-permute-done.1.far
  24.6 0.4 route.1
  25.0 20.5 %all_to_all.20.arrived = bf16[16,16,1792]{2,1,0:T(8,128)(2,1)S(1)} all-to-all(bf16[16,16,1792]{2,1,0:T(8,128)(2,1)S(1)} %get-tuple-element.47), channel_id=1, replica_groups=mesh['ep_0'=8,'ep_1'=4,'ep_2'=4,'tp'=2] {'ep_1','ep_2'}, dimensions={0} | all-to-all | bytes 1835008 | tf_op jit(solution)/shard_map/all_to_all | solution.py:33
  45.5 2.9 %collective-permute-start.4 = (bf16[64,1024]{1,0:T(8,128)(2,1)S(1)}, bf16[64,1024]{1,0:T(8,128)(2,1)S(1)}, u32[]{:S(2)}, u32[]{:S(2)}) collective-permute-start(bf16[64,1024]{1,0:T(8,128)(2,1)S(1)} %get-tuple-element.57), channel_id=1, source_target_pairs={{0,1},{1,0},{2,3},{3,2},{4,5},{5,4},{6,7},{7,6},{8,9},{9,8},{10,11... | collective-permute-start | bytes 393224 | tf_op jit(solution)/shard_map/ppermute | solution.py:24
  48.4 0.3 shard_map.199
  48.7 0.7 collective-permute-done.4.rest
  49.3 0.5 shard_map.200
  49.9 0.4 collective-permute-start.5
  50.3 0.6 widen.1
  50.9 0.2 collective-permute-start.3
  51.1 0.2 collective-permute-done.5
  51.4 1.2 %collective-permute-done.3.came = bf16[256,512]{1,0:T(8,128)(2,1)S(1)} collective-permute-done((bf16[256,512]{1,0:T(8,128)(2,1)S(1)}, bf16[256,512]{1,0:T(8,128)(2,1)S(1)}, u32[]{:S(2)}, u32[]{:S(2)}) %collective-permute-start.3) | collective-permute-done | bytes 262176 | tf_op jit(solution)/shard_map/ppermute | solution.py:24
  52.5 0.4 narrow.1
  53.0 13.6 %all_to_all.21 = bf16[16,16,1024]{2,1,0:T(8,128)(2,1)S(1)} all-to-all(bf16[16,16,1024]{2,1,0:T(8,128)(2,1)S(1)} %narrow.1), channel_id=1, replica_groups=mesh['ep_0'=8,'ep_1'=4,'ep_2'=4,'tp'=2] {'ep_1','ep_2'}, dimensions={0} | all-to-all | bytes 1048576 | tf_op jit(solution)/shard_map/all_to_all | solution.py:33
  66.6 0.2 fusion.4
  66.8 0.2 fusion.2
  67.1 10.3 %all_to_all.22 = bf16[8,8,1024]{2,1,0:T(8,128)(2,1)S(1)} all-to-all(bf16[8,8,1024]{2,1,0:T(8,128)(2,1)S(1)} %fusion.2), channel_id=1, replica_groups=mesh['ep_0'=8,'ep_1'=4,'ep_2'=4,'tp'=2] {'ep_0'}, dimensions={0} | all-to-all | bytes 262144 | tf_op jit(solution)/shard_map/all_to_all | solution.py:33
  77.4 0.6 add_convert_fusion
  (5 shorter events, 0.1 us)
Async XLA Ops:
  0.0 7.7 %copy-start.3 = (bf16[8,2048]{1,0:T(8,128)(2,1)S(1)}, bf16[8,2048]{1,0:T(8,128)(2,1)}, u32[]{:S(2)}) copy-start(bf16[8,2048]{1,0:T(8,128)(2,1)} %tokens.1) | copy-start | bytes 98308
  0.0 8.5 %copy-start.1 = (bf16[1,2048,128]{2,1,0:T(8,128)(2,1)S(1)}, bf16[1,2048,128]{2,1,0:T(8,128)(2,1)}, u32[]{:S(2)}) copy-start(bf16[1,2048,128]{2,1,0:T(8,128)(2,1)} %param.35) | copy-start | bytes 1572868
  0.0 8.5 %copy-start.2 = (bf16[1,2048,128]{2,1,0:T(8,128)(2,1)S(1)}, bf16[1,2048,128]{2,1,0:T(8,128)(2,1)}, u32[]{:S(2)}) copy-start(bf16[1,2048,128]{2,1,0:T(8,128)(2,1)} %param.36) | copy-start | bytes 1572868
  3.5 4.1 %collective-permute-start = (bf16[8,2048]{1,0:T(8,128)(2,1)S(1)}, bf16[8,2048]{1,0:T(8,128)(2,1)S(1)}, u32[]{:S(2)}, u32[]{:S(2)}) collective-permute-start(bf16[8,2048]{1,0:T(8,128)(2,1)S(1)} %get-tuple-element.38.mine), channel_id=1, source_target_pairs={{0,1},{1,0},{2,3},{3,2},{4,5},{5,4},{6,7},{7,6},{8,9},{9,8},{10,11... | collective-permute-start | bytes 98312 | tf_op jit(solution)/shard_map/ppermute | solution.py:24
  6.8 0.9 %copy-start.4 = (bf16[2048]{0:T(1024)(128)(2,1)S(1)}, bf16[2048]{0:T(1024)(128)(2,1)}, u32[]{:S(2)}) copy-start(bf16[2048]{0:T(1024)(128)(2,1)} %gain.1) | copy-start | bytes 12292
  8.6 7.0 %copy-start = (bf16[1,128,2048]{2,1,0:T(8,128)(2,1)S(1)}, bf16[1,128,2048]{2,1,0:T(8,128)(2,1)}, u32[]{:S(2)}) copy-start(bf16[1,128,2048]{2,1,0:T(8,128)(2,1)} %param.37) | copy-start | bytes 1572868
  8.7 15.9 %collective-permute-start.1 = (bf16[1024,256]{1,0:T(8,128)(2,1)S(1)}, bf16[1024,256]{1,0:T(8,128)(2,1)S(1)}, u32[]{:S(2)}, u32[]{:S(2)}) collective-permute-start(bf16[1024,256]{1,0:T(8,128)(2,1)S(1)} %pad_maximum_fusion), channel_id=1, source_target_pairs={{0,1},{1,0},{2,3},{3,2},{4,5},{5,4},{6,7},{7,6},{8,9},{9,8},{10,11... | collective-permute-start | bytes 1572872 | tf_op jit(solution)/shard_map/ppermute | solution.py:24
  9.1 15.5 %all-to-all-start = ((bf16[8,8,1280]{2,1,0:T(8,128)(2,1)}), bf16[8,8,1280]{2,1,0:T(8,128)(2,1)S(1)}, u32[]{:S(2)}, u32[]{:S(2)}) async-start(bf16[8,8,1280]{2,1,0:T(8,128)(2,1)} %get-tuple-element.42), calls=%async_computation | async-start | bytes 327680 | tf_op jit(solution)/shard_map/all_to_all | solution.py:33
  15.6 0.7 copy-start.5
  15.6 1.7 %collective-permute-start.2 = (bf16[128,1024]{1,0:T(8,128)(2,1)S(1)}, bf16[128,1024]{1,0:T(8,128)(2,1)S(1)}, u32[]{:S(2)}, u32[]{:S(2)}) collective-permute-start(bf16[128,1024]{1,0:T(8,128)(2,1)S(1)} %constant_dynamic-slice_fusion), channel_id=1, source_target_pairs={{0,1},{1,0},{2,3},{3,2},{4,5},{5,4},{6,7},{7,6},{8,9},{9,8},{10,11... | collective-permute-start | bytes 786440 | tf_op jit(solution)/shard_map/ppermute | solution.py:24
  45.5 3.9 %collective-permute-start.4 = (bf16[64,1024]{1,0:T(8,128)(2,1)S(1)}, bf16[64,1024]{1,0:T(8,128)(2,1)S(1)}, u32[]{:S(2)}, u32[]{:S(2)}) collective-permute-start(bf16[64,1024]{1,0:T(8,128)(2,1)S(1)} %get-tuple-element.57), channel_id=1, source_target_pairs={{0,1},{1,0},{2,3},{3,2},{4,5},{5,4},{6,7},{7,6},{8,9},{9,8},{10,11... | collective-permute-start | bytes 393224 | tf_op jit(solution)/shard_map/ppermute | solution.py:24
  49.9 1.4 %collective-permute-start.5 = (bf16[64,1024]{1,0:T(8,128)(2,1)S(1)}, bf16[64,1024]{1,0:T(8,128)(2,1)S(1)}, u32[]{:S(2)}, u32[]{:S(2)}) collective-permute-start(bf16[64,1024]{1,0:T(8,128)(2,1)S(1)} %get-tuple-element.64), channel_id=1, source_target_pairs={{0,1},{1,0},{2,3},{3,2},{4,5},{5,4},{6,7},{7,6},{8,9},{9,8},{10,11... | collective-permute-start | bytes 393224 | tf_op jit(solution)/shard_map/ppermute | solution.py:24
  50.9 1.6 %collective-permute-start.3 = (bf16[256,512]{1,0:T(8,128)(2,1)S(1)}, bf16[256,512]{1,0:T(8,128)(2,1)S(1)}, u32[]{:S(2)}, u32[]{:S(2)}) collective-permute-start(bf16[256,512]{1,0:T(8,128)(2,1)S(1)} %get-tuple-element.54), channel_id=1, source_target_pairs={{0,1},{1,0},{2,3},{3,2},{4,5},{5,4},{6,7},{7,6},{8,9},{9,8},{10,11... | collective-permute-start | bytes 786440 | tf_op jit(solution)/shard_map/ppermute | solution.py:24
